TPU v7x, 1024 devices: a whole 4x8x16 slice. The times are simulated.
1024 devices in a mesh: kv: 256 (over z, y, core), tp: 4 (over x).
Axes of the slice: x: 4, y: 8, z: 16, core: 2. Of those that a mesh axis runs over, the one named last changes fastest.
Arguments:
- layer_input: bfloat16 [49152, 2048], P('kv', 'tp'), may hold values from -0.109375 to 0.109375
- queries: bfloat16 [49152, 1024], P('kv', 'tp'), may hold values from -6 to 6
- keys: bfloat16 [49152, 256], P('kv', 'tp'), may hold values from -6 to 6
- values: bfloat16 [49152, 256], P('kv', 'tp'), may hold values from -6 to 6
- attn_out: bfloat16 [49152, 1024], P('kv', 'tp'), may hold values from -1.25 to 1.25
- grad_out: bfloat16 [49152, 1024], P('kv', 'tp'), may hold values from -128 to 128
- log_sum: float32 [49152, 16], P('kv', 'tp'), may hold values from 6 to 7.5
- chosen: int32 [768, 8], replicated, may hold values from -1 to 767, as said below
Outputs:
- grad_queries: bfloat16 [49152, 1024], P('kv', 'tp')
- grad_keys: bfloat16 [49152, 256], P('kv', 'tp')
- grad_values: bfloat16 [49152, 256], P('kv', 'tp')
- grad_weight: float32 [2048, 1024], P('kv', 'tp')
Inputs may be any that keep to these rules, and one draw needn't show every extreme that they name: Write R = 3 and call positions [s * 192, (s + 1) * 192) segment s. For query block b in segment c = b // R and level l < 4, the entries chosen[b, 2 l + i] for i < 2 name 2 different key blocks of segment c - g_l, with g = 1, 32, 64, 128; all of them are -1 where c - g_l is negative.
All inputs are finite; a program needn't handle non-finite values.
Results may differ from a plain program's by a relative error of at most 0.0053.
Values may be sent and summed in bfloat16 or wider, within the bound.
No kernel may reach another device: no remote copies, remote signals or barrier semaphores. Data moves between devices by JAX's collectives and lax.ppermute only.
A program may use at most 64 MiB of HBM per device.

v0:
```python
import jax
import jax.numpy as jnp
from jax import lax
from jax.sharding import Mesh
from jax.sharding import PartitionSpec as P

DH = 64
BLOCK = 64
PER = 2
KV = ("kv_0", "kv_1", "kv_2")


def shifted(block, axis, distance):
    devices = range(lax.axis_size(axis))
    route = [(i - distance, i) for i in devices if i - distance in devices]
    return lax.ppermute(block, axis, route)


def laid_out(tiles, dim):
    tiles = jnp.moveaxis(tiles, 0, dim)
    shape = tiles.shape
    return tiles.reshape(*shape[:dim], shape[dim] * shape[dim + 1], *shape[dim + 2 :])


def sent_to_all(x, axis):
    copies = jnp.broadcast_to(x, (lax.axis_size(axis), *x.shape))
    return lax.all_to_all(copies, axis, split_axis=0, concat_axis=0, tiled=True)


def gather_directly(x, axis, dim):
    return laid_out(sent_to_all(x, axis), dim)


def reduced_to_own(tiles, axes, sequence):
    inside = tiles.shape[1:]
    tiles = tiles.reshape(*(lax.axis_size(a) for a in axes), *inside)
    tiles = jnp.moveaxis(tiles, sequence, range(len(axes))).reshape(-1, *inside)
    for k in sequence:
        tiles = lax.psum_scatter(tiles, axes[k], scatter_dimension=0, tiled=True)
    return tiles[0]


def in_blocks(x, dim, length):
    before, after = (x.shape[:dim], x.shape[dim + 1 :])
    return jnp.moveaxis(x.reshape(*before, length, -1, *after), dim, 0)


def summed_rows_2(x, axes, sequence, dim):
    length = lax.axis_size(axes)
    return reduced_to_own(in_blocks(x, dim, length), axes, sequence)


def pair_terms(
    query_rows, grad_rows, lse_rows, delta_rows, key_rows, value_rows, keep_mask, scale_value
):
    scores = (
        jnp.einsum("pbkge,pcke->pkgbc", query_rows, key_rows, preferred_element_type=jnp.float32)
        * scale_value
    )
    lse_cols = jnp.transpose(lse_rows, (0, 2, 3, 1))[..., None]
    delta_cols = jnp.transpose(delta_rows, (0, 2, 3, 1))[..., None]
    weights = jnp.where(keep_mask[:, None, None], jnp.exp(scores - lse_cols), jnp.float32(0.0))
    weights_low = weights.astype(jnp.bfloat16)
    dweights = jnp.einsum(
        "pbkge,pcke->pkgbc", grad_rows, value_rows, preferred_element_type=jnp.float32
    )
    dscores = (weights * (dweights - delta_cols)).astype(jnp.bfloat16)
    grad_query = (
        jnp.einsum("pkgbc,pcke->pbkge", dscores, key_rows, preferred_element_type=jnp.float32)
        * scale_value
    )
    grad_key = (
        jnp.einsum("pkgbc,pbkge->pcke", dscores, query_rows, preferred_element_type=jnp.float32)
        * scale_value
    )
    grad_value = jnp.einsum(
        "pkgbc,pbkge->pcke", weights_low, grad_rows, preferred_element_type=jnp.float32
    )
    return (grad_query, grad_key, grad_value)


def repeat_rows(array_in):
    return jnp.repeat(array_in, PER, axis=0)


def fold_pairs(pair_array, blocks_here):
    return jnp.sum(pair_array.reshape((blocks_here, PER) + pair_array.shape[1:]), axis=1)


def to_owner(select_table, pair_array, blocks_here):
    shaped = pair_array.reshape((blocks_here, PER) + pair_array.shape[1:])
    return jnp.einsum("qpb,qpcke->bcke", select_table, shaped, precision=lax.Precision.HIGHEST)


def shards(layer_input, queries, keys, values, attn_out, grad_out, log_sum, chosen):
    axis_size = lax.axis_size(KV)
    my_index = lax.axis_index(KV)
    tok_rows = queries.shape[0]
    kv_heads = keys.shape[1] // DH
    q_heads = queries.shape[1] // DH
    group_size = q_heads // kv_heads
    blocks_here = tok_rows // BLOCK
    query_width = queries.shape[1]
    key_width = keys.shape[1]
    scale_value = DH ** (-0.5)
    distances = [1, axis_size // 8, axis_size // 4, axis_size // 2]
    query_rows = queries.reshape(blocks_here, BLOCK, kv_heads, group_size, DH)
    grad_rows = grad_out.reshape(blocks_here, BLOCK, kv_heads, group_size, DH)
    delta_flat = jnp.sum(
        (grad_out.astype(jnp.float32) * attn_out.astype(jnp.float32)).reshape(
            tok_rows, q_heads, DH
        ),
        axis=-1,
    )
    delta_rows = delta_flat.reshape(blocks_here, BLOCK, kv_heads, group_size)
    lse_rows = log_sum.reshape(blocks_here, BLOCK, kv_heads, group_size)
    key_rows = keys.reshape(blocks_here, BLOCK, kv_heads, DH)
    value_rows = values.reshape(blocks_here, BLOCK, kv_heads, DH)
    causal = lax.broadcasted_iota(jnp.int32, (BLOCK, BLOCK), 0) >= lax.broadcasted_iota(
        jnp.int32, (BLOCK, BLOCK), 1
    )
    own_keep = jnp.broadcast_to(causal, (blocks_here, BLOCK, BLOCK))
    grad_query, grad_key, grad_value = pair_terms(
        query_rows, grad_rows, lse_rows, delta_rows, key_rows, value_rows, own_keep, scale_value
    )
    block_ids = jnp.arange(blocks_here, dtype=jnp.int32)
    pair_count = blocks_here * PER
    key_pair = jnp.concatenate([keys, values], axis=1)
    query_many = repeat_rows(query_rows)
    grad_many = repeat_rows(grad_rows)
    lse_many = repeat_rows(lse_rows)
    delta_many = repeat_rows(delta_rows)
    for section_num, distance in enumerate(distances):
        listed = lax.dynamic_slice(
            chosen, (my_index * blocks_here, PER * section_num), (blocks_here, PER)
        )
        is_valid = listed >= 0
        offset = jnp.where(is_valid, listed - (my_index - distance) * blocks_here, 0)
        arrived = shifted(key_pair, KV, distance)
        far_keys = arrived[:, :key_width].reshape(blocks_here, BLOCK, kv_heads, DH)[
            offset.reshape(-1)
        ]
        far_values = arrived[:, key_width:].reshape(blocks_here, BLOCK, kv_heads, DH)[
            offset.reshape(-1)
        ]
        keep_pairs = jnp.broadcast_to(
            is_valid.reshape(-1)[:, None, None], (pair_count, BLOCK, BLOCK)
        )
        pair_query, pair_key, pair_value = pair_terms(
            query_many,
            grad_many,
            lse_many,
            delta_many,
            far_keys,
            far_values,
            keep_pairs,
            scale_value,
        )
        grad_query = grad_query + fold_pairs(pair_query, blocks_here)
        select_table = ((offset[..., None] == block_ids) & is_valid[..., None]).astype(jnp.float32)
        back_key = to_owner(select_table, pair_key, blocks_here).reshape(tok_rows, key_width)
        back_value = to_owner(select_table, pair_value, blocks_here).reshape(tok_rows, key_width)
        returned = shifted(jnp.concatenate([back_key, back_value], axis=1), KV, -distance)
        grad_key = grad_key + returned[:, :key_width].reshape(blocks_here, BLOCK, kv_heads, DH)
        grad_value = grad_value + returned[:, key_width:].reshape(blocks_here, BLOCK, kv_heads, DH)
    query_low = grad_query.reshape(tok_rows, query_width).astype(jnp.bfloat16)
    whole_input = gather_directly(layer_input, "tp", 1)
    grad_weight = summed_rows_2(
        jnp.einsum("td,tc->dc", whole_input, query_low, preferred_element_type=jnp.float32),
        KV,
        (2, 0, 1),
        0,
    )
    grad_keys = grad_key.reshape(tok_rows, key_width).astype(jnp.bfloat16)
    grad_values = grad_value.reshape(tok_rows, key_width).astype(jnp.bfloat16)
    return (query_low, grad_keys, grad_values, grad_weight)


def solution(mesh):
    torus = Mesh(mesh.devices.reshape(16, 8, 2, mesh.shape["tp"]), ("kv_0", "kv_1", "kv_2", "tp"))
    return jax.shard_map(
        shards,
        mesh=torus,
        in_specs=(
            P(KV, "tp"),
            P(KV, "tp"),
            P(KV, "tp"),
            P(KV, "tp"),
            P(KV, "tp"),
            P(KV, "tp"),
            P(KV, "tp"),
            P(),
        ),
        out_specs=(P(KV, "tp"), P(KV, "tp"), P(KV, "tp"), P(KV, "tp")),
        check_vma=False,
    )
```

profile of v0, /device:TPU:6, one launch (start us, length us, event | category | flops | bytes accessed | tf_op | source)
XLA Modules:
  0.0 234.1 jit_solution(6559204231608417810)
XLA Ops:
  7.2 0.9 copy.217
  9.1 19.4 %collective-permute-start.3 = (bf16[192,128]{1,0:T(8,128)(2,1)S(1)}, bf16[192,128]{1,0:T(8,128)(2,1)S(1)}, u32[]{:S(2)}, u32[]{:S(2)}) collective-permute-start(bf16[192,128]{1,0:T(8,128)(2,1)S(1)} %pad_maximum_fusion.4), channel_id=1, source_target_pairs={{0,512},{4,516},{8,520},{12,524},{16,528},{20,532},{24,536},{28,54... | collective-permute-start | bytes 147464 | tf_op jit(solution)/shard_map/ppermute | solution.py:16
  28.5 6.1 %collective-permute-start.2 = (bf16[192,128]{1,0:T(8,128)(2,1)S(1)}, bf16[192,128]{1,0:T(8,128)(2,1)S(1)}, u32[]{:S(2)}, u32[]{:S(2)}) collective-permute-start(bf16[192,128]{1,0:T(8,128)(2,1)S(1)} %pad_maximum_fusion.4), channel_id=1, source_target_pairs={{0,256},{4,260},{8,264},{12,268},{16,272},{20,276},{24,280},{28,28... | collective-permute-start | bytes 147464 | tf_op jit(solution)/shard_map/ppermute | solution.py:16
  34.6 4.3 %collective-permute-start.1 = (bf16[192,128]{1,0:T(8,128)(2,1)S(1)}, bf16[192,128]{1,0:T(8,128)(2,1)S(1)}, u32[]{:S(2)}, u32[]{:S(2)}) collective-permute-start(bf16[192,128]{1,0:T(8,128)(2,1)S(1)} %pad_maximum_fusion.4), channel_id=1, source_target_pairs={{0,128},{4,132},{8,136},{12,140},{16,144},{20,148},{24,152},{28,15... | collective-permute-start | bytes 147464 | tf_op jit(solution)/shard_map/ppermute | solution.py:16
  38.9 1.3 collective-permute-start
  40.2 1.9 broadcast_in_dim.115
  42.1 4.8 %all-to-all-start = ((bf16[4,192,512]{2,1,0:T(8,128)(2,1)}), bf16[4,192,512]{2,1,0:T(8,128)(2,1)S(1)}, u32[]{:S(2)}, u32[]{:S(2)}) async-start(bf16[4,192,512]{2,1,0:T(8,128)(2,1)} %broadcast_in_dim.115), calls=%async_computation | async-start | bytes 1572864 | tf_op jit(solution)/shard_map/all_to_all | solution.py:27
  46.9 0.9 subtract_select_fusion.3
  53.0 1.2 gather_fusion.5
  54.8 1.2 gather_fusion.3
  56.7 1.2 gather_fusion.1
  61.7 1.2 convolution_multiply_fusion.2
  64.3 1.2 convolution_multiply_fusion.4
  68.3 1.9 copy.250
  70.2 1.2 reduce_sum.58
  71.5 0.9 copy.245
  72.4 1.2 reduce_sum.56
  73.6 0.9 copy.240
  75.7 1.2 copy.235
  76.9 1.5 fusion.43
  79.5 1.4 convolution_bitcast_fusion
  80.9 1.8 copy.271
  82.7 3.2 %copy.272 = f32[2,16,8,8,256]{4,3,2,1,0:T(8,128)} copy(f32[2,16,8,8,256]{4,3,0,2,1:T(8,128)} %bitcast.521) | data formatting | bytes 4194304 | tf_op jit(solution)/shard_map/transpose | solution.py:37
  89.7 1.4 collective-permute-start.7
  92.7 1.5 collective-permute-start.6
  95.7 6.1 %reduce-scatter.4.cloned.1.call-done = f32[128,8,256]{2,1,0:T(8,128)} async-done(((f32[256,8,256]{2,1,0:T(8,128)}), f32[128,8,256]{2,1,0:T(8,128)}) %reduce-scatter.4.cloned.1.call-update) | async-done | bytes 1048592 | tf_op jit(solution)/shard_map/reduce_scatter | solution.py:39
  102.0 1.3 collective-permute-start.5
  104.9 1.3 collective-permute-start.4
  106.3 7.7 %collective-permute-done.6 = f32[192,128]{1,0:T(8,128)S(1)} collective-permute-done((f32[192,128]{1,0:T(8,128)S(1)}, f32[192,128]{1,0:T(8,128)S(1)}, u32[]{:S(2)}, u32[]{:S(2)}) %collective-permute-start.6) | collective-permute-done | bytes 98336 | tf_op jit(solution)/shard_map/ppermute | solution.py:16
  114.0 1.2 collective-permute-done.5
  116.1 66.1 %reduce-scatter.6.cloned.1.call-done = f32[8,8,256]{2,1,0:T(8,128)} async-done(((f32[128,8,256]{2,1,0:T(8,128)}), f32[8,8,256]{2,1,0:T(8,128)}) %reduce-scatter.6.cloned.1.call-update) | async-done | bytes 65552 | tf_op jit(solution)/shard_map/reduce_scatter | solution.py:39
  183.0 44.6 %reduce-scatter.8.cloned.1.call-done = f32[1,8,256]{2,1,0:T(8,128)} async-done(((f32[8,8,256]{2,1,0:T(8,128)}), f32[1,8,256]{2,1,0:T(8,128)}) %reduce-scatter.8.cloned.1.call-update) | async-done | bytes 8208 | tf_op jit(solution)/shard_map/reduce_scatter | solution.py:39
  (179 shorter events, 27.4 us)
Async XLA Ops:
  7.2 41.4 %copy-start.27 = (f32[192,4]{0,1:T(4,128)S(1)}, f32[192,4]{0,1:T(4,128)}, u32[]{:S(2)}) copy-start(f32[192,4]{0,1:T(4,128)} %param.14) | copy-start | bytes 9220
  7.2 41.5 %copy-start.25 = (bf16[192,256]{1,0:T(8,128)(2,1)S(1)}, bf16[192,256]{1,0:T(8,128)(2,1)}, u32[]{:S(2)}) copy-start(bf16[192,256]{1,0:T(8,128)(2,1)} %param.9) | copy-start | bytes 294916
  7.2 41.6 %copy-start.23 = (bf16[192,256]{1,0:T(8,128)(2,1)S(1)}, bf16[192,256]{1,0:T(8,128)(2,1)}, u32[]{:S(2)}) copy-start(bf16[192,256]{1,0:T(8,128)(2,1)} %param.13) | copy-start | bytes 294916
  7.2 41.8 %copy-start.26 = (bf16[192,256]{1,0:T(8,128)(2,1)S(1)}, bf16[192,256]{1,0:T(8,128)(2,1)}, u32[]{:S(2)}) copy-start(bf16[192,256]{1,0:T(8,128)(2,1)} %param.12) | copy-start | bytes 294916
  9.1 41.9 %collective-permute-start.3 = (bf16[192,128]{1,0:T(8,128)(2,1)S(1)}, bf16[192,128]{1,0:T(8,128)(2,1)S(1)}, u32[]{:S(2)}, u32[]{:S(2)}) collective-permute-start(bf16[192,128]{1,0:T(8,128)(2,1)S(1)} %pad_maximum_fusion.4), channel_id=1, source_target_pairs={{0,512},{4,516},{8,520},{12,524},{16,528},{20,532},{24,536},{28,54... | collective-permute-start | bytes 147464 | tf_op jit(solution)/shard_map/ppermute | solution.py:16
  28.5 22.6 %collective-permute-start.2 = (bf16[192,128]{1,0:T(8,128)(2,1)S(1)}, bf16[192,128]{1,0:T(8,128)(2,1)S(1)}, u32[]{:S(2)}, u32[]{:S(2)}) collective-permute-start(bf16[192,128]{1,0:T(8,128)(2,1)S(1)} %pad_maximum_fusion.4), channel_id=1, source_target_pairs={{0,256},{4,260},{8,264},{12,268},{16,272},{20,276},{24,280},{28,28... | collective-permute-start | bytes 147464 | tf_op jit(solution)/shard_map/ppermute | solution.py:16
  34.6 16.6 %collective-permute-start.1 = (bf16[192,128]{1,0:T(8,128)(2,1)S(1)}, bf16[192,128]{1,0:T(8,128)(2,1)S(1)}, u32[]{:S(2)}, u32[]{:S(2)}) collective-permute-start(bf16[192,128]{1,0:T(8,128)(2,1)S(1)} %pad_maximum_fusion.4), channel_id=1, source_target_pairs={{0,128},{4,132},{8,136},{12,140},{16,144},{20,148},{24,152},{28,15... | collective-permute-start | bytes 147464 | tf_op jit(solution)/shard_map/ppermute | solution.py:16
  38.9 17.1 %collective-permute-start = (bf16[192,128]{1,0:T(8,128)(2,1)S(1)}, bf16[192,128]{1,0:T(8,128)(2,1)S(1)}, u32[]{:S(2)}, u32[]{:S(2)}) collective-permute-start(bf16[192,128]{1,0:T(8,128)(2,1)S(1)} %pad_maximum_fusion.4), channel_id=1, source_target_pairs={{0,4},{4,8},{8,12},{12,16},{16,20},{20,24},{24,28},{28,32},{32,36}... | collective-permute-start | bytes 147464 | tf_op jit(solution)/shard_map/ppermute | solution.py:16
  42.1 37.3 %all-to-all-start = ((bf16[4,192,512]{2,1,0:T(8,128)(2,1)}), bf16[4,192,512]{2,1,0:T(8,128)(2,1)S(1)}, u32[]{:S(2)}, u32[]{:S(2)}) async-start(bf16[4,192,512]{2,1,0:T(8,128)(2,1)} %broadcast_in_dim.115), calls=%async_computation | async-start | bytes 1572864 | tf_op jit(solution)/shard_map/all_to_all | solution.py:27
  46.8 54.9 %reduce-scatter.4.cloned.1.call-start = ((), (), s32[]{:S(2)}) async-start(), calls=%async_computation.4 | async-start | bytes 3145728 | tf_op jit(solution)/shard_map/reduce_scatter | solution.py:39
  48.8 2.4 %copy-start.14 = (bf16[3,64,4,64]{3,2,1,0:T(4,128)(2,1)}, bf16[3,64,4,64]{3,2,1,0:T(4,128)(2,1)S(1)}, u32[]{:S(2)}) copy-start(bf16[3,64,4,64]{3,2,1,0:T(4,128)(2,1)S(1)} %reshape.544) | copy-start | bytes 294916
  49.6 8.2 %copy-start.18 = (f32[3,1,4,64,64]{3,4,2,0,1:T(8,128)}, f32[3,1,4,64,64]{3,4,2,0,1:T(8,128)S(1)}, u32[]{:S(2)}) copy-start(f32[3,1,4,64,64]{3,4,2,0,1:T(8,128)S(1)} %fusion.38) | copy-start | bytes 589828
  49.9 26.9 %copy-start.16 = (bf16[3,4,64,64]{2,3,1,0:T(8,128)(2,1)}, bf16[3,4,64,64]{2,3,1,0:T(8,128)(2,1)S(1)}, u32[]{:S(2)}) copy-start(bf16[3,4,64,64]{2,3,1,0:T(8,128)(2,1)S(1)} %fusion.45) | copy-start | bytes 294916
  58.6 2.1 copy-start.20
  60.7 2.7 %copy-start.21 = (bf16[6,64,64]{2,1,0:T(8,128)(2,1)S(1)}, bf16[6,64,64]{2,1,0:T(8,128)(2,1)}, u32[]{:S(2)}) copy-start(bf16[6,64,64]{2,1,0:T(8,128)(2,1)} %gather_fusion.3) | copy-start | bytes 147460
  61.7 1.3 copy-start.10
  63.5 3.5 %copy-start.22 = (bf16[6,64,64]{2,1,0:T(8,128)(2,1)S(1)}, bf16[6,64,64]{2,1,0:T(8,128)(2,1)}, u32[]{:S(2)}) copy-start(bf16[6,64,64]{2,1,0:T(8,128)(2,1)} %gather_fusion.1) | copy-start | bytes 147460
  64.3 3.2 %copy-start.8 = (bf16[6,4,64,64]{2,3,1,0:T(8,128)(2,1)}, bf16[6,4,64,64]{2,3,1,0:T(8,128)(2,1)S(1)}, u32[]{:S(2)}) copy-start(bf16[6,4,64,64]{2,3,1,0:T(8,128)(2,1)S(1)} %fusion.29) | copy-start | bytes 589828
  85.9 2.1 copy-start.7
  86.0 2.8 %copy-start.13 = (bf16[6,4,64,64]{2,3,1,0:T(8,128)(2,1)S(1)}, bf16[6,4,64,64]{2,3,1,0:T(8,128)(2,1)}, u32[]{:S(2)}) copy-start(bf16[6,4,64,64]{2,3,1,0:T(8,128)(2,1)} %copy-done.12) | copy-start | bytes 589828
  86.0 96.3 %reduce-scatter.6.cloned.1.call-start = ((), (), s32[]{:S(2)}) async-start(), calls=%async_computation.5 | async-start | bytes 1114112 | tf_op jit(solution)/shard_map/reduce_scatter | solution.py:39
  88.0 3.1 %copy-start.5 = (f32[6,1,4,64,64]{3,4,2,0,1:T(8,128)S(1)}, f32[6,1,4,64,64]{3,4,2,0,1:T(8,128)}, u32[]{:S(2)}) copy-start(f32[6,1,4,64,64]{3,4,2,0,1:T(8,128)} %copy-done.4) | copy-start | bytes 1179652
  88.8 3.1 %copy-start.11 = (bf16[6,4,64,64]{2,3,1,0:T(8,128)(2,1)S(1)}, bf16[6,4,64,64]{2,3,1,0:T(8,128)(2,1)}, u32[]{:S(2)}) copy-start(bf16[6,4,64,64]{2,3,1,0:T(8,128)(2,1)} %copy-done.10) | copy-start | bytes 589828
  89.6 4.6 %copy-start.3 = (f32[6,1,4,64,64]{3,4,2,0,1:T(8,128)S(1)}, f32[6,1,4,64,64]{3,4,2,0,1:T(8,128)}, u32[]{:S(2)}) copy-start(f32[6,1,4,64,64]{3,4,2,0,1:T(8,128)} %copy-done.2) | copy-start | bytes 1179652
  89.7 16.5 %collective-permute-start.7 = (f32[192,128]{1,0:T(8,128)S(1)}, f32[192,128]{1,0:T(8,128)S(1)}, u32[]{:S(2)}, u32[]{:S(2)}) collective-permute-start(f32[192,128]{1,0:T(8,128)S(1)} %pad_maximum_fusion.3), channel_id=1, source_target_pairs={{512,0},{516,4},{520,8},{524,12},{528,16},{532,20},{536,24},{540,2... | collective-permute-start | bytes 294920 | tf_op jit(solution)/shard_map/ppermute | solution.py:16
  91.8 3.1 %copy-start.9 = (bf16[6,4,64,64]{2,3,1,0:T(8,128)(2,1)S(1)}, bf16[6,4,64,64]{2,3,1,0:T(8,128)(2,1)}, u32[]{:S(2)}) copy-start(bf16[6,4,64,64]{2,3,1,0:T(8,128)(2,1)} %copy-done.8) | copy-start | bytes 589828
  92.7 21.2 %collective-permute-start.6 = (f32[192,128]{1,0:T(8,128)S(1)}, f32[192,128]{1,0:T(8,128)S(1)}, u32[]{:S(2)}, u32[]{:S(2)}) collective-permute-start(f32[192,128]{1,0:T(8,128)S(1)} %pad_maximum_fusion.2), channel_id=1, source_target_pairs={{256,0},{260,4},{264,8},{268,12},{272,16},{276,20},{280,24},{284,2... | collective-permute-start | bytes 294920 | tf_op jit(solution)/shard_map/ppermute | solution.py:16
  95.0 9.0 %copy-start.1 = (f32[6,1,4,64,64]{3,4,2,0,1:T(8,128)S(1)}, f32[6,1,4,64,64]{3,4,2,0,1:T(8,128)}, u32[]{:S(2)}) copy-start(f32[6,1,4,64,64]{3,4,2,0,1:T(8,128)} %copy-done) | copy-start | bytes 1179652
  101.8 125.8 %reduce-scatter.8.cloned.1.call-start = ((), (), s32[]{:S(2)}) async-start(), calls=%async_computation.6 | async-start | bytes 73728 | tf_op jit(solution)/shard_map/reduce_scatter | solution.py:39
  102.0 13.2 %collective-permute-start.5 = (f32[192,128]{1,0:T(8,128)S(1)}, f32[192,128]{1,0:T(8,128)S(1)}, u32[]{:S(2)}, u32[]{:S(2)}) collective-permute-start(f32[192,128]{1,0:T(8,128)S(1)} %pad_maximum_fusion.1), channel_id=1, source_target_pairs={{128,0},{132,4},{136,8},{140,12},{144,16},{148,20},{152,24},{156,2... | collective-permute-start | bytes 294920 | tf_op jit(solution)/shard_map/ppermute | solution.py:16
  104.0 11.4 %copy-start.24 = (f32[3,64,1,64]{3,1,0,2:T(8,128)S(1)}, f32[3,64,1,64]{3,1,0,2:T(8,128)}, u32[]{:S(2)}) copy-start(f32[3,64,1,64]{3,1,0,2:T(8,128)} %convolution_bitcast_fusion.18) | copy-start | bytes 147460
  104.9 10.4 %collective-permute-start.4 = (f32[192,128]{1,0:T(8,128)S(1)}, f32[192,128]{1,0:T(8,128)S(1)}, u32[]{:S(2)}, u32[]{:S(2)}) collective-permute-start(f32[192,128]{1,0:T(8,128)S(1)} %pad_maximum_fusion), channel_id=1, source_target_pairs={{4,0},{8,4},{12,8},{16,12},{20,16},{24,20},{28,24},{32,28},{36,32}... | collective-permute-start | bytes 294920 | tf_op jit(solution)/shard_map/ppermute | solution.py:16
  (8 other events, 7.6 us)
Sparse Core Ops, SparseCore 0:
  86.1 15.6 reduce-scatter.3
  105.2 77.0 reduce-scatter.5
  186.2 41.3 reduce-scatter.7
where the time goes:
time: 235 us; the launch traced here: 234 us
  waiting for transfers between devices  126 us (54%)
  starting transfers between devices  41.4 us (18%)
  local copies, waits for them, and re-layouts  29.2 us (12%)
  matrix products  17.5 us (7%)
  between operations  14.7 us (6%)
  other arithmetic  5.72 us (2%)
    reduce_scatter x3, waiting for transfers between devices, reduced_to_own(): tiles = lax.psum_scatter(tiles, axes[k], scatter_dimension=0, tiled=True)  117 us
    ppermute x8, starting transfers between devices, shifted(): return lax.ppermute(block, axis, route)  36.5 us
    ppermute x8, waiting for transfers between devices, shifted(): return lax.ppermute(block, axis, route)  8.82 us
    unnamed x60, local copies, waits for them, and re-layouts  6.66 us
    reduce_sum x4, local copies, waits for them, and re-layouts, fold_pairs(): jnp.sum(pair_array.reshape((blocks_here, PER) + pair_array.shape[1:]), ax...  4.92 us
    all_to_all x1, starting transfers between devices, sent_to_all(): return lax.all_to_all(copies, axis, split_axis=0, concat_axis=0, tiled=True)  4.77 us
  transfers between devices with their start and end apart: 12, of which 5 were waited for; matrix products, arithmetic and copies ran while one was open for 17% of the time, Pallas kernels for 0%

commit v1 on v0

v1 whole, which is shorter than its diff:
```python
import functools

import jax
import jax.numpy as jnp
from jax import lax
from jax.experimental import pallas as pl
from jax.experimental.pallas import tpu as pltpu
from jax.sharding import Mesh
from jax.sharding import PartitionSpec as P

DH = 64
BLOCK = 64
PER = 2
LEVELS = 4
SIDES = (8, 2)
KV = ("z", "y", "c")
NT = (((1,), (1,)), ((), ()))
TN = (((0,), (0,)), ((), ()))


def shifted(block, axis, distance):
    devices = range(lax.axis_size(axis))
    route = [(i - distance, i) for i in devices if i - distance in devices]
    return lax.ppermute(block, axis, route)


def exchanged(tiles, axis):
    return lax.all_to_all(tiles, axis, split_axis=0, concat_axis=0, tiled=True)


def dot(a, b, dims=(((1,), (0,)), ((), ()))):
    return lax.dot_general(a, b, dims, preferred_element_type=jnp.float32)


def spread_kernel(rows, ys, cores, peers, x_ref, out_ref):
    width = x_ref.shape[1]
    source = lax.broadcasted_iota(jnp.int32, (width, width), 0)
    target = lax.broadcasted_iota(jnp.int32, (width, width), 1)
    inner, left = source % rows, source // rows
    core, left = left % cores, left // cores
    y, z = left % ys, left // ys
    zs = width // (rows * cores * ys)
    place = ((core * ys + y) * zs + z) * rows + inner
    move = jnp.where(place == target, 1.0, 0.0).astype(jnp.bfloat16)
    moved = dot(x_ref[...], move).astype(jnp.bfloat16)
    part = width // cores
    for core in range(cores):
        for peer in range(peers):
            out_ref[core * peers + peer] = moved[:, core * part : (core + 1) * part]


def spread(x, rows, ys, cores, peers):
    tokens, width = x.shape
    return pl.pallas_call(
        functools.partial(spread_kernel, rows, ys, cores, peers),
        out_shape=jax.ShapeDtypeStruct((cores * peers, tokens, width // cores), x.dtype),
        cost_estimate=pl.CostEstimate(
            flops=2 * tokens * width * width, bytes_accessed=2 * tokens * width * (1 + peers), transcendentals=0
        ),
        name="spread",
    )(x)


def stacked(block, at):
    block = block.astype(jnp.float32)
    lane = lax.broadcasted_iota(jnp.int32, (BLOCK, 2 * DH), 1)
    keep = (lane >= at) & (lane < at + DH)
    parts = []
    for head in range(block.shape[1] // DH):
        pair = block[:, (head // 2) * 2 * DH : (head // 2 + 1) * 2 * DH]
        if (head % 2) * DH != at:
            pair = pltpu.roll(pair, DH, 1)
        parts.append(jnp.where(keep, pair, 0.0))
    return jnp.concatenate(parts, axis=0)


def row_sums(terms, pieces):
    ones = jnp.ones((8, terms.shape[1]), jnp.bfloat16)
    total = None
    for _ in range(pieces):
        piece = terms.astype(jnp.bfloat16)
        terms = terms - piece.astype(jnp.float32)
        part = dot(ones, piece, NT)
        total = part if total is None else total + part
    return total[:1]


def attention_kernel(
    offs_ref, q_ref, go_ref, ao_ref, lse_ref, k_ref, v_ref, *refs
):
    far_refs = refs[:LEVELS]
    gq_ref, own_ref = refs[LEVELS : LEVELS + 2]
    back_refs = refs[LEVELS + 2 : 2 * LEVELS + 2]
    sums = refs[2 * LEVELS + 2]
    blocks = q_ref.shape[0] // BLOCK
    heads = q_ref.shape[1] // DH
    own_kv = jnp.concatenate([k_ref[...], v_ref[...]], axis=1)
    lane = lax.broadcasted_iota(jnp.int32, (BLOCK, 2 * DH), 1)
    sums[...] = jnp.zeros_like(sums)
    key_at = lax.broadcasted_iota(jnp.int32, (BLOCK, heads * BLOCK), 0)
    query_at = lax.broadcasted_iota(jnp.int32, (BLOCK, heads * BLOCK), 1) % BLOCK
    causal = key_at <= query_at
    for b in range(blocks):
        rows = slice(b * BLOCK, (b + 1) * BLOCK)
        low = stacked(q_ref[rows] * DH ** (-0.5), 0)
        high = stacked(go_ref[rows], DH)
        delta = row_sums(high * stacked(ao_ref[rows], DH), 2)
        lse_rows = lse_ref[rows]
        lse = row_sums(
            jnp.concatenate(
                [jnp.where(lane == 0, lse_rows[:, h : h + 1], 0.0) for h in range(heads)], axis=0
            ),
            3,
        )
        low = low.astype(jnp.bfloat16)
        high = high.astype(jnp.bfloat16)
        places = [
            pl.multiple_of(offs_ref[b, n] * BLOCK, BLOCK) for n in range(LEVELS * PER)
        ]
        kv = jnp.concatenate(
            [own_kv[rows]]
            + [far_refs[n // PER][pl.ds(places[n], BLOCK), :] for n in range(LEVELS * PER)],
            axis=0,
        )
        weights = jnp.exp(dot(kv, low, NT) - lse)
        weights = jnp.concatenate(
            [jnp.where(causal, weights[:BLOCK], 0.0), weights[BLOCK:]], axis=0
        )
        dscores = (weights * (dot(kv, high, NT) - delta)).astype(jnp.bfloat16)
        grad_kv = dot(dscores, low) + dot(weights.astype(jnp.bfloat16), high)
        own_ref[rows] = grad_kv[:BLOCK]
        for n in range(LEVELS * PER):
            at = pl.ds(places[n], BLOCK)
            sums[n // PER, at, :] += grad_kv[(n + 1) * BLOCK : (n + 2) * BLOCK]
        grad_q = dot(dscores, kv, TN) * DH ** (-0.5)
        for pair in range(heads // 2):
            first = grad_q[2 * pair * BLOCK : (2 * pair + 1) * BLOCK]
            second = grad_q[(2 * pair + 1) * BLOCK : (2 * pair + 2) * BLOCK]
            gq_ref[rows, pair * 2 * DH : (pair + 1) * 2 * DH] = jnp.where(
                lane < DH, first, pltpu.roll(second, DH, 1)
            ).astype(gq_ref.dtype)
    for level in range(LEVELS):
        back_refs[level][...] = sums[level].astype(jnp.bfloat16)


def attention(offs, q, go, ao, lse, k, v, far):
    tokens, width = q.shape
    vmem = pl.BlockSpec(memory_space=pltpu.VMEM)
    return pl.pallas_call(
        attention_kernel,
        out_shape=(
            jax.ShapeDtypeStruct((tokens, width), jnp.bfloat16),
            jax.ShapeDtypeStruct((tokens, 2 * DH), jnp.float32),
        )
        + (jax.ShapeDtypeStruct((tokens, 2 * DH), jnp.bfloat16),) * LEVELS,
        in_specs=[pl.BlockSpec(memory_space=pltpu.SMEM)] + [vmem] * (6 + LEVELS),
        out_specs=(vmem,) * (2 + LEVELS),
        scratch_shapes=[pltpu.VMEM((LEVELS, tokens, 2 * DH), jnp.float32)],
        cost_estimate=pl.CostEstimate(flops=2 * 10**9, bytes_accessed=10**6, transcendentals=10**6),
        name="attention",
    )(offs, q, go, ao, lse, k, v, *far)


def weight_kernel(core_ref, mine_ref, other_ref, x_ref, out_ref):
    core = core_ref[0]
    peers = x_ref.shape[0] // 2
    ys = out_ref.shape[0]
    grads = jnp.concatenate([mine_ref[...], other_ref[...]], axis=0)
    for peer in range(peers):
        x = jnp.concatenate(
            [x_ref[core * peers + peer], x_ref[(1 - core) * peers + peer]], axis=0
        )
        part = dot(x, grads, TN).astype(out_ref.dtype)
        step = part.shape[0] // ys
        for y in range(ys):
            out_ref[y, peer * step : (peer + 1) * step] = part[y * step : (y + 1) * step]


def weight(core, mine, other, x, ys):
    peers, tokens, part = x.shape[0] // 2, x.shape[1], x.shape[2]
    vmem = pl.BlockSpec(memory_space=pltpu.VMEM)
    return pl.pallas_call(
        weight_kernel,
        out_shape=jax.ShapeDtypeStruct((ys, peers * part // ys, mine.shape[1]), jnp.bfloat16),
        in_specs=[pl.BlockSpec(memory_space=pltpu.SMEM), vmem, vmem, vmem],
        out_specs=vmem,
        cost_estimate=pl.CostEstimate(
            flops=4 * tokens * peers * part * mine.shape[1], bytes_accessed=2 * 10**6, transcendentals=0
        ),
        name="weight",
    )(core, mine, other, x)


def summed(tiles):
    return jnp.sum(tiles.astype(jnp.float32), axis=0)


def shards(layer_input, queries, keys, values, attn_out, grad_out, log_sum, chosen):
    axis_size = lax.axis_size(KV)
    my_index = lax.axis_index(KV)
    ys, cores, peers = lax.axis_size("y"), lax.axis_size("c"), lax.axis_size("x")
    tok_rows = queries.shape[0]
    blocks_here = tok_rows // BLOCK
    key_width = keys.shape[1]
    out_rows = layer_input.shape[1] * peers // axis_size
    distances = [1, axis_size // 8, axis_size // 4, axis_size // 2]
    key_pair = jnp.concatenate([keys, values], axis=1)
    far = [shifted(key_pair, KV, distance) for distance in distances]
    whole_input = exchanged(spread(layer_input, out_rows, ys, cores, peers), ("c", "x"))
    listed = lax.dynamic_slice(chosen, (my_index * blocks_here, 0), (blocks_here, LEVELS * PER))
    first = (my_index - jnp.repeat(jnp.array(distances, jnp.int32), PER)) * blocks_here
    offs = jnp.where(listed >= 0, listed - first, 0)
    grad_queries, own, *back = attention(
        offs, queries, grad_out, attn_out, log_sum, keys, values, far
    )
    other = lax.ppermute(grad_queries, "c", [(i, cores - 1 - i) for i in range(cores)])
    core = lax.axis_index("c").astype(jnp.int32).reshape(1)
    parts = weight(core, grad_queries, other, whole_input, ys)
    over_y = summed(exchanged(parts, "y")).astype(jnp.bfloat16)
    over_z = exchanged(over_y.reshape(-1, out_rows, over_y.shape[1]), "z")
    grad_weight = summed(over_z)
    for level, distance in enumerate(distances):
        own = own + shifted(back[level], KV, -distance).astype(jnp.float32)
    own = own.astype(jnp.bfloat16)
    return (grad_queries, own[:, :key_width], own[:, key_width:], grad_weight)


def solution(mesh):
    ys, cores = SIDES
    shape = (mesh.shape["kv"] // (ys * cores), ys, cores, mesh.shape["tp"])
    torus = Mesh(mesh.devices.reshape(shape), (*KV, "x"))
    return jax.shard_map(
        shards,
        mesh=torus,
        in_specs=(P(KV, "x"),) * 7 + (P(),),
        out_specs=(P(KV, "x"),) * 4,
        check_vma=False,
    )
```

time: 235 us -> 102 us (0.43)
  waiting for transfers between devices: 126 us -> 24.9 us
  local copies, waits for them, and re-layouts: 29.2 us -> 6.92 us
  matrix products: 17.5 us -> 0 us
  starting transfers between devices: 41.4 us -> 57 us
  between operations: 14.7 us -> 0.9 us
  Pallas kernels: 0 us -> 8.53 us
  other arithmetic: 5.72 us -> 2.03 us
    reduce_scatter x3 -> x0, waiting for transfers between devices: 117 us -> none  [reduced_to_own(): tiles = lax.psum_scatter(tiles, axes[k], scatter_dimension=0, tiled=True)]
    all_to_all x1 -> x3, waiting for transfers between devices: 0.01 us -> 23.5 us  [exchanged(): return lax.all_to_all(tiles, axis, split_axis=0, concat_axis=0, tiled=True)]
    dot_general x34 -> x0, matrix products: 17.5 us -> none  [the longest x5 4.63 us: pair_terms(): jnp.einsum('pkgbc,pcke->pbkge', dscores, key_rows, preferred_element_type...]
    all_to_all x1 -> x3, starting transfers between devices: 4.77 us -> 18.7 us  [exchanged(): return lax.all_to_all(tiles, axis, split_axis=0, concat_axis=0, tiled=True)]
    ppermute x8, waiting for transfers between devices: 8.82 us -> 0.02 us  [shifted(): return lax.ppermute(block, axis, route)]
    pallas_call x0 -> x3, Pallas kernels: none -> 8.53 us  [the longest x1 3.77 us: attention(): pl.pallas_call(attention_kernel, out_shape=(jax.ShapeDtypeStruct((tokens,...]
    gather x8 -> x0, local copies, waits for them, and re-layouts: 6.42 us -> none  [the longest x4 4.16 us: shards(): arrived[:, key_width:].reshape(blocks_here, BLOCK, kv_heads, DH)]
    reduce_sum x4 -> x0, local copies, waits for them, and re-layouts: 4.92 us -> none  [fold_pairs(): jnp.sum(pair_array.reshape((blocks_here, PER) + pair_array.shape[1:]), ax...]
  transfers between devices with their start and end apart: 12 -> 12, of which waited for: 5 -> 4; matrix products, arithmetic and copies ran while one was open for 17% -> 4% of each run, Pallas kernels for 0% -> 6%
where the time goes in v1:
time: 102 us; the launch traced here: 100 us
  starting transfers between devices  57 us (56%)
  waiting for transfers between devices  24.9 us (24%)
  Pallas kernels  8.53 us (8%)
  local copies, waits for them, and re-layouts  6.92 us (7%)
  other arithmetic  2.03 us (2%)
    ppermute x8, starting transfers between devices, shifted(): return lax.ppermute(block, axis, route)  36.2 us
    all_to_all x3, waiting for transfers between devices, exchanged(): return lax.all_to_all(tiles, axis, split_axis=0, concat_axis=0, tiled=True)  23.5 us
    all_to_all x3, starting transfers between devices, exchanged(): return lax.all_to_all(tiles, axis, split_axis=0, concat_axis=0, tiled=True)  18.7 us
    unnamed x40, local copies, waits for them, and re-layouts  6.6 us
    pallas_call x1, Pallas kernels, attention(): pl.pallas_call(attention_kernel, out_shape=(jax.ShapeDtypeStruct((tokens,...  3.77 us
    pallas_call x1, Pallas kernels, weight(): pl.pallas_call(weight_kernel, out_shape=jax.ShapeDtypeStruct((ys, peers *...  2.54 us
    pallas_call x1, Pallas kernels, spread(): pl.pallas_call(functools.partial(spread_kernel, rows, ys, cores, peers),...  2.22 us
  transfers between devices with their start and end apart: 12, of which 4 were waited for; matrix products, arithmetic and copies ran while one was open for 4% of the time, Pallas kernels for 6%

profile of v1, /device:TPU:6, one launch (start us, length us, event | category | flops | bytes accessed | tf_op | source)
XLA Modules:
  0.0 100.3 jit_solution(5525999098010267896)
XLA Ops:
  0.7 0.9 copy.33.k_ref
  1.8 0.4 copy-done.2
  2.3 19.3 %collective-permute-start.3 = (bf16[192,128]{1,0:T(8,128)(2,1)S(1)}, bf16[192,128]{1,0:T(8,128)(2,1)S(1)}, u32[]{:S(2)}, u32[]{:S(2)}) collective-permute-start(bf16[192,128]{1,0:T(8,128)(2,1)S(1)} %pad_maximum_fusion), channel_id=1, source_target_pairs={{0,512},{4,516},{8,520},{12,524},{16,528},{20,532},{24,536},{28,54... | collective-permute-start | bytes 147464 | tf_op jit(solution)/shard_map/ppermute | solution.py:24
  21.6 6.1 %collective-permute-start.2 = (bf16[192,128]{1,0:T(8,128)(2,1)S(1)}, bf16[192,128]{1,0:T(8,128)(2,1)S(1)}, u32[]{:S(2)}, u32[]{:S(2)}) collective-permute-start(bf16[192,128]{1,0:T(8,128)(2,1)S(1)} %pad_maximum_fusion), channel_id=1, source_target_pairs={{0,256},{4,260},{8,264},{12,268},{16,272},{20,276},{24,280},{28,28... | collective-permute-start | bytes 147464 | tf_op jit(solution)/shard_map/ppermute | solution.py:24
  27.8 4.3 %collective-permute-start.1 = (bf16[192,128]{1,0:T(8,128)(2,1)S(1)}, bf16[192,128]{1,0:T(8,128)(2,1)S(1)}, u32[]{:S(2)}, u32[]{:S(2)}) collective-permute-start(bf16[192,128]{1,0:T(8,128)(2,1)S(1)} %pad_maximum_fusion), channel_id=1, source_target_pairs={{0,128},{4,132},{8,136},{12,140},{16,144},{20,148},{24,152},{28,15... | collective-permute-start | bytes 147464 | tf_op jit(solution)/shard_map/ppermute | solution.py:24
  32.1 1.3 %collective-permute-start = (bf16[192,128]{1,0:T(8,128)(2,1)S(1)}, bf16[192,128]{1,0:T(8,128)(2,1)S(1)}, u32[]{:S(2)}, u32[]{:S(2)}) collective-permute-start(bf16[192,128]{1,0:T(8,128)(2,1)S(1)} %pad_maximum_fusion), channel_id=1, source_target_pairs={{0,4},{4,8},{8,12},{12,16},{16,20},{20,24},{24,28},{28,32},{32,36}... | collective-permute-start | bytes 147464 | tf_op jit(solution)/shard_map/ppermute | solution.py:24
  33.4 2.2 %spread.1 = bf16[8,192,256]{2,1,0:T(8,128)(2,1)} custom-call(bf16[192,512]{1,0:T(8,128)(2,1)} %x_ref.1), custom_call_target="tpu_custom_call" | custom-call | flops 100663296 | bytes 983040 | tf_op jit(solution)/shard_map/spread/pallas_call | solution.py:54
  35.6 6.7 %all-to-all-start = ((bf16[8,192,256]{2,1,0:T(8,128)(2,1)}), bf16[8,192,256]{2,1,0:T(8,128)(2,1)S(1)}, u32[]{:S(2)}, u32[]{:S(2)}) async-start(bf16[8,192,256]{2,1,0:T(8,128)(2,1)} %spread.1), calls=%async_computation | async-start | bytes 1572864 | tf_op jit(solution)/shard_map/all_to_all | solution.py:28
  42.3 0.7 copy-done.16
  43.2 0.6 subtract_select_fusion.offs_ref
  43.9 0.8 copy.32.lse_ref
  44.7 0.6 copy-done.8
  45.3 0.6 copy-done.11
  45.9 3.8 %attention.1 = (bf16[192,256]{1,0:T(8,128)(2,1)}, f32[192,128]{1,0:T(8,128)}, bf16[192,128]{1,0:T(8,128)(2,1)}, bf16[192,128]{1,0:T(8,128)(2,1)}, bf16[192,128]{1,0:T(8,128)(2,1)}, /*index=5*/bf16[192,128]{1,0:T(8,128)(2,1)}) custom-call(s32[3,8]{1,0:T(4,128)} %subtract_select_fusion.offs_ref, bf16[192,256]{1,0:T(8,128)(2,1)} %q_ref.1, ...), custom_call_target="tpu_custom_call" | custom-call | flops 2000000000 | bytes 1000000 | tf_op jit(solution)/shard_map/attention/pallas_call | solution.py:149
  49.7 2.0 %collective-permute-start.8 = (bf16[192,256]{1,0:T(8,128)(2,1)}, bf16[192,256]{1,0:T(8,128)(2,1)S(1)}, u32[]{:S(2)}, u32[]{:S(2)}) collective-permute-start(bf16[192,256]{1,0:T(8,128)(2,1)} %get-tuple-element.24.mine_ref), channel_id=1, source_target_pairs={{0,4},{4,0},{1,5},{5,1},{2,6},{6,2},{3,7},{7,3},{8,12},{12,8},{9,1... | collective-permute-start | bytes 294920 | tf_op jit(solution)/shard_map/ppermute | solution.py:216
  51.7 1.4 %collective-permute-done.8.other_ref = bf16[192,256]{1,0:T(8,128)(2,1)S(1)} collective-permute-done((bf16[192,256]{1,0:T(8,128)(2,1)}, bf16[192,256]{1,0:T(8,128)(2,1)S(1)}, u32[]{:S(2)}, u32[]{:S(2)}) %collective-permute-start.8) | collective-permute-done | bytes 98336 | tf_op jit(solution)/shard_map/ppermute | solution.py:216
  53.1 0.3 all-to-all-done.x_ref
  53.3 0.4 copy-done.5
  53.7 0.5 copy-done.1
  54.2 2.5 %weight.1 = bf16[8,128,256]{2,1,0:T(8,128)(2,1)} custom-call(s32[1]{0:T(128)} %bitcast.core_ref, bf16[192,256]{1,0:T(8,128)(2,1)} %get-tuple-element.24.mine_ref, bf16[192,256]{1,0:T(8,128)(2,1)} %copy-done.5, bf16[8,192,256]{2,1,0:T(8,128)(2,1)} %copy-done.1), custom_call_target="tpu_custom_call" | custom-call | flops 201326592 | bytes 2000000 | tf_op jit(solution)/shard_map/weight/pallas_call | solution.py:182
  56.8 6.3 %all-to-all-start.1 = ((bf16[8,128,256]{2,1,0:T(8,128)(2,1)}), bf16[8,128,256]{2,1,0:T(8,128)(2,1)S(1)}, u32[]{:S(2)}, u32[]{:S(2)}) async-start(bf16[8,128,256]{2,1,0:T(8,128)(2,1)} %weight.1), calls=%async_computation.1 | async-start | bytes 1048576 | tf_op jit(solution)/shard_map/all_to_all | solution.py:28
  63.1 1.3 %collective-permute-start.4 = (bf16[192,128]{1,0:T(8,128)(2,1)S(1)}, bf16[192,128]{1,0:T(8,128)(2,1)S(1)}, u32[]{:S(2)}, u32[]{:S(2)}) collective-permute-start(bf16[192,128]{1,0:T(8,128)(2,1)S(1)} %copy-done.15), channel_id=1, source_target_pairs={{4,0},{8,4},{12,8},{16,12},{20,16},{24,20},{28,24},{32,28},{36,32}... | collective-permute-start | bytes 147464 | tf_op jit(solution)/shard_map/ppermute | solution.py:24
  64.4 1.3 %collective-permute-start.5 = (bf16[192,128]{1,0:T(8,128)(2,1)S(1)}, bf16[192,128]{1,0:T(8,128)(2,1)S(1)}, u32[]{:S(2)}, u32[]{:S(2)}) collective-permute-start(bf16[192,128]{1,0:T(8,128)(2,1)S(1)} %copy-done.14), channel_id=1, source_target_pairs={{128,0},{132,4},{136,8},{140,12},{144,16},{148,20},{152,24},{156,2... | collective-permute-start | bytes 147464 | tf_op jit(solution)/shard_map/ppermute | solution.py:24
  65.7 1.3 %collective-permute-start.6 = (bf16[192,128]{1,0:T(8,128)(2,1)S(1)}, bf16[192,128]{1,0:T(8,128)(2,1)S(1)}, u32[]{:S(2)}, u32[]{:S(2)}) collective-permute-start(bf16[192,128]{1,0:T(8,128)(2,1)S(1)} %copy-done.13), channel_id=1, source_target_pairs={{256,0},{260,4},{264,8},{268,12},{272,16},{276,20},{280,24},{284,2... | collective-permute-start | bytes 147464 | tf_op jit(solution)/shard_map/ppermute | solution.py:24
  67.1 1.3 %collective-permute-start.7 = (bf16[192,128]{1,0:T(8,128)(2,1)S(1)}, bf16[192,128]{1,0:T(8,128)(2,1)S(1)}, u32[]{:S(2)}, u32[]{:S(2)}) collective-permute-start(bf16[192,128]{1,0:T(8,128)(2,1)S(1)} %copy-done.12), channel_id=1, source_target_pairs={{512,0},{516,4},{520,8},{524,12},{528,16},{532,20},{536,24},{540,2... | collective-permute-start | bytes 147464 | tf_op jit(solution)/shard_map/ppermute | solution.py:24
  68.4 12.3 %all-to-all-done.1 = bf16[8,128,256]{2,1,0:T(8,128)(2,1)S(1)} async-done(((bf16[8,128,256]{2,1,0:T(8,128)(2,1)}), bf16[8,128,256]{2,1,0:T(8,128)(2,1)S(1)}, u32[]{:S(2)}, u32[]{:S(2)}) %all-to-all-start.1) | async-done | bytes 524320 | tf_op jit(solution)/shard_map/all_to_all | solution.py:28
  80.7 0.7 reduce_sum.21
  81.4 5.7 %all-to-all-start.2 = ((bf16[16,8,256]{2,1,0:T(8,128)(2,1)}), bf16[16,8,256]{2,1,0:T(8,128)(2,1)S(1)}, u32[]{:S(2)}, u32[]{:S(2)}) async-start(bf16[16,8,256]{2,1,0:T(8,128)(2,1)} %bitcast.1), calls=%async_computation.2 | async-start | bytes 131072 | tf_op jit(solution)/shard_map/all_to_all | solution.py:28
  87.3 0.7 copy.36
  88.0 0.7 copy.35
  88.7 10.9 %all-to-all-done.2 = bf16[16,8,256]{2,1,0:T(8,128)(2,1)S(1)} async-done(((bf16[16,8,256]{2,1,0:T(8,128)(2,1)}), bf16[16,8,256]{2,1,0:T(8,128)(2,1)S(1)}, u32[]{:S(2)}, u32[]{:S(2)}) %all-to-all-start.2) | async-done | bytes 65568 | tf_op jit(solution)/shard_map/all_to_all | solution.py:28
  99.6 0.6 convert_reduce_fusion
  (45 shorter events, 0.9 us)
Async XLA Ops:
  0.6 42.5 %copy-start = (s32[768,8]{0,1:T(8,128)S(1)}, s32[768,8]{0,1:T(8,128)}, u32[]{:S(2)}) copy-start(s32[768,8]{0,1:T(8,128)} %param.16) | copy-start | bytes 73732
  0.6 0.9 copy-start.6
  1.5 0.6 copy-start.2
  1.7 0.6 copy-start.3
  2.3 42.3 %collective-permute-start.3 = (bf16[192,128]{1,0:T(8,128)(2,1)S(1)}, bf16[192,128]{1,0:T(8,128)(2,1)S(1)}, u32[]{:S(2)}, u32[]{:S(2)}) collective-permute-start(bf16[192,128]{1,0:T(8,128)(2,1)S(1)} %pad_maximum_fusion), channel_id=1, source_target_pairs={{0,512},{4,516},{8,520},{12,524},{16,528},{20,532},{24,536},{28,54... | collective-permute-start | bytes 147464 | tf_op jit(solution)/shard_map/ppermute | solution.py:24
  21.6 23.0 %collective-permute-start.2 = (bf16[192,128]{1,0:T(8,128)(2,1)S(1)}, bf16[192,128]{1,0:T(8,128)(2,1)S(1)}, u32[]{:S(2)}, u32[]{:S(2)}) collective-permute-start(bf16[192,128]{1,0:T(8,128)(2,1)S(1)} %pad_maximum_fusion), channel_id=1, source_target_pairs={{0,256},{4,260},{8,264},{12,268},{16,272},{20,276},{24,280},{28,28... | collective-permute-start | bytes 147464 | tf_op jit(solution)/shard_map/ppermute | solution.py:24
  27.8 16.9 %collective-permute-start.1 = (bf16[192,128]{1,0:T(8,128)(2,1)S(1)}, bf16[192,128]{1,0:T(8,128)(2,1)S(1)}, u32[]{:S(2)}, u32[]{:S(2)}) collective-permute-start(bf16[192,128]{1,0:T(8,128)(2,1)S(1)} %pad_maximum_fusion), channel_id=1, source_target_pairs={{0,128},{4,132},{8,136},{12,140},{16,144},{20,148},{24,152},{28,15... | collective-permute-start | bytes 147464 | tf_op jit(solution)/shard_map/ppermute | solution.py:24
  32.1 12.6 %collective-permute-start = (bf16[192,128]{1,0:T(8,128)(2,1)S(1)}, bf16[192,128]{1,0:T(8,128)(2,1)S(1)}, u32[]{:S(2)}, u32[]{:S(2)}) collective-permute-start(bf16[192,128]{1,0:T(8,128)(2,1)S(1)} %pad_maximum_fusion), channel_id=1, source_target_pairs={{0,4},{4,8},{8,12},{12,16},{16,20},{20,24},{24,28},{28,32},{32,36}... | collective-permute-start | bytes 147464 | tf_op jit(solution)/shard_map/ppermute | solution.py:24
  35.6 17.8 %all-to-all-start = ((bf16[8,192,256]{2,1,0:T(8,128)(2,1)}), bf16[8,192,256]{2,1,0:T(8,128)(2,1)S(1)}, u32[]{:S(2)}, u32[]{:S(2)}) async-start(bf16[8,192,256]{2,1,0:T(8,128)(2,1)} %spread.1), calls=%async_computation | async-start | bytes 1572864 | tf_op jit(solution)/shard_map/all_to_all | solution.py:28
  42.3 0.7 copy-start.16
  43.2 0.7 copy-start.7
  44.6 0.6 copy-start.8
  44.6 0.6 copy-start.9
  44.6 0.6 copy-start.10
  45.3 0.6 copy-start.11
  49.7 3.4 %collective-permute-start.8 = (bf16[192,256]{1,0:T(8,128)(2,1)}, bf16[192,256]{1,0:T(8,128)(2,1)S(1)}, u32[]{:S(2)}, u32[]{:S(2)}) collective-permute-start(bf16[192,256]{1,0:T(8,128)(2,1)} %get-tuple-element.24.mine_ref), channel_id=1, source_target_pairs={{0,4},{4,0},{1,5},{5,1},{2,6},{6,2},{3,7},{7,3},{8,12},{12,8},{9,1... | collective-permute-start | bytes 294920 | tf_op jit(solution)/shard_map/ppermute | solution.py:216
  53.1 0.6 copy-start.5
  53.3 0.9 copy-start.1
  56.8 6.4 %copy-start.15 = (bf16[192,128]{1,0:T(8,128)(2,1)S(1)}, bf16[192,128]{1,0:T(8,128)(2,1)}, u32[]{:S(2)}) copy-start(bf16[192,128]{1,0:T(8,128)(2,1)} %get-tuple-element.12) | copy-start | bytes 147460
  56.8 7.7 %copy-start.14 = (bf16[192,128]{1,0:T(8,128)(2,1)S(1)}, bf16[192,128]{1,0:T(8,128)(2,1)}, u32[]{:S(2)}) copy-start(bf16[192,128]{1,0:T(8,128)(2,1)} %get-tuple-element.13) | copy-start | bytes 147460
  56.8 9.0 %copy-start.13 = (bf16[192,128]{1,0:T(8,128)(2,1)S(1)}, bf16[192,128]{1,0:T(8,128)(2,1)}, u32[]{:S(2)}) copy-start(bf16[192,128]{1,0:T(8,128)(2,1)} %get-tuple-element.14) | copy-start | bytes 147460
  56.8 10.3 %copy-start.12 = (bf16[192,128]{1,0:T(8,128)(2,1)S(1)}, bf16[192,128]{1,0:T(8,128)(2,1)}, u32[]{:S(2)}) copy-start(bf16[192,128]{1,0:T(8,128)(2,1)} %get-tuple-element.15) | copy-start | bytes 147460
  56.8 23.9 %all-to-all-start.1 = ((bf16[8,128,256]{2,1,0:T(8,128)(2,1)}), bf16[8,128,256]{2,1,0:T(8,128)(2,1)S(1)}, u32[]{:S(2)}, u32[]{:S(2)}) async-start(bf16[8,128,256]{2,1,0:T(8,128)(2,1)} %weight.1), calls=%async_computation.1 | async-start | bytes 1048576 | tf_op jit(solution)/shard_map/all_to_all | solution.py:28
  63.1 24.0 %collective-permute-start.4 = (bf16[192,128]{1,0:T(8,128)(2,1)S(1)}, bf16[192,128]{1,0:T(8,128)(2,1)S(1)}, u32[]{:S(2)}, u32[]{:S(2)}) collective-permute-start(bf16[192,128]{1,0:T(8,128)(2,1)S(1)} %copy-done.15), channel_id=1, source_target_pairs={{4,0},{8,4},{12,8},{16,12},{20,16},{24,20},{28,24},{32,28},{36,32}... | collective-permute-start | bytes 147464 | tf_op jit(solution)/shard_map/ppermute | solution.py:24
  64.4 22.7 %collective-permute-start.5 = (bf16[192,128]{1,0:T(8,128)(2,1)S(1)}, bf16[192,128]{1,0:T(8,128)(2,1)S(1)}, u32[]{:S(2)}, u32[]{:S(2)}) collective-permute-start(bf16[192,128]{1,0:T(8,128)(2,1)S(1)} %copy-done.14), channel_id=1, source_target_pairs={{128,0},{132,4},{136,8},{140,12},{144,16},{148,20},{152,24},{156,2... | collective-permute-start | bytes 147464 | tf_op jit(solution)/shard_map/ppermute | solution.py:24
  65.7 21.4 %collective-permute-start.6 = (bf16[192,128]{1,0:T(8,128)(2,1)S(1)}, bf16[192,128]{1,0:T(8,128)(2,1)S(1)}, u32[]{:S(2)}, u32[]{:S(2)}) collective-permute-start(bf16[192,128]{1,0:T(8,128)(2,1)S(1)} %copy-done.13), channel_id=1, source_target_pairs={{256,0},{260,4},{264,8},{268,12},{272,16},{276,20},{280,24},{284,2... | collective-permute-start | bytes 147464 | tf_op jit(solution)/shard_map/ppermute | solution.py:24
  67.1 20.1 %collective-permute-start.7 = (bf16[192,128]{1,0:T(8,128)(2,1)S(1)}, bf16[192,128]{1,0:T(8,128)(2,1)S(1)}, u32[]{:S(2)}, u32[]{:S(2)}) collective-permute-start(bf16[192,128]{1,0:T(8,128)(2,1)S(1)} %copy-done.12), channel_id=1, source_target_pairs={{512,0},{516,4},{520,8},{524,12},{528,16},{532,20},{536,24},{540,2... | collective-permute-start | bytes 147464 | tf_op jit(solution)/shard_map/ppermute | solution.py:24
  81.4 5.7 %copy-start.4 = (f32[192,128]{1,0:T(8,128)S(1)}, f32[192,128]{1,0:T(8,128)}, u32[]{:S(2)}) copy-start(f32[192,128]{1,0:T(8,128)} %get-tuple-element.11) | copy-start | bytes 294916
  81.4 18.2 %all-to-all-start.2 = ((bf16[16,8,256]{2,1,0:T(8,128)(2,1)}), bf16[16,8,256]{2,1,0:T(8,128)(2,1)S(1)}, u32[]{:S(2)}, u32[]{:S(2)}) async-start(bf16[16,8,256]{2,1,0:T(8,128)(2,1)} %bitcast.1), calls=%async_computation.2 | async-start | bytes 131072 | tf_op jit(solution)/shard_map/all_to_all | solution.py:28

commit v2 on v1

v2 whole, which is shorter than its diff:
```python
import functools

import jax
import jax.numpy as jnp
from jax import lax
from jax.experimental import pallas as pl
from jax.experimental.pallas import tpu as pltpu
from jax.sharding import Mesh
from jax.sharding import PartitionSpec as P

DH = 64
BLOCK = 64
PER = 2
LEVELS = 4
SIDES = (8, 2)
KV = ("z", "y", "c")
NT = (((1,), (1,)), ((), ()))
TN = (((0,), (0,)), ((), ()))
VMEM_LIMIT = 16 * 2**20


def shifted(block, axis, distance):
    devices = range(lax.axis_size(axis))
    route = [(i - distance, i) for i in devices if i - distance in devices]
    return lax.ppermute(block, axis, route)


def exchanged(tiles, axis):
    return lax.all_to_all(tiles, axis, split_axis=0, concat_axis=0, tiled=True)


def dot(a, b, dims=(((1,), (0,)), ((), ()))):
    return lax.dot_general(a, b, dims, preferred_element_type=jnp.float32)


def call(kernel, flops, out_shape, *args, smem=0, scratch=()):
    vmem = pl.BlockSpec(memory_space=pltpu.VMEM)
    many = isinstance(out_shape, tuple)
    size = sum(a.size * a.dtype.itemsize for a in args)
    return pl.pallas_call(
        kernel,
        out_shape=out_shape,
        in_specs=[pl.BlockSpec(memory_space=pltpu.SMEM)] * smem + [vmem] * (len(args) - smem),
        out_specs=(vmem,) * len(out_shape) if many else vmem,
        scratch_shapes=scratch,
        cost_estimate=pl.CostEstimate(flops=flops, bytes_accessed=size, transcendentals=0),
        compiler_params=pltpu.CompilerParams(vmem_limit_bytes=VMEM_LIMIT),
    )(*args)


def turned(x):
    return jnp.transpose(x.astype(jnp.float32))


def pack_kernel(k_ref, v_ref, out_ref):
    out_ref[...] = turned(jnp.concatenate([k_ref[...], v_ref[...]], axis=0)).astype(out_ref.dtype)


def pack(k, v):
    shape = jax.ShapeDtypeStruct((k.shape[1], 2 * k.shape[0]), k.dtype)
    return call(pack_kernel, 10**6, shape, k, v)


def spread_kernel(rows, ys, cores, peers, x_ref, out_ref):
    width = x_ref.shape[1]
    source = lax.broadcasted_iota(jnp.int32, (width, 1), 0)
    target = lax.broadcasted_iota(jnp.int32, (width, width), 1)
    inner, left = source & (rows - 1), source // rows
    core, left = left & (cores - 1), left // cores
    y, z = left & (ys - 1), left // ys
    zs = width // (rows * cores * ys)
    place = ((core * ys + y) * zs + z) * rows + inner
    move = jnp.where(place == target, 1.0, 0.0).astype(jnp.bfloat16)
    moved = dot(x_ref[...], move).astype(jnp.bfloat16)
    part = width // cores
    for core in range(cores):
        for peer in range(peers):
            out_ref[core * peers + peer] = moved[:, core * part : (core + 1) * part]


def spread(x, rows, ys, cores, peers):
    tokens, width = x.shape
    kernel = functools.partial(spread_kernel, rows, ys, cores, peers)
    shape = jax.ShapeDtypeStruct((cores * peers, tokens, width // cores), x.dtype)
    return call(kernel, 2 * tokens * width * width, shape, x)


def stacked(block, at):
    block = block.astype(jnp.float32)
    lane = lax.broadcasted_iota(jnp.int32, (BLOCK, 2 * DH), 1)
    keep = (lane >= at) & (lane < at + DH)
    parts = []
    for head in range(block.shape[1] // DH):
        pair = block[:, (head // 2) * 2 * DH : (head // 2 + 1) * 2 * DH]
        if (head % 2) * DH != at:
            pair = pltpu.roll(pair, DH, 1)
        parts.append(jnp.where(keep, pair, 0.0))
    return jnp.concatenate(parts, axis=0)


def row_sums(terms, pieces):
    ones = jnp.ones((8, terms.shape[1]), jnp.bfloat16)
    total = None
    for _ in range(pieces):
        piece = terms.astype(jnp.bfloat16)
        terms = terms - piece.astype(jnp.float32)
        part = dot(ones, piece, NT)
        total = part if total is None else total + part
    return total[:1]


def attention_kernel(distances, chosen_ref, q_ref, go_ref, ao_ref, lse_ref, kv_ref, *refs):
    far_refs = refs[:LEVELS]
    gq_ref, own_ref = refs[LEVELS : LEVELS + 2]
    back_refs = refs[LEVELS + 2 : 2 * LEVELS + 2]
    sums = refs[2 * LEVELS + 2]
    blocks = q_ref.shape[0] // BLOCK
    heads = q_ref.shape[1] // DH
    me = lax.axis_index(KV)
    lane = lax.broadcasted_iota(jnp.int32, (BLOCK, 2 * DH), 1)
    sums[...] = jnp.zeros_like(sums)
    key_at = lax.broadcasted_iota(jnp.int32, (BLOCK, heads * BLOCK), 0)
    query_at = lax.broadcasted_iota(jnp.int32, (BLOCK, heads * BLOCK), 1) & (BLOCK - 1)
    causal = key_at <= query_at
    for b in range(blocks):
        rows = slice(b * BLOCK, (b + 1) * BLOCK)
        low = stacked(q_ref[rows] * DH ** (-0.5), 0)
        high = stacked(go_ref[rows], DH)
        delta = row_sums(high * stacked(ao_ref[rows], DH), 2)
        lse = jnp.concatenate([lse_ref[h : h + 1, rows] for h in range(heads)], axis=1)
        low = low.astype(jnp.bfloat16)
        high = high.astype(jnp.bfloat16)
        places = []
        for n in range(LEVELS * PER):
            block = chosen_ref[n, me * blocks + b]
            block = jnp.where(block >= 0, block - (me - distances[n // PER]) * blocks, 0)
            places.append(pl.multiple_of(block * BLOCK, BLOCK))
        kv = jnp.concatenate(
            [kv_ref[rows]]
            + [far_refs[n // PER][pl.ds(places[n], BLOCK), :] for n in range(LEVELS * PER)],
            axis=0,
        )
        weights = jnp.exp(dot(kv, low, NT) - lse)
        weights = jnp.concatenate(
            [jnp.where(causal, weights[:BLOCK], 0.0), weights[BLOCK:]], axis=0
        )
        dscores = (weights * (dot(kv, high, NT) - delta)).astype(jnp.bfloat16)
        grad_kv = dot(dscores, low) + dot(weights.astype(jnp.bfloat16), high)
        own_ref[rows] = grad_kv[:BLOCK]
        for n in range(LEVELS * PER):
            at = pl.ds(places[n], BLOCK)
            sums[n // PER, at, :] += grad_kv[(n + 1) * BLOCK : (n + 2) * BLOCK]
        grad_q = dot(dscores, kv, TN) * DH ** (-0.5)
        for pair in range(heads // 2):
            first = grad_q[2 * pair * BLOCK : (2 * pair + 1) * BLOCK]
            second = grad_q[(2 * pair + 1) * BLOCK : (2 * pair + 2) * BLOCK]
            gq_ref[rows, pair * 2 * DH : (pair + 1) * 2 * DH] = jnp.where(
                lane < DH, first, pltpu.roll(second, DH, 1)
            ).astype(gq_ref.dtype)
    for level in range(LEVELS):
        back_refs[level][...] = sums[level].astype(jnp.bfloat16)


def attention(distances, chosen, q, go, ao, lse, kv, far):
    tokens, width = q.shape
    shape = (jax.ShapeDtypeStruct((tokens, width), jnp.bfloat16),)
    shape += (jax.ShapeDtypeStruct(kv.shape, jnp.float32),)
    shape += (jax.ShapeDtypeStruct(kv.shape, jnp.bfloat16),) * LEVELS
    return call(
        functools.partial(attention_kernel, distances),
        2 * 10**9,
        shape,
        chosen,
        q,
        go,
        ao,
        lse,
        kv,
        *far,
        smem=1,
        scratch=[pltpu.VMEM((LEVELS, *kv.shape), jnp.float32)],
    )


def weight_kernel(mine_ref, other_ref, x_ref, out_ref):
    core = lax.axis_index("c")
    peers = x_ref.shape[0] // 2
    ys = out_ref.shape[0]
    grads = jnp.concatenate([mine_ref[...], other_ref[...]], axis=0)
    for peer in range(peers):
        x = jnp.concatenate(
            [x_ref[core * peers + peer], x_ref[(1 - core) * peers + peer]], axis=0
        )
        part = dot(x, grads, TN).astype(out_ref.dtype)
        step = part.shape[0] // ys
        for y in range(ys):
            out_ref[y, peer * step : (peer + 1) * step] = part[y * step : (y + 1) * step]


def weight(mine, other, x, ys):
    peers, tokens, part = x.shape[0] // 2, x.shape[1], x.shape[2]
    shape = jax.ShapeDtypeStruct((ys, peers * part // ys, mine.shape[1]), jnp.bfloat16)
    flops = 4 * tokens * peers * part * mine.shape[1]
    return call(weight_kernel, flops, shape, mine, other, x)


def sum_kernel(tiles_ref, out_ref):
    total = tiles_ref[0].astype(jnp.float32)
    for n in range(1, tiles_ref.shape[0]):
        total = total + tiles_ref[n].astype(jnp.float32)
    out_ref[...] = total.astype(out_ref.dtype)


def summed(tiles, dtype):
    shape = jax.ShapeDtypeStruct(tiles.shape[1:], dtype)
    return call(sum_kernel, tiles.size, shape, tiles)


def collect_kernel(own_ref, *refs):
    total = own_ref[...]
    for ref in refs[:LEVELS]:
        total = total + ref[...].astype(jnp.float32)
    total = turned(total)
    width = total.shape[0] // 2
    refs[LEVELS][...] = total[:width].astype(jnp.bfloat16)
    refs[LEVELS + 1][...] = total[width:].astype(jnp.bfloat16)


def collect(own, back):
    shape = jax.ShapeDtypeStruct((own.shape[1] // 2, own.shape[0]), jnp.bfloat16)
    return call(collect_kernel, 10**6, (shape, shape), own, *back)


def shards(layer_input, queries, keys, values, attn_out, grad_out, log_sum, chosen):
    axis_size = lax.axis_size(KV)
    ys, cores, peers = lax.axis_size("y"), lax.axis_size("c"), lax.axis_size("x")
    out_rows = layer_input.shape[1] * peers // axis_size
    distances = [1, axis_size // 8, axis_size // 4, axis_size // 2]
    key_pair = pack(keys.T, values.T)
    far = []
    for distance in distances:
        far.append(shifted(key_pair, KV, distance))
    sent = spread(layer_input, out_rows, ys, cores, peers)
    whole_input = exchanged(sent, ("c", "x"))
    grad_queries, own, *back = attention(
        distances, chosen.T, queries, grad_out, attn_out, log_sum.T, key_pair, far
    )
    route = [(i, cores - 1 - i) for i in range(cores)]
    other = lax.ppermute(grad_queries, "c", route)
    parts = weight(grad_queries, other, whole_input, ys)
    over_y = exchanged(parts, "y")
    returned = []
    for level, distance in enumerate(distances):
        returned.append(shifted(back[level], KV, -distance))
    over_y = summed(over_y.reshape(ys, -1, out_rows, over_y.shape[2]), jnp.bfloat16)
    over_z = exchanged(over_y, "z")
    grad_keys, grad_values = collect(own, returned)
    grad_weight = summed(over_z, jnp.float32)
    return (grad_queries, grad_keys.T, grad_values.T, grad_weight)


def solution(mesh):
    ys, cores = SIDES
    shape = (mesh.shape["kv"] // (ys * cores), ys, cores, mesh.shape["tp"])
    torus = Mesh(mesh.devices.reshape(shape), (*KV, "x"))
    return jax.shard_map(
        shards,
        mesh=torus,
        in_specs=(P(KV, "x"),) * 7 + (P(),),
        out_specs=(P(KV, "x"),) * 4,
        check_vma=False,
    )
```

time: 102 us -> 110 us (1.078)
  the two profiles are of different devices: /device:TPU:6 before, /device:TPU:67 now
where the time goes in v2:
time: 110 us; the launch traced here: 109 us
  starting transfers between devices  55.7 us (51%)
  blocking collectives  22.6 us (21%)
  waiting for transfers between devices  20.8 us (19%)
  Pallas kernels  7.26 us (7%)
  local copies, waits for them, and re-layouts  1.84 us (2%)
    ppermute x8, starting transfers between devices, shifted(): return lax.ppermute(block, axis, route)  40.1 us
    all_to_all x1, blocking collectives, exchanged(): return lax.all_to_all(tiles, axis, split_axis=0, concat_axis=0, tiled=True)  22.6 us
    ppermute x8, waiting for transfers between devices, shifted(): return lax.ppermute(block, axis, route)  19.6 us
    all_to_all x2, starting transfers between devices, exchanged(): return lax.all_to_all(tiles, axis, split_axis=0, concat_axis=0, tiled=True)  10.5 us
    pallas_call x7, Pallas kernels, call(): pl.pallas_call(kernel, out_shape=out_shape, in_specs=[pl.BlockSpec(memory...  7.26 us
    ppermute x1, starting transfers between devices, shards(): other = lax.ppermute(grad_queries, 'c', route)  5.17 us
  transfers between devices with their start and end apart: 11, of which 5 were waited for; matrix products, arithmetic and copies ran while one was open for 0% of the time, Pallas kernels for 4%

profile of v2, /device:TPU:67, one launch (start us, length us, event | category | flops | bytes accessed | tf_op | source)
XLA Modules:
  0.0 109.0 jit_solution(5787671166734245225)
XLA Ops:
  0.6 0.9 copy-done
  1.6 1.2 %shard_map.114 = bf16[8,192,256]{2,1,0:T(8,128)(2,1)} custom-call(bf16[192,512]{1,0:T(8,128)(2,1)S(1)} %copy-done), custom_call_target="tpu_custom_call" | custom-call | flops 100663296 | bytes 196608 | tf_op jit(solution)/shard_map/pallas_call | solution.py:40
  2.8 0.0 copy-start.7
  2.8 5.3 %all-to-all-start = ((bf16[8,192,256]{2,1,0:T(8,128)(2,1)}), bf16[8,192,256]{2,1,0:T(8,128)(2,1)S(1)}, u32[]{:S(2)}, u32[]{:S(2)}) async-start(bf16[8,192,256]{2,1,0:T(8,128)(2,1)} %shard_map.114), calls=%async_computation | async-start | bytes 1572864 | tf_op jit(solution)/shard_map/all_to_all | solution.py:29
  8.1 0.0 copy-start.8
  8.1 0.1 shard_map.111.kv_ref
  8.2 18.2 %collective-permute-start.3 = (bf16[192,128]{1,0:T(8,128)(2,1)S(1)}, bf16[192,128]{1,0:T(8,128)(2,1)S(1)}, u32[]{:S(2)}, u32[]{:S(2)}) collective-permute-start(bf16[192,128]{1,0:T(8,128)(2,1)S(1)} %shard_map.111.kv_ref), channel_id=1, source_target_pairs={{0,512},{4,516},{8,520},{12,524},{16,528},{20,532},{24,536},{28,54... | collective-permute-start | bytes 147464 | tf_op jit(solution)/shard_map/ppermute | solution.py:25
  26.4 5.8 %collective-permute-start.2 = (bf16[192,128]{1,0:T(8,128)(2,1)S(1)}, bf16[192,128]{1,0:T(8,128)(2,1)S(1)}, u32[]{:S(2)}, u32[]{:S(2)}) collective-permute-start(bf16[192,128]{1,0:T(8,128)(2,1)S(1)} %shard_map.111.kv_ref), channel_id=1, source_target_pairs={{0,256},{4,260},{8,264},{12,268},{16,272},{20,276},{24,280},{28,28... | collective-permute-start | bytes 147464 | tf_op jit(solution)/shard_map/ppermute | solution.py:25
  32.2 4.0 %collective-permute-start.1 = (bf16[192,128]{1,0:T(8,128)(2,1)S(1)}, bf16[192,128]{1,0:T(8,128)(2,1)S(1)}, u32[]{:S(2)}, u32[]{:S(2)}) collective-permute-start(bf16[192,128]{1,0:T(8,128)(2,1)S(1)} %shard_map.111.kv_ref), channel_id=1, source_target_pairs={{0,128},{4,132},{8,136},{12,140},{16,144},{20,148},{24,152},{28,15... | collective-permute-start | bytes 147464 | tf_op jit(solution)/shard_map/ppermute | solution.py:25
  36.2 4.3 %collective-permute-start = (bf16[192,128]{1,0:T(8,128)(2,1)S(1)}, bf16[192,128]{1,0:T(8,128)(2,1)S(1)}, u32[]{:S(2)}, u32[]{:S(2)}) collective-permute-start(bf16[192,128]{1,0:T(8,128)(2,1)S(1)} %shard_map.111.kv_ref), channel_id=1, source_target_pairs={{0,4},{4,8},{8,12},{12,16},{16,20},{20,24},{24,28},{28,32},{32,36}... | collective-permute-start | bytes 147464 | tf_op jit(solution)/shard_map/ppermute | solution.py:25
  40.6 0.0 collective-permute-done.3.refs_3_
  40.6 0.0 collective-permute-done.2.refs_2_
  40.6 0.0 collective-permute-done.1.refs_1_
  40.6 1.1 %collective-permute-done.refs_0_ = bf16[192,128]{1,0:T(8,128)(2,1)S(1)} collective-permute-done((bf16[192,128]{1,0:T(8,128)(2,1)S(1)}, bf16[192,128]{1,0:T(8,128)(2,1)S(1)}, u32[]{:S(2)}, u32[]{:S(2)}) %collective-permute-start) | collective-permute-done | bytes 49184 | tf_op jit(solution)/shard_map/ppermute | solution.py:25
  41.8 3.4 %shard_map.112 = (bf16[192,256]{1,0:T(8,128)(2,1)}, f32[192,128]{1,0:T(8,128)S(1)}, bf16[192,128]{1,0:T(8,128)(2,1)S(1)}, bf16[192,128]{1,0:T(8,128)(2,1)S(1)}, ...) custom-call(s32[8,768]{1,0:T(8,128)S(1)} %bitcast.10, bf16[192,256]{1,0:T(8,128)(2,1)S(1)} %copy-done.4, ...), custom_call_target="tpu_custom_call" | custom-call | flops 2000000000 | bytes 568320 | tf_op jit(solution)/shard_map/pallas_call | solution.py:40
  45.2 5.2 %collective-permute-start.8 = (bf16[192,256]{1,0:T(8,128)(2,1)}, bf16[192,256]{1,0:T(8,128)(2,1)S(1)}, u32[]{:S(2)}, u32[]{:S(2)}) collective-permute-start(bf16[192,256]{1,0:T(8,128)(2,1)} %get-tuple-element.8.mine_ref), channel_id=1, source_target_pairs={{0,4},{4,0},{1,5},{5,1},{2,6},{6,2},{3,7},{7,3},{8,12},{12,8},{9,1... | collective-permute-start | bytes 294920 | tf_op jit(solution)/shard_map/ppermute | solution.py:249
  50.3 1.1 %collective-permute-done.8.other_ref = bf16[192,256]{1,0:T(8,128)(2,1)S(1)} collective-permute-done((bf16[192,256]{1,0:T(8,128)(2,1)}, bf16[192,256]{1,0:T(8,128)(2,1)S(1)}, u32[]{:S(2)}, u32[]{:S(2)}) %collective-permute-start.8) | collective-permute-done | bytes 98336 | tf_op jit(solution)/shard_map/ppermute | solution.py:249
  51.5 0.0 all-to-all-done.x_ref
  51.5 0.9 copy-done.1
  52.4 0.5 shard_map.115
  52.9 22.6 %all_to_all.15 = bf16[8,128,256]{2,1,0:T(8,128)(2,1)S(1)} all-to-all(bf16[8,128,256]{2,1,0:T(8,128)(2,1)S(1)} %shard_map.115), channel_id=1, replica_groups=mesh['z'=16,'y'=8,'c'=2,'x'=4] {'y'}, dimensions={0} | all-to-all | bytes 1048576 | tf_op jit(solution)/shard_map/all_to_all | solution.py:29
  75.4 0.7 shard_map.116
  76.1 5.2 %all-to-all-start.2 = ((bf16[16,8,256]{2,1,0:T(8,128)(2,1)}), bf16[16,8,256]{2,1,0:T(8,128)(2,1)S(1)}, u32[]{:S(2)}, u32[]{:S(2)}) async-start(bf16[16,8,256]{2,1,0:T(8,128)(2,1)} %shard_map.116), calls=%async_computation.2 | async-start | bytes 131072 | tf_op jit(solution)/shard_map/all_to_all | solution.py:29
  81.3 3.9 %collective-permute-start.4 = (bf16[192,128]{1,0:T(8,128)(2,1)S(1)}, bf16[192,128]{1,0:T(8,128)(2,1)S(1)}, u32[]{:S(2)}, u32[]{:S(2)}) collective-permute-start(bf16[192,128]{1,0:T(8,128)(2,1)S(1)} %get-tuple-element.14), channel_id=1, source_target_pairs={{4,0},{8,4},{12,8},{16,12},{20,16},{24,20},{28,24},{32,28},{36,32}... | collective-permute-start | bytes 147464 | tf_op jit(solution)/shard_map/ppermute | solution.py:25
  85.2 1.3 %collective-permute-start.5 = (bf16[192,128]{1,0:T(8,128)(2,1)S(1)}, bf16[192,128]{1,0:T(8,128)(2,1)S(1)}, u32[]{:S(2)}, u32[]{:S(2)}) collective-permute-start(bf16[192,128]{1,0:T(8,128)(2,1)S(1)} %get-tuple-element.15), channel_id=1, source_target_pairs={{128,0},{132,4},{136,8},{140,12},{144,16},{148,20},{152,24},{156,2... | collective-permute-start | bytes 147464 | tf_op jit(solution)/shard_map/ppermute | solution.py:25
  86.5 1.3 %collective-permute-start.6 = (bf16[192,128]{1,0:T(8,128)(2,1)S(1)}, bf16[192,128]{1,0:T(8,128)(2,1)S(1)}, u32[]{:S(2)}, u32[]{:S(2)}) collective-permute-start(bf16[192,128]{1,0:T(8,128)(2,1)S(1)} %get-tuple-element.16), channel_id=1, source_target_pairs={{256,0},{260,4},{264,8},{268,12},{272,16},{276,20},{280,24},{284,2... | collective-permute-start | bytes 147464 | tf_op jit(solution)/shard_map/ppermute | solution.py:25
  87.8 1.3 %collective-permute-start.7 = (bf16[192,128]{1,0:T(8,128)(2,1)S(1)}, bf16[192,128]{1,0:T(8,128)(2,1)S(1)}, u32[]{:S(2)}, u32[]{:S(2)}) collective-permute-start(bf16[192,128]{1,0:T(8,128)(2,1)S(1)} %get-tuple-element.17), channel_id=1, source_target_pairs={{512,0},{516,4},{520,8},{524,12},{528,16},{532,20},{536,24},{540,2... | collective-permute-start | bytes 147464 | tf_op jit(solution)/shard_map/ppermute | solution.py:25
  89.1 2.5 %collective-permute-done.5.refs_1_ = bf16[192,128]{1,0:T(8,128)(2,1)S(1)} collective-permute-done((bf16[192,128]{1,0:T(8,128)(2,1)S(1)}, bf16[192,128]{1,0:T(8,128)(2,1)S(1)}, u32[]{:S(2)}, u32[]{:S(2)}) %collective-permute-start.5) | collective-permute-done | bytes 49184 | tf_op jit(solution)/shard_map/ppermute | solution.py:25
  91.6 4.9 %collective-permute-done.6.refs_2_ = bf16[192,128]{1,0:T(8,128)(2,1)S(1)} collective-permute-done((bf16[192,128]{1,0:T(8,128)(2,1)S(1)}, bf16[192,128]{1,0:T(8,128)(2,1)S(1)}, u32[]{:S(2)}, u32[]{:S(2)}) %collective-permute-start.6) | collective-permute-done | bytes 49184 | tf_op jit(solution)/shard_map/ppermute | solution.py:25
  96.5 11.1 %collective-permute-done.7.refs_3_ = bf16[192,128]{1,0:T(8,128)(2,1)S(1)} collective-permute-done((bf16[192,128]{1,0:T(8,128)(2,1)S(1)}, bf16[192,128]{1,0:T(8,128)(2,1)S(1)}, u32[]{:S(2)}, u32[]{:S(2)}) %collective-permute-start.7) | collective-permute-done | bytes 49184 | tf_op jit(solution)/shard_map/ppermute | solution.py:25
  107.6 0.7 shard_map.113
  108.4 0.6 shard_map.117
  (16 shorter events, 0.0 us)
Async XLA Ops:
  0.6 0.9 copy-start
  2.8 5.3 %copy-start.2 = (bf16[192,64]{0,1:T(8,128)(2,1)S(1)}, bf16[192,64]{0,1:T(8,128)(2,1)}, u32[]{:S(2)}) copy-start(bf16[192,64]{0,1:T(8,128)(2,1)} %param.10) | copy-start | bytes 73732
  2.8 5.3 %copy-start.3 = (bf16[192,64]{0,1:T(8,128)(2,1)S(1)}, bf16[192,64]{0,1:T(8,128)(2,1)}, u32[]{:S(2)}) copy-start(bf16[192,64]{0,1:T(8,128)(2,1)} %param.11) | copy-start | bytes 73732
  2.8 38.9 %copy-start.5 = (bf16[192,256]{1,0:T(8,128)(2,1)S(1)}, bf16[192,256]{1,0:T(8,128)(2,1)}, u32[]{:S(2)}) copy-start(bf16[192,256]{1,0:T(8,128)(2,1)} %go_ref.1) | copy-start | bytes 294916
  2.8 38.9 %copy-start.6 = (bf16[192,256]{1,0:T(8,128)(2,1)S(1)}, bf16[192,256]{1,0:T(8,128)(2,1)}, u32[]{:S(2)}) copy-start(bf16[192,256]{1,0:T(8,128)(2,1)} %ao_ref.1) | copy-start | bytes 294916
  2.8 38.9 %copy-start.7 = (s32[768,8]{0,1:T(8,128)S(1)}, s32[768,8]{0,1:T(8,128)}, u32[]{:S(2)}) copy-start(s32[768,8]{0,1:T(8,128)} %param.15) | copy-start | bytes 73732
  2.8 48.7 %all-to-all-start = ((bf16[8,192,256]{2,1,0:T(8,128)(2,1)}), bf16[8,192,256]{2,1,0:T(8,128)(2,1)S(1)}, u32[]{:S(2)}, u32[]{:S(2)}) async-start(bf16[8,192,256]{2,1,0:T(8,128)(2,1)} %shard_map.114), calls=%async_computation | async-start | bytes 1572864 | tf_op jit(solution)/shard_map/all_to_all | solution.py:29
  8.1 33.7 %copy-start.4 = (bf16[192,256]{1,0:T(8,128)(2,1)S(1)}, bf16[192,256]{1,0:T(8,128)(2,1)}, u32[]{:S(2)}) copy-start(bf16[192,256]{1,0:T(8,128)(2,1)} %q_ref.1) | copy-start | bytes 294916
  8.1 33.7 %copy-start.8 = (f32[192,4]{0,1:T(4,128)S(1)}, f32[192,4]{0,1:T(4,128)}, u32[]{:S(2)}) copy-start(f32[192,4]{0,1:T(4,128)} %param.14) | copy-start | bytes 9220
  8.2 32.4 %collective-permute-start.3 = (bf16[192,128]{1,0:T(8,128)(2,1)S(1)}, bf16[192,128]{1,0:T(8,128)(2,1)S(1)}, u32[]{:S(2)}, u32[]{:S(2)}) collective-permute-start(bf16[192,128]{1,0:T(8,128)(2,1)S(1)} %shard_map.111.kv_ref), channel_id=1, source_target_pairs={{0,512},{4,516},{8,520},{12,524},{16,528},{20,532},{24,536},{28,54... | collective-permute-start | bytes 147464 | tf_op jit(solution)/shard_map/ppermute | solution.py:25
  26.4 14.2 %collective-permute-start.2 = (bf16[192,128]{1,0:T(8,128)(2,1)S(1)}, bf16[192,128]{1,0:T(8,128)(2,1)S(1)}, u32[]{:S(2)}, u32[]{:S(2)}) collective-permute-start(bf16[192,128]{1,0:T(8,128)(2,1)S(1)} %shard_map.111.kv_ref), channel_id=1, source_target_pairs={{0,256},{4,260},{8,264},{12,268},{16,272},{20,276},{24,280},{28,28... | collective-permute-start | bytes 147464 | tf_op jit(solution)/shard_map/ppermute | solution.py:25
  32.2 8.4 %collective-permute-start.1 = (bf16[192,128]{1,0:T(8,128)(2,1)S(1)}, bf16[192,128]{1,0:T(8,128)(2,1)S(1)}, u32[]{:S(2)}, u32[]{:S(2)}) collective-permute-start(bf16[192,128]{1,0:T(8,128)(2,1)S(1)} %shard_map.111.kv_ref), channel_id=1, source_target_pairs={{0,128},{4,132},{8,136},{12,140},{16,144},{20,148},{24,152},{28,15... | collective-permute-start | bytes 147464 | tf_op jit(solution)/shard_map/ppermute | solution.py:25
  36.2 5.5 %collective-permute-start = (bf16[192,128]{1,0:T(8,128)(2,1)S(1)}, bf16[192,128]{1,0:T(8,128)(2,1)S(1)}, u32[]{:S(2)}, u32[]{:S(2)}) collective-permute-start(bf16[192,128]{1,0:T(8,128)(2,1)S(1)} %shard_map.111.kv_ref), channel_id=1, source_target_pairs={{0,4},{4,8},{8,12},{12,16},{16,20},{20,24},{24,28},{28,32},{32,36}... | collective-permute-start | bytes 147464 | tf_op jit(solution)/shard_map/ppermute | solution.py:25
  45.2 6.3 %collective-permute-start.8 = (bf16[192,256]{1,0:T(8,128)(2,1)}, bf16[192,256]{1,0:T(8,128)(2,1)S(1)}, u32[]{:S(2)}, u32[]{:S(2)}) collective-permute-start(bf16[192,256]{1,0:T(8,128)(2,1)} %get-tuple-element.8.mine_ref), channel_id=1, source_target_pairs={{0,4},{4,0},{1,5},{5,1},{2,6},{6,2},{3,7},{7,3},{8,12},{12,8},{9,1... | collective-permute-start | bytes 294920 | tf_op jit(solution)/shard_map/ppermute | solution.py:249
  51.5 0.9 copy-start.1
  76.1 32.3 %all-to-all-start.2 = ((bf16[16,8,256]{2,1,0:T(8,128)(2,1)}), bf16[16,8,256]{2,1,0:T(8,128)(2,1)S(1)}, u32[]{:S(2)}, u32[]{:S(2)}) async-start(bf16[16,8,256]{2,1,0:T(8,128)(2,1)} %shard_map.116), calls=%async_computation.2 | async-start | bytes 131072 | tf_op jit(solution)/shard_map/all_to_all | solution.py:29
  81.3 7.8 %collective-permute-start.4 = (bf16[192,128]{1,0:T(8,128)(2,1)S(1)}, bf16[192,128]{1,0:T(8,128)(2,1)S(1)}, u32[]{:S(2)}, u32[]{:S(2)}) collective-permute-start(bf16[192,128]{1,0:T(8,128)(2,1)S(1)} %get-tuple-element.14), channel_id=1, source_target_pairs={{4,0},{8,4},{12,8},{16,12},{20,16},{24,20},{28,24},{32,28},{36,32}... | collective-permute-start | bytes 147464 | tf_op jit(solution)/shard_map/ppermute | solution.py:25
  85.2 6.4 %collective-permute-start.5 = (bf16[192,128]{1,0:T(8,128)(2,1)S(1)}, bf16[192,128]{1,0:T(8,128)(2,1)S(1)}, u32[]{:S(2)}, u32[]{:S(2)}) collective-permute-start(bf16[192,128]{1,0:T(8,128)(2,1)S(1)} %get-tuple-element.15), channel_id=1, source_target_pairs={{128,0},{132,4},{136,8},{140,12},{144,16},{148,20},{152,24},{156,2... | collective-permute-start | bytes 147464 | tf_op jit(solution)/shard_map/ppermute | solution.py:25
  86.5 10.0 %collective-permute-start.6 = (bf16[192,128]{1,0:T(8,128)(2,1)S(1)}, bf16[192,128]{1,0:T(8,128)(2,1)S(1)}, u32[]{:S(2)}, u32[]{:S(2)}) collective-permute-start(bf16[192,128]{1,0:T(8,128)(2,1)S(1)} %get-tuple-element.16), channel_id=1, source_target_pairs={{256,0},{260,4},{264,8},{268,12},{272,16},{276,20},{280,24},{284,2... | collective-permute-start | bytes 147464 | tf_op jit(solution)/shard_map/ppermute | solution.py:25
  87.8 19.8 %collective-permute-start.7 = (bf16[192,128]{1,0:T(8,128)(2,1)S(1)}, bf16[192,128]{1,0:T(8,128)(2,1)S(1)}, u32[]{:S(2)}, u32[]{:S(2)}) collective-permute-start(bf16[192,128]{1,0:T(8,128)(2,1)S(1)} %get-tuple-element.17), channel_id=1, source_target_pairs={{512,0},{516,4},{520,8},{524,12},{528,16},{532,20},{536,24},{540,2... | collective-permute-start | bytes 147464 | tf_op jit(solution)/shard_map/ppermute | solution.py:25

commit v3 on v2

--- a/solution.py
+++ b/solution.py
@@ -23,6 +23,11 @@
     devices = range(lax.axis_size(axis))
     route = [(i - distance, i) for i in devices if i - distance in devices]
     return lax.ppermute(block, axis, route)
+
+
+def between(block, quarters, pairs):
+    route = [p for a, b in pairs for p in zip(quarters[a], quarters[b])]
+    return lax.ppermute(block, "z", route)
 
 
 def exchanged(tiles, axis):
@@ -52,13 +57,14 @@
     return jnp.transpose(x.astype(jnp.float32))
 
 
-def pack_kernel(k_ref, v_ref, out_ref):
-    out_ref[...] = turned(jnp.concatenate([k_ref[...], v_ref[...]], axis=0)).astype(out_ref.dtype)
+def pack_kernel(kv_ref, out_ref):
+    out_ref[...] = turned(kv_ref[...]).astype(out_ref.dtype)
 
 
 def pack(k, v):
-    shape = jax.ShapeDtypeStruct((k.shape[1], 2 * k.shape[0]), k.dtype)
-    return call(pack_kernel, 10**6, shape, k, v)
+    kv = jnp.concatenate([k, v], axis=0)
+    shape = jax.ShapeDtypeStruct(kv.shape[::-1], kv.dtype)
+    return call(pack_kernel, 10**10, shape, kv)
 
 
 def spread_kernel(rows, ys, cores, peers, x_ref, out_ref):
@@ -110,10 +116,14 @@
 
 
 def attention_kernel(distances, chosen_ref, q_ref, go_ref, ao_ref, lse_ref, kv_ref, *refs):
-    far_refs = refs[:LEVELS]
-    gq_ref, own_ref = refs[LEVELS : LEVELS + 2]
-    back_refs = refs[LEVELS + 2 : 2 * LEVELS + 2]
-    sums = refs[2 * LEVELS + 2]
+    one_ref, two_ref, traded_ref, fetched_ref, passed_ref = refs[: LEVELS + 1]
+    gq_ref, gq_too_ref, own_ref = refs[LEVELS + 1 : LEVELS + 4]
+    back_refs = refs[LEVELS + 4 : 2 * LEVELS + 4]
+    sums, four_ref = refs[2 * LEVELS + 4 :]
+    at, quarter = lax.axis_index("z"), lax.axis_size("z") // 4
+    in_second = jnp.logical_and(at >= quarter, at < 2 * quarter)
+    four_ref[...] = jnp.where(in_second, traded_ref[...], fetched_ref[...])
+    far_refs = (one_ref, two_ref, four_ref, passed_ref)
     blocks = q_ref.shape[0] // BLOCK
     heads = q_ref.shape[1] // DH
     me = lax.axis_index(KV)
@@ -154,16 +164,16 @@
         for pair in range(heads // 2):
             first = grad_q[2 * pair * BLOCK : (2 * pair + 1) * BLOCK]
             second = grad_q[(2 * pair + 1) * BLOCK : (2 * pair + 2) * BLOCK]
-            gq_ref[rows, pair * 2 * DH : (pair + 1) * 2 * DH] = jnp.where(
-                lane < DH, first, pltpu.roll(second, DH, 1)
-            ).astype(gq_ref.dtype)
+            both = jnp.where(lane < DH, first, pltpu.roll(second, DH, 1)).astype(gq_ref.dtype)
+            gq_ref[rows, pair * 2 * DH : (pair + 1) * 2 * DH] = both
+            gq_too_ref[rows, pair * 2 * DH : (pair + 1) * 2 * DH] = both
     for level in range(LEVELS):
         back_refs[level][...] = sums[level].astype(jnp.bfloat16)
 
 
 def attention(distances, chosen, q, go, ao, lse, kv, far):
     tokens, width = q.shape
-    shape = (jax.ShapeDtypeStruct((tokens, width), jnp.bfloat16),)
+    shape = (jax.ShapeDtypeStruct((tokens, width), jnp.bfloat16),) * 2
     shape += (jax.ShapeDtypeStruct(kv.shape, jnp.float32),)
     shape += (jax.ShapeDtypeStruct(kv.shape, jnp.bfloat16),) * LEVELS
     return call(
@@ -178,7 +188,7 @@
         kv,
         *far,
         smem=1,
-        scratch=[pltpu.VMEM((LEVELS, *kv.shape), jnp.float32)],
+        scratch=[pltpu.VMEM((LEVELS, *kv.shape), jnp.float32), pltpu.VMEM(kv.shape, kv.dtype)],
     )
 
 
@@ -238,16 +248,22 @@
     distances = [1, axis_size // 8, axis_size // 4, axis_size // 2]
     key_pair = pack(keys.T, values.T)
     far = []
-    for distance in distances:
+    for distance in distances[:2]:
         far.append(shifted(key_pair, KV, distance))
+    quarter = lax.axis_size("z") // 4
+    quarters = [range(n * quarter, (n + 1) * quarter) for n in range(4)]
+    traded = between(key_pair, quarters, ((0, 1), (1, 0)))
+    passed = between(traded, quarters, ((1, 2), (0, 3)))
+    fetched = between(key_pair, quarters, ((1, 2), (2, 3)))
+    far += [traded, fetched, passed]
     sent = spread(layer_input, out_rows, ys, cores, peers)
     whole_input = exchanged(sent, ("c", "x"))
-    grad_queries, own, *back = attention(
+    grad_queries, grads, own, *back = attention(
         distances, chosen.T, queries, grad_out, attn_out, log_sum.T, key_pair, far
     )
     route = [(i, cores - 1 - i) for i in range(cores)]
-    other = lax.ppermute(grad_queries, "c", route)
-    parts = weight(grad_queries, other, whole_input, ys)
+    other = lax.ppermute(grads, "c", route)
+    parts = weight(grads, other, whole_input, ys)
     over_y = exchanged(parts, "y")
     returned = []
     for level, distance in enumerate(distances):

time: 110 us -> 110 us (level)
    ppermute x8 -> x6, starting transfers between devices: 40.1 us -> 17.8 us  [shifted(): return lax.ppermute(block, axis, route)]
    ppermute x1 -> x4, starting transfers between devices: 5.17 us -> 19.2 us  [the longest x3 17 us: between(): return lax.ppermute(block, 'z', route)]
    all_to_all x2, starting transfers between devices: 10.5 us -> 19.2 us  [exchanged(): return lax.all_to_all(tiles, axis, split_axis=0, concat_axis=0, tiled=True)]
    ppermute x1 -> x4, waiting for transfers between devices: 1.13 us -> 2.8 us  [the longest x3 1.79 us: between(): return lax.ppermute(block, 'z', route)]
    ppermute x8 -> x6, waiting for transfers between devices: 19.6 us -> 18.5 us  [shifted(): return lax.ppermute(block, axis, route)]
  transfers between devices with their start and end apart: 11 -> 12, of which waited for: 5 -> 5; matrix products, arithmetic and copies ran while one was open for 0% -> 0% of each run, Pallas kernels for 4% -> 4%
where the time goes in v3:
time: 110 us
  starting transfers between devices  56.2 us (51%)
  blocking collectives  23.1 us (21%)
  waiting for transfers between devices  21.3 us (19%)
  Pallas kernels  7.28 us (7%)
    all_to_all x1, blocking collectives, exchanged(): return lax.all_to_all(tiles, axis, split_axis=0, concat_axis=0, tiled=True)  23.1 us
    all_to_all x2, starting transfers between devices, exchanged(): return lax.all_to_all(tiles, axis, split_axis=0, concat_axis=0, tiled=True)  19.2 us
    ppermute x6, waiting for transfers between devices, shifted(): return lax.ppermute(block, axis, route)  18.5 us
    ppermute x6, starting transfers between devices, shifted(): return lax.ppermute(block, axis, route)  17.8 us
    ppermute x3, starting transfers between devices, between(): return lax.ppermute(block, 'z', route)  17 us
    pallas_call x7, Pallas kernels, call(): pl.pallas_call(kernel, out_shape=out_shape, in_specs=[pl.BlockSpec(memory...  7.28 us
  transfers between devices with their start and end apart: 12, of which 5 were waited for; matrix products, arithmetic and copies ran while one was open for 0% of the time, Pallas kernels for 4%

profile of v3, /device:TPU:67, one launch (start us, length us, event | category | flops | bytes accessed | tf_op | source)
XLA Modules:
  0.0 109.7 jit_solution(11383105416934677920)
XLA Ops:
  0.6 0.9 copy-done
  1.6 1.2 %shard_map.114 = bf16[8,192,256]{2,1,0:T(8,128)(2,1)} custom-call(bf16[192,512]{1,0:T(8,128)(2,1)S(1)} %copy-done), custom_call_target="tpu_custom_call" | custom-call | flops 100663296 | bytes 196608 | tf_op jit(solution)/shard_map/pallas_call | solution.py:45
  2.8 5.2 %all-to-all-start = ((bf16[8,192,256]{2,1,0:T(8,128)(2,1)}), bf16[8,192,256]{2,1,0:T(8,128)(2,1)S(1)}, u32[]{:S(2)}, u32[]{:S(2)}) async-start(bf16[8,192,256]{2,1,0:T(8,128)(2,1)} %shard_map.114), calls=%async_computation | async-start | bytes 1572864 | tf_op jit(solution)/shard_map/all_to_all | solution.py:34
  8.1 0.0 copy-start.1
  8.1 0.0 copy-start.2
  8.1 0.0 copy-start.3
  8.1 0.0 copy-start.4
  8.1 0.0 copy-start.5
  8.1 0.1 shard_map.111.kv_ref
  8.2 10.8 %collective-permute-start.2 = (bf16[192,128]{1,0:T(8,128)(2,1)S(1)}, bf16[192,128]{1,0:T(8,128)(2,1)S(1)}, u32[]{:S(2)}, u32[]{:S(2)}) collective-permute-start(bf16[192,128]{1,0:T(8,128)(2,1)S(1)} %shard_map.111.kv_ref), channel_id=1, source_target_pairs={{0,256},{64,320},{128,384},{192,448},{256,0},{320,64},{384,128},{4... | collective-permute-start | bytes 147464 | tf_op jit(solution)/shard_map/ppermute | solution.py:30
  19.0 0.7 collective-permute-start.3
  19.7 5.8 %collective-permute-start.1 = (bf16[192,128]{1,0:T(8,128)(2,1)S(1)}, bf16[192,128]{1,0:T(8,128)(2,1)S(1)}, u32[]{:S(2)}, u32[]{:S(2)}) collective-permute-start(bf16[192,128]{1,0:T(8,128)(2,1)S(1)} %shard_map.111.kv_ref), channel_id=1, source_target_pairs={{0,128},{4,132},{8,136},{12,140},{16,144},{20,148},{24,152},{28,15... | collective-permute-start | bytes 147464 | tf_op jit(solution)/shard_map/ppermute | solution.py:25
  25.5 4.0 %collective-permute-start = (bf16[192,128]{1,0:T(8,128)(2,1)S(1)}, bf16[192,128]{1,0:T(8,128)(2,1)S(1)}, u32[]{:S(2)}, u32[]{:S(2)}) collective-permute-start(bf16[192,128]{1,0:T(8,128)(2,1)S(1)} %shard_map.111.kv_ref), channel_id=1, source_target_pairs={{0,4},{4,8},{8,12},{12,16},{16,20},{20,24},{24,28},{28,32},{32,36}... | collective-permute-start | bytes 147464 | tf_op jit(solution)/shard_map/ppermute | solution.py:25
  29.6 0.0 collective-permute-done.2.refs_2_
  29.6 5.6 %collective-permute-start.4 = (bf16[192,128]{1,0:T(8,128)(2,1)S(1)}, bf16[192,128]{1,0:T(8,128)(2,1)S(1)}, u32[]{:S(2)}, u32[]{:S(2)}) collective-permute-start(bf16[192,128]{1,0:T(8,128)(2,1)S(1)} %collective-permute-done.2.refs_2_), channel_id=1, source_target_pairs={{256,512},{320,576},{384,640},{448,704},{0,768},{64,832},{128,896}... | collective-permute-start | bytes 147464 | tf_op jit(solution)/shard_map/ppermute | solution.py:30
  35.2 1.8 %collective-permute-done.4.refs_4_ = bf16[192,128]{1,0:T(8,128)(2,1)S(1)} collective-permute-done((bf16[192,128]{1,0:T(8,128)(2,1)S(1)}, bf16[192,128]{1,0:T(8,128)(2,1)S(1)}, u32[]{:S(2)}, u32[]{:S(2)}) %collective-permute-start.4) | collective-permute-done | bytes 49184 | tf_op jit(solution)/shard_map/ppermute | solution.py:30
  37.0 3.4 %shard_map.112 = (bf16[192,256]{1,0:T(8,128)(2,1)}, bf16[192,256]{1,0:T(8,128)(2,1)S(1)}, f32[192,128]{1,0:T(8,128)S(1)}, bf16[192,128]{1,0:T(8,128)(2,1)S(1)}, ...) custom-call(s32[8,768]{1,0:T(8,128)S(1)} %bitcast.8, ...), custom_call_target="tpu_custom_call" | custom-call | flops 2000000000 | bytes 617472 | tf_op jit(solution)/shard_map/pallas_call | solution.py:45
  40.4 2.2 %collective-permute-start.9 = (bf16[192,256]{1,0:T(8,128)(2,1)S(1)}, bf16[192,256]{1,0:T(8,128)(2,1)S(1)}, u32[]{:S(2)}, u32[]{:S(2)}) collective-permute-start(bf16[192,256]{1,0:T(8,128)(2,1)S(1)} %get-tuple-element.21.mine_ref), channel_id=1, source_target_pairs={{0,4},{4,0},{1,5},{5,1},{2,6},{6,2},{3,7},{7,3},{8,12},{12,8},{9,1... | collective-permute-start | bytes 294920 | tf_op jit(solution)/shard_map/ppermute | solution.py:265
  42.6 1.0 collective-permute-done.9.other_ref
  43.6 0.5 shard_map.115
  44.1 23.1 %all_to_all.15 = bf16[8,128,256]{2,1,0:T(8,128)(2,1)S(1)} all-to-all(bf16[8,128,256]{2,1,0:T(8,128)(2,1)S(1)} %shard_map.115), channel_id=1, replica_groups=mesh['z'=16,'y'=8,'c'=2,'x'=4] {'y'}, dimensions={0} | all-to-all | bytes 1048576 | tf_op jit(solution)/shard_map/all_to_all | solution.py:34
  67.2 0.7 shard_map.116
  67.9 13.9 %all-to-all-start.2 = ((bf16[16,8,256]{2,1,0:T(8,128)(2,1)}), bf16[16,8,256]{2,1,0:T(8,128)(2,1)S(1)}, u32[]{:S(2)}, u32[]{:S(2)}) async-start(bf16[16,8,256]{2,1,0:T(8,128)(2,1)} %shard_map.116), calls=%async_computation.2 | async-start | bytes 131072 | tf_op jit(solution)/shard_map/all_to_all | solution.py:34
  81.8 4.1 %collective-permute-start.5 = (bf16[192,128]{1,0:T(8,128)(2,1)S(1)}, bf16[192,128]{1,0:T(8,128)(2,1)S(1)}, u32[]{:S(2)}, u32[]{:S(2)}) collective-permute-start(bf16[192,128]{1,0:T(8,128)(2,1)S(1)} %get-tuple-element.15), channel_id=1, source_target_pairs={{4,0},{8,4},{12,8},{16,12},{20,16},{24,20},{28,24},{32,28},{36,32}... | collective-permute-start | bytes 147464 | tf_op jit(solution)/shard_map/ppermute | solution.py:25
  85.9 1.3 %collective-permute-start.6 = (bf16[192,128]{1,0:T(8,128)(2,1)S(1)}, bf16[192,128]{1,0:T(8,128)(2,1)S(1)}, u32[]{:S(2)}, u32[]{:S(2)}) collective-permute-start(bf16[192,128]{1,0:T(8,128)(2,1)S(1)} %get-tuple-element.16), channel_id=1, source_target_pairs={{128,0},{132,4},{136,8},{140,12},{144,16},{148,20},{152,24},{156,2... | collective-permute-start | bytes 147464 | tf_op jit(solution)/shard_map/ppermute | solution.py:25
  87.2 1.3 %collective-permute-start.7 = (bf16[192,128]{1,0:T(8,128)(2,1)S(1)}, bf16[192,128]{1,0:T(8,128)(2,1)S(1)}, u32[]{:S(2)}, u32[]{:S(2)}) collective-permute-start(bf16[192,128]{1,0:T(8,128)(2,1)S(1)} %get-tuple-element.17), channel_id=1, source_target_pairs={{256,0},{260,4},{264,8},{268,12},{272,16},{276,20},{280,24},{284,2... | collective-permute-start | bytes 147464 | tf_op jit(solution)/shard_map/ppermute | solution.py:25
  88.5 1.3 %collective-permute-start.8 = (bf16[192,128]{1,0:T(8,128)(2,1)S(1)}, bf16[192,128]{1,0:T(8,128)(2,1)S(1)}, u32[]{:S(2)}, u32[]{:S(2)}) collective-permute-start(bf16[192,128]{1,0:T(8,128)(2,1)S(1)} %get-tuple-element.18), channel_id=1, source_target_pairs={{512,0},{516,4},{520,8},{524,12},{528,16},{532,20},{536,24},{540,2... | collective-permute-start | bytes 147464 | tf_op jit(solution)/shard_map/ppermute | solution.py:25
  89.8 2.6 %collective-permute-done.6.refs_1_ = bf16[192,128]{1,0:T(8,128)(2,1)S(1)} collective-permute-done((bf16[192,128]{1,0:T(8,128)(2,1)S(1)}, bf16[192,128]{1,0:T(8,128)(2,1)S(1)}, u32[]{:S(2)}, u32[]{:S(2)}) %collective-permute-start.6) | collective-permute-done | bytes 49184 | tf_op jit(solution)/shard_map/ppermute | solution.py:25
  92.4 4.9 %collective-permute-done.7.refs_2_ = bf16[192,128]{1,0:T(8,128)(2,1)S(1)} collective-permute-done((bf16[192,128]{1,0:T(8,128)(2,1)S(1)}, bf16[192,128]{1,0:T(8,128)(2,1)S(1)}, u32[]{:S(2)}, u32[]{:S(2)}) %collective-permute-start.7) | collective-permute-done | bytes 49184 | tf_op jit(solution)/shard_map/ppermute | solution.py:25
  97.3 11.1 %collective-permute-done.8.refs_3_ = bf16[192,128]{1,0:T(8,128)(2,1)S(1)} collective-permute-done((bf16[192,128]{1,0:T(8,128)(2,1)S(1)}, bf16[192,128]{1,0:T(8,128)(2,1)S(1)}, u32[]{:S(2)}, u32[]{:S(2)}) %collective-permute-start.8) | collective-permute-done | bytes 49184 | tf_op jit(solution)/shard_map/ppermute | solution.py:25
  108.3 0.7 shard_map.113
  109.1 0.6 shard_map.117
  (17 shorter events, 0.0 us)
Async XLA Ops:
  0.6 0.9 copy-start
  2.8 5.3 %copy-start.6 = (bf16[192,64]{0,1:T(8,128)(2,1)S(1)}, bf16[192,64]{0,1:T(8,128)(2,1)}, u32[]{:S(2)}) copy-start(bf16[192,64]{0,1:T(8,128)(2,1)} %param.11) | copy-start | bytes 73732
  2.8 5.3 %copy-start.7 = (bf16[192,64]{0,1:T(8,128)(2,1)S(1)}, bf16[192,64]{0,1:T(8,128)(2,1)}, u32[]{:S(2)}) copy-start(bf16[192,64]{0,1:T(8,128)(2,1)} %param.10) | copy-start | bytes 73732
  2.8 40.8 %all-to-all-start = ((bf16[8,192,256]{2,1,0:T(8,128)(2,1)}), bf16[8,192,256]{2,1,0:T(8,128)(2,1)S(1)}, u32[]{:S(2)}, u32[]{:S(2)}) async-start(bf16[8,192,256]{2,1,0:T(8,128)(2,1)} %shard_map.114), calls=%async_computation | async-start | bytes 1572864 | tf_op jit(solution)/shard_map/all_to_all | solution.py:34
  8.1 28.9 %copy-start.1 = (bf16[192,256]{1,0:T(8,128)(2,1)S(1)}, bf16[192,256]{1,0:T(8,128)(2,1)}, u32[]{:S(2)}) copy-start(bf16[192,256]{1,0:T(8,128)(2,1)} %q_ref.1) | copy-start | bytes 294916
  8.1 28.9 %copy-start.2 = (bf16[192,256]{1,0:T(8,128)(2,1)S(1)}, bf16[192,256]{1,0:T(8,128)(2,1)}, u32[]{:S(2)}) copy-start(bf16[192,256]{1,0:T(8,128)(2,1)} %go_ref.1) | copy-start | bytes 294916
  8.1 28.9 %copy-start.3 = (bf16[192,256]{1,0:T(8,128)(2,1)S(1)}, bf16[192,256]{1,0:T(8,128)(2,1)}, u32[]{:S(2)}) copy-start(bf16[192,256]{1,0:T(8,128)(2,1)} %ao_ref.1) | copy-start | bytes 294916
  8.1 28.9 %copy-start.4 = (s32[768,8]{0,1:T(8,128)S(1)}, s32[768,8]{0,1:T(8,128)}, u32[]{:S(2)}) copy-start(s32[768,8]{0,1:T(8,128)} %param.15) | copy-start | bytes 73732
  8.1 28.9 %copy-start.5 = (f32[192,4]{0,1:T(4,128)S(1)}, f32[192,4]{0,1:T(4,128)}, u32[]{:S(2)}) copy-start(f32[192,4]{0,1:T(4,128)} %param.14) | copy-start | bytes 9220
  8.2 21.3 %collective-permute-start.2 = (bf16[192,128]{1,0:T(8,128)(2,1)S(1)}, bf16[192,128]{1,0:T(8,128)(2,1)S(1)}, u32[]{:S(2)}, u32[]{:S(2)}) collective-permute-start(bf16[192,128]{1,0:T(8,128)(2,1)S(1)} %shard_map.111.kv_ref), channel_id=1, source_target_pairs={{0,256},{64,320},{128,384},{192,448},{256,0},{320,64},{384,128},{4... | collective-permute-start | bytes 147464 | tf_op jit(solution)/shard_map/ppermute | solution.py:30
  19.0 16.2 %collective-permute-start.3 = (bf16[192,128]{1,0:T(8,128)(2,1)S(1)}, bf16[192,128]{1,0:T(8,128)(2,1)S(1)}, u32[]{:S(2)}, u32[]{:S(2)}) collective-permute-start(bf16[192,128]{1,0:T(8,128)(2,1)S(1)} %shard_map.111.kv_ref), channel_id=1, source_target_pairs={{256,512},{320,576},{384,640},{448,704},{512,768},{576,832},{640,8... | collective-permute-start | bytes 147464 | tf_op jit(solution)/shard_map/ppermute | solution.py:30
  19.7 15.5 %collective-permute-start.1 = (bf16[192,128]{1,0:T(8,128)(2,1)S(1)}, bf16[192,128]{1,0:T(8,128)(2,1)S(1)}, u32[]{:S(2)}, u32[]{:S(2)}) collective-permute-start(bf16[192,128]{1,0:T(8,128)(2,1)S(1)} %shard_map.111.kv_ref), channel_id=1, source_target_pairs={{0,128},{4,132},{8,136},{12,140},{16,144},{20,148},{24,152},{28,15... | collective-permute-start | bytes 147464 | tf_op jit(solution)/shard_map/ppermute | solution.py:25
  25.5 9.7 %collective-permute-start = (bf16[192,128]{1,0:T(8,128)(2,1)S(1)}, bf16[192,128]{1,0:T(8,128)(2,1)S(1)}, u32[]{:S(2)}, u32[]{:S(2)}) collective-permute-start(bf16[192,128]{1,0:T(8,128)(2,1)S(1)} %shard_map.111.kv_ref), channel_id=1, source_target_pairs={{0,4},{4,8},{8,12},{12,16},{16,20},{20,24},{24,28},{28,32},{32,36}... | collective-permute-start | bytes 147464 | tf_op jit(solution)/shard_map/ppermute | solution.py:25
  29.6 7.4 %collective-permute-start.4 = (bf16[192,128]{1,0:T(8,128)(2,1)S(1)}, bf16[192,128]{1,0:T(8,128)(2,1)S(1)}, u32[]{:S(2)}, u32[]{:S(2)}) collective-permute-start(bf16[192,128]{1,0:T(8,128)(2,1)S(1)} %collective-permute-done.2.refs_2_), channel_id=1, source_target_pairs={{256,512},{320,576},{384,640},{448,704},{0,768},{64,832},{128,896}... | collective-permute-start | bytes 147464 | tf_op jit(solution)/shard_map/ppermute | solution.py:30
  40.4 3.2 %collective-permute-start.9 = (bf16[192,256]{1,0:T(8,128)(2,1)S(1)}, bf16[192,256]{1,0:T(8,128)(2,1)S(1)}, u32[]{:S(2)}, u32[]{:S(2)}) collective-permute-start(bf16[192,256]{1,0:T(8,128)(2,1)S(1)} %get-tuple-element.21.mine_ref), channel_id=1, source_target_pairs={{0,4},{4,0},{1,5},{5,1},{2,6},{6,2},{3,7},{7,3},{8,12},{12,8},{9,1... | collective-permute-start | bytes 294920 | tf_op jit(solution)/shard_map/ppermute | solution.py:265
  67.9 41.2 %all-to-all-start.2 = ((bf16[16,8,256]{2,1,0:T(8,128)(2,1)}), bf16[16,8,256]{2,1,0:T(8,128)(2,1)S(1)}, u32[]{:S(2)}, u32[]{:S(2)}) async-start(bf16[16,8,256]{2,1,0:T(8,128)(2,1)} %shard_map.116), calls=%async_computation.2 | async-start | bytes 131072 | tf_op jit(solution)/shard_map/all_to_all | solution.py:34
  81.8 8.0 %collective-permute-start.5 = (bf16[192,128]{1,0:T(8,128)(2,1)S(1)}, bf16[192,128]{1,0:T(8,128)(2,1)S(1)}, u32[]{:S(2)}, u32[]{:S(2)}) collective-permute-start(bf16[192,128]{1,0:T(8,128)(2,1)S(1)} %get-tuple-element.15), channel_id=1, source_target_pairs={{4,0},{8,4},{12,8},{16,12},{20,16},{24,20},{28,24},{32,28},{36,32}... | collective-permute-start | bytes 147464 | tf_op jit(solution)/shard_map/ppermute | solution.py:25
  85.9 6.5 %collective-permute-start.6 = (bf16[192,128]{1,0:T(8,128)(2,1)S(1)}, bf16[192,128]{1,0:T(8,128)(2,1)S(1)}, u32[]{:S(2)}, u32[]{:S(2)}) collective-permute-start(bf16[192,128]{1,0:T(8,128)(2,1)S(1)} %get-tuple-element.16), channel_id=1, source_target_pairs={{128,0},{132,4},{136,8},{140,12},{144,16},{148,20},{152,24},{156,2... | collective-permute-start | bytes 147464 | tf_op jit(solution)/shard_map/ppermute | solution.py:25
  87.2 10.1 %collective-permute-start.7 = (bf16[192,128]{1,0:T(8,128)(2,1)S(1)}, bf16[192,128]{1,0:T(8,128)(2,1)S(1)}, u32[]{:S(2)}, u32[]{:S(2)}) collective-permute-start(bf16[192,128]{1,0:T(8,128)(2,1)S(1)} %get-tuple-element.17), channel_id=1, source_target_pairs={{256,0},{260,4},{264,8},{268,12},{272,16},{276,20},{280,24},{284,2... | collective-permute-start | bytes 147464 | tf_op jit(solution)/shard_map/ppermute | solution.py:25
  88.5 19.8 %collective-permute-start.8 = (bf16[192,128]{1,0:T(8,128)(2,1)S(1)}, bf16[192,128]{1,0:T(8,128)(2,1)S(1)}, u32[]{:S(2)}, u32[]{:S(2)}) collective-permute-start(bf16[192,128]{1,0:T(8,128)(2,1)S(1)} %get-tuple-element.18), channel_id=1, source_target_pairs={{512,0},{516,4},{520,8},{524,12},{528,16},{532,20},{536,24},{540,2... | collective-permute-start | bytes 147464 | tf_op jit(solution)/shard_map/ppermute | solution.py:25

commit v4 on v3

--- a/solution.py
+++ b/solution.py
@@ -16,6 +16,7 @@
 KV = ("z", "y", "c")
 NT = (((1,), (1,)), ((), ()))
 TN = (((0,), (0,)), ((), ()))
+Y_ORDERS = ((4, 5, 6, 7, 0, 1, 2, 3), (3, 2, 1, 0, 7, 6, 5, 4))
 VMEM_LIMIT = 16 * 2**20
 
 
@@ -30,8 +31,10 @@
     return lax.ppermute(block, "z", route)
 
 
-def exchanged(tiles, axis):
-    return lax.all_to_all(tiles, axis, split_axis=0, concat_axis=0, tiled=True)
+def exchanged(tiles, axis, groups=None):
+    return lax.all_to_all(
+        tiles, axis, split_axis=0, concat_axis=0, tiled=True, axis_index_groups=groups
+    )
 
 
 def dot(a, b, dims=(((1,), (0,)), ((), ()))):
@@ -204,7 +207,8 @@
         part = dot(x, grads, TN).astype(out_ref.dtype)
         step = part.shape[0] // ys
         for y in range(ys):
-            out_ref[y, peer * step : (peer + 1) * step] = part[y * step : (y + 1) * step]
+            slot = jnp.where(core == 0, *(order.index(y) for order in Y_ORDERS))
+            out_ref[slot, peer * step : (peer + 1) * step] = part[y * step : (y + 1) * step]
 
 
 def weight(mine, other, x, ys):
@@ -264,7 +268,8 @@
     route = [(i, cores - 1 - i) for i in range(cores)]
     other = lax.ppermute(grads, "c", route)
     parts = weight(grads, other, whole_input, ys)
-    over_y = exchanged(parts, "y")
+    groups = [[y * cores + c for y in order] for c, order in enumerate(Y_ORDERS)]
+    over_y = exchanged(parts, ("y", "c"), groups)
     returned = []
     for level, distance in enumerate(distances):
         returned.append(shifted(back[level], KV, -distance))

time: 110 us -> 107 us (0.973)
  blocking collectives: 23.1 us -> 20.2 us
    all_to_all x1, blocking collectives: 23.1 us -> 20.2 us  [exchanged(): lax.all_to_all(tiles, axis, split_axis=0, concat_axis=0, tiled=True, axis...]
where the time goes in v4:
time: 107 us
  starting transfers between devices  56.1 us (52%)
  waiting for transfers between devices  21.3 us (20%)
  blocking collectives  20.2 us (19%)
  Pallas kernels  7.28 us (7%)
    all_to_all x1, blocking collectives, exchanged(): lax.all_to_all(tiles, axis, split_axis=0, concat_axis=0, tiled=True, axis...  20.2 us
    all_to_all x2, starting transfers between devices, exchanged(): lax.all_to_all(tiles, axis, split_axis=0, concat_axis=0, tiled=True, axis...  19.2 us
    ppermute x6, waiting for transfers between devices, shifted(): return lax.ppermute(block, axis, route)  18.5 us
    ppermute x6, starting transfers between devices, shifted(): return lax.ppermute(block, axis, route)  17.7 us
    ppermute x3, starting transfers between devices, between(): return lax.ppermute(block, 'z', route)  17 us
    pallas_call x7, Pallas kernels, call(): pl.pallas_call(kernel, out_shape=out_shape, in_specs=[pl.BlockSpec(memory...  7.28 us
    ppermute x1, starting transfers between devices, shards(): other = lax.ppermute(grads, 'c', route)  2.16 us
  transfers between devices with their start and end apart: 12, of which 5 were waited for; matrix products, arithmetic and copies ran while one was open for 0% of the time, Pallas kernels for 4%

profile of v4, /device:TPU:67, one launch (start us, length us, event | category | flops | bytes accessed | tf_op | source)
XLA Modules:
  0.0 106.7 jit_solution(10525340884976352835)
XLA Ops:
  0.6 0.9 copy-done
  1.6 1.2 %shard_map.114 = bf16[8,192,256]{2,1,0:T(8,128)(2,1)} custom-call(bf16[192,512]{1,0:T(8,128)(2,1)S(1)} %copy-done), custom_call_target="tpu_custom_call" | custom-call | flops 100663296 | bytes 196608 | tf_op jit(solution)/shard_map/pallas_call | solution.py:48
  2.8 5.2 %all-to-all-start = ((bf16[8,192,256]{2,1,0:T(8,128)(2,1)}), bf16[8,192,256]{2,1,0:T(8,128)(2,1)S(1)}, u32[]{:S(2)}, u32[]{:S(2)}) async-start(bf16[8,192,256]{2,1,0:T(8,128)(2,1)} %shard_map.114), calls=%async_computation | async-start | bytes 1572864 | tf_op jit(solution)/shard_map/all_to_all | solution.py:35
  8.1 0.0 copy-start.1
  8.1 0.0 copy-start.2
  8.1 0.0 copy-start.3
  8.1 0.0 copy-start.4
  8.1 0.0 copy-start.5
  8.1 0.1 shard_map.111.kv_ref
  8.2 10.8 %collective-permute-start.2 = (bf16[192,128]{1,0:T(8,128)(2,1)S(1)}, bf16[192,128]{1,0:T(8,128)(2,1)S(1)}, u32[]{:S(2)}, u32[]{:S(2)}) collective-permute-start(bf16[192,128]{1,0:T(8,128)(2,1)S(1)} %shard_map.111.kv_ref), channel_id=1, source_target_pairs={{0,256},{64,320},{128,384},{192,448},{256,0},{320,64},{384,128},{4... | collective-permute-start | bytes 147464 | tf_op jit(solution)/shard_map/ppermute | solution.py:31
  19.0 0.7 collective-permute-start.3
  19.7 5.8 %collective-permute-start.1 = (bf16[192,128]{1,0:T(8,128)(2,1)S(1)}, bf16[192,128]{1,0:T(8,128)(2,1)S(1)}, u32[]{:S(2)}, u32[]{:S(2)}) collective-permute-start(bf16[192,128]{1,0:T(8,128)(2,1)S(1)} %shard_map.111.kv_ref), channel_id=1, source_target_pairs={{0,128},{4,132},{8,136},{12,140},{16,144},{20,148},{24,152},{28,15... | collective-permute-start | bytes 147464 | tf_op jit(solution)/shard_map/ppermute | solution.py:26
  25.5 4.0 %collective-permute-start = (bf16[192,128]{1,0:T(8,128)(2,1)S(1)}, bf16[192,128]{1,0:T(8,128)(2,1)S(1)}, u32[]{:S(2)}, u32[]{:S(2)}) collective-permute-start(bf16[192,128]{1,0:T(8,128)(2,1)S(1)} %shard_map.111.kv_ref), channel_id=1, source_target_pairs={{0,4},{4,8},{8,12},{12,16},{16,20},{20,24},{24,28},{28,32},{32,36}... | collective-permute-start | bytes 147464 | tf_op jit(solution)/shard_map/ppermute | solution.py:26
  29.6 0.0 collective-permute-done.2.refs_2_
  29.6 5.6 %collective-permute-start.4 = (bf16[192,128]{1,0:T(8,128)(2,1)S(1)}, bf16[192,128]{1,0:T(8,128)(2,1)S(1)}, u32[]{:S(2)}, u32[]{:S(2)}) collective-permute-start(bf16[192,128]{1,0:T(8,128)(2,1)S(1)} %collective-permute-done.2.refs_2_), channel_id=1, source_target_pairs={{256,512},{320,576},{384,640},{448,704},{0,768},{64,832},{128,896}... | collective-permute-start | bytes 147464 | tf_op jit(solution)/shard_map/ppermute | solution.py:31
  35.2 1.8 %collective-permute-done.4.refs_4_ = bf16[192,128]{1,0:T(8,128)(2,1)S(1)} collective-permute-done((bf16[192,128]{1,0:T(8,128)(2,1)S(1)}, bf16[192,128]{1,0:T(8,128)(2,1)S(1)}, u32[]{:S(2)}, u32[]{:S(2)}) %collective-permute-start.4) | collective-permute-done | bytes 49184 | tf_op jit(solution)/shard_map/ppermute | solution.py:31
  37.0 3.4 %shard_map.112 = (bf16[192,256]{1,0:T(8,128)(2,1)}, bf16[192,256]{1,0:T(8,128)(2,1)S(1)}, f32[192,128]{1,0:T(8,128)S(1)}, bf16[192,128]{1,0:T(8,128)(2,1)S(1)}, ...) custom-call(s32[8,768]{1,0:T(8,128)S(1)} %bitcast.8, ...), custom_call_target="tpu_custom_call" | custom-call | flops 2000000000 | bytes 617472 | tf_op jit(solution)/shard_map/pallas_call | solution.py:48
  40.4 2.2 %collective-permute-start.9 = (bf16[192,256]{1,0:T(8,128)(2,1)S(1)}, bf16[192,256]{1,0:T(8,128)(2,1)S(1)}, u32[]{:S(2)}, u32[]{:S(2)}) collective-permute-start(bf16[192,256]{1,0:T(8,128)(2,1)S(1)} %get-tuple-element.21.mine_ref), channel_id=1, source_target_pairs={{0,4},{4,0},{1,5},{5,1},{2,6},{6,2},{3,7},{7,3},{8,12},{12,8},{9,1... | collective-permute-start | bytes 294920 | tf_op jit(solution)/shard_map/ppermute | solution.py:269
  42.6 1.0 collective-permute-done.9.other_ref
  43.6 0.5 shard_map.115
  44.1 20.2 %all_to_all.15 = bf16[8,128,256]{2,1,0:T(8,128)(2,1)S(1)} all-to-all(bf16[8,128,256]{2,1,0:T(8,128)(2,1)S(1)} %shard_map.115), channel_id=1, replica_groups={{32,40,48,56,0,8,16,24},{28,20,12,4,60,52,44,36},{33,41,49,57,1,9,17,25..., dimensions={0} | all-to-all | bytes 1048576 | tf_op jit(solution)/shard_map/all_to_all | solution.py:35
  64.3 0.7 shard_map.116
  65.0 13.9 %all-to-all-start.2 = ((bf16[16,8,256]{2,1,0:T(8,128)(2,1)}), bf16[16,8,256]{2,1,0:T(8,128)(2,1)S(1)}, u32[]{:S(2)}, u32[]{:S(2)}) async-start(bf16[16,8,256]{2,1,0:T(8,128)(2,1)} %shard_map.116), calls=%async_computation.2 | async-start | bytes 131072 | tf_op jit(solution)/shard_map/all_to_all | solution.py:35
  78.9 4.0 %collective-permute-start.5 = (bf16[192,128]{1,0:T(8,128)(2,1)S(1)}, bf16[192,128]{1,0:T(8,128)(2,1)S(1)}, u32[]{:S(2)}, u32[]{:S(2)}) collective-permute-start(bf16[192,128]{1,0:T(8,128)(2,1)S(1)} %get-tuple-element.15), channel_id=1, source_target_pairs={{4,0},{8,4},{12,8},{16,12},{20,16},{24,20},{28,24},{32,28},{36,32}... | collective-permute-start | bytes 147464 | tf_op jit(solution)/shard_map/ppermute | solution.py:26
  82.9 1.3 %collective-permute-start.6 = (bf16[192,128]{1,0:T(8,128)(2,1)S(1)}, bf16[192,128]{1,0:T(8,128)(2,1)S(1)}, u32[]{:S(2)}, u32[]{:S(2)}) collective-permute-start(bf16[192,128]{1,0:T(8,128)(2,1)S(1)} %get-tuple-element.16), channel_id=1, source_target_pairs={{128,0},{132,4},{136,8},{140,12},{144,16},{148,20},{152,24},{156,2... | collective-permute-start | bytes 147464 | tf_op jit(solution)/shard_map/ppermute | solution.py:26
  84.2 1.3 %collective-permute-start.7 = (bf16[192,128]{1,0:T(8,128)(2,1)S(1)}, bf16[192,128]{1,0:T(8,128)(2,1)S(1)}, u32[]{:S(2)}, u32[]{:S(2)}) collective-permute-start(bf16[192,128]{1,0:T(8,128)(2,1)S(1)} %get-tuple-element.17), channel_id=1, source_target_pairs={{256,0},{260,4},{264,8},{268,12},{272,16},{276,20},{280,24},{284,2... | collective-permute-start | bytes 147464 | tf_op jit(solution)/shard_map/ppermute | solution.py:26
  85.5 1.3 %collective-permute-start.8 = (bf16[192,128]{1,0:T(8,128)(2,1)S(1)}, bf16[192,128]{1,0:T(8,128)(2,1)S(1)}, u32[]{:S(2)}, u32[]{:S(2)}) collective-permute-start(bf16[192,128]{1,0:T(8,128)(2,1)S(1)} %get-tuple-element.18), channel_id=1, source_target_pairs={{512,0},{516,4},{520,8},{524,12},{528,16},{532,20},{536,24},{540,2... | collective-permute-start | bytes 147464 | tf_op jit(solution)/shard_map/ppermute | solution.py:26
  86.8 2.5 %collective-permute-done.6.refs_1_ = bf16[192,128]{1,0:T(8,128)(2,1)S(1)} collective-permute-done((bf16[192,128]{1,0:T(8,128)(2,1)S(1)}, bf16[192,128]{1,0:T(8,128)(2,1)S(1)}, u32[]{:S(2)}, u32[]{:S(2)}) %collective-permute-start.6) | collective-permute-done | bytes 49184 | tf_op jit(solution)/shard_map/ppermute | solution.py:26
  89.3 4.9 %collective-permute-done.7.refs_2_ = bf16[192,128]{1,0:T(8,128)(2,1)S(1)} collective-permute-done((bf16[192,128]{1,0:T(8,128)(2,1)S(1)}, bf16[192,128]{1,0:T(8,128)(2,1)S(1)}, u32[]{:S(2)}, u32[]{:S(2)}) %collective-permute-start.7) | collective-permute-done | bytes 49184 | tf_op jit(solution)/shard_map/ppermute | solution.py:26
  94.3 11.1 %collective-permute-done.8.refs_3_ = bf16[192,128]{1,0:T(8,128)(2,1)S(1)} collective-permute-done((bf16[192,128]{1,0:T(8,128)(2,1)S(1)}, bf16[192,128]{1,0:T(8,128)(2,1)S(1)}, u32[]{:S(2)}, u32[]{:S(2)}) %collective-permute-start.8) | collective-permute-done | bytes 49184 | tf_op jit(solution)/shard_map/ppermute | solution.py:26
  105.4 0.7 shard_map.113
  106.1 0.6 shard_map.117
  (17 shorter events, 0.0 us)
Async XLA Ops:
  0.6 0.9 copy-start
  2.8 5.3 %copy-start.6 = (bf16[192,64]{0,1:T(8,128)(2,1)S(1)}, bf16[192,64]{0,1:T(8,128)(2,1)}, u32[]{:S(2)}) copy-start(bf16[192,64]{0,1:T(8,128)(2,1)} %param.11) | copy-start | bytes 73732
  2.8 5.3 %copy-start.7 = (bf16[192,64]{0,1:T(8,128)(2,1)S(1)}, bf16[192,64]{0,1:T(8,128)(2,1)}, u32[]{:S(2)}) copy-start(bf16[192,64]{0,1:T(8,128)(2,1)} %param.10) | copy-start | bytes 73732
  2.8 40.8 %all-to-all-start = ((bf16[8,192,256]{2,1,0:T(8,128)(2,1)}), bf16[8,192,256]{2,1,0:T(8,128)(2,1)S(1)}, u32[]{:S(2)}, u32[]{:S(2)}) async-start(bf16[8,192,256]{2,1,0:T(8,128)(2,1)} %shard_map.114), calls=%async_computation | async-start | bytes 1572864 | tf_op jit(solution)/shard_map/all_to_all | solution.py:35
  8.1 28.9 %copy-start.1 = (bf16[192,256]{1,0:T(8,128)(2,1)S(1)}, bf16[192,256]{1,0:T(8,128)(2,1)}, u32[]{:S(2)}) copy-start(bf16[192,256]{1,0:T(8,128)(2,1)} %q_ref.1) | copy-start | bytes 294916
  8.1 28.9 %copy-start.2 = (bf16[192,256]{1,0:T(8,128)(2,1)S(1)}, bf16[192,256]{1,0:T(8,128)(2,1)}, u32[]{:S(2)}) copy-start(bf16[192,256]{1,0:T(8,128)(2,1)} %go_ref.1) | copy-start | bytes 294916
  8.1 28.9 %copy-start.3 = (bf16[192,256]{1,0:T(8,128)(2,1)S(1)}, bf16[192,256]{1,0:T(8,128)(2,1)}, u32[]{:S(2)}) copy-start(bf16[192,256]{1,0:T(8,128)(2,1)} %ao_ref.1) | copy-start | bytes 294916
  8.1 28.9 %copy-start.4 = (s32[768,8]{0,1:T(8,128)S(1)}, s32[768,8]{0,1:T(8,128)}, u32[]{:S(2)}) copy-start(s32[768,8]{0,1:T(8,128)} %param.15) | copy-start | bytes 73732
  8.1 28.9 %copy-start.5 = (f32[192,4]{0,1:T(4,128)S(1)}, f32[192,4]{0,1:T(4,128)}, u32[]{:S(2)}) copy-start(f32[192,4]{0,1:T(4,128)} %param.14) | copy-start | bytes 9220
  8.2 21.3 %collective-permute-start.2 = (bf16[192,128]{1,0:T(8,128)(2,1)S(1)}, bf16[192,128]{1,0:T(8,128)(2,1)S(1)}, u32[]{:S(2)}, u32[]{:S(2)}) collective-permute-start(bf16[192,128]{1,0:T(8,128)(2,1)S(1)} %shard_map.111.kv_ref), channel_id=1, source_target_pairs={{0,256},{64,320},{128,384},{192,448},{256,0},{320,64},{384,128},{4... | collective-permute-start | bytes 147464 | tf_op jit(solution)/shard_map/ppermute | solution.py:31
  19.0 16.2 %collective-permute-start.3 = (bf16[192,128]{1,0:T(8,128)(2,1)S(1)}, bf16[192,128]{1,0:T(8,128)(2,1)S(1)}, u32[]{:S(2)}, u32[]{:S(2)}) collective-permute-start(bf16[192,128]{1,0:T(8,128)(2,1)S(1)} %shard_map.111.kv_ref), channel_id=1, source_target_pairs={{256,512},{320,576},{384,640},{448,704},{512,768},{576,832},{640,8... | collective-permute-start | bytes 147464 | tf_op jit(solution)/shard_map/ppermute | solution.py:31
  19.7 15.5 %collective-permute-start.1 = (bf16[192,128]{1,0:T(8,128)(2,1)S(1)}, bf16[192,128]{1,0:T(8,128)(2,1)S(1)}, u32[]{:S(2)}, u32[]{:S(2)}) collective-permute-start(bf16[192,128]{1,0:T(8,128)(2,1)S(1)} %shard_map.111.kv_ref), channel_id=1, source_target_pairs={{0,128},{4,132},{8,136},{12,140},{16,144},{20,148},{24,152},{28,15... | collective-permute-start | bytes 147464 | tf_op jit(solution)/shard_map/ppermute | solution.py:26
  25.5 9.7 %collective-permute-start = (bf16[192,128]{1,0:T(8,128)(2,1)S(1)}, bf16[192,128]{1,0:T(8,128)(2,1)S(1)}, u32[]{:S(2)}, u32[]{:S(2)}) collective-permute-start(bf16[192,128]{1,0:T(8,128)(2,1)S(1)} %shard_map.111.kv_ref), channel_id=1, source_target_pairs={{0,4},{4,8},{8,12},{12,16},{16,20},{20,24},{24,28},{28,32},{32,36}... | collective-permute-start | bytes 147464 | tf_op jit(solution)/shard_map/ppermute | solution.py:26
  29.6 7.4 %collective-permute-start.4 = (bf16[192,128]{1,0:T(8,128)(2,1)S(1)}, bf16[192,128]{1,0:T(8,128)(2,1)S(1)}, u32[]{:S(2)}, u32[]{:S(2)}) collective-permute-start(bf16[192,128]{1,0:T(8,128)(2,1)S(1)} %collective-permute-done.2.refs_2_), channel_id=1, source_target_pairs={{256,512},{320,576},{384,640},{448,704},{0,768},{64,832},{128,896}... | collective-permute-start | bytes 147464 | tf_op jit(solution)/shard_map/ppermute | solution.py:31
  40.4 3.2 %collective-permute-start.9 = (bf16[192,256]{1,0:T(8,128)(2,1)S(1)}, bf16[192,256]{1,0:T(8,128)(2,1)S(1)}, u32[]{:S(2)}, u32[]{:S(2)}) collective-permute-start(bf16[192,256]{1,0:T(8,128)(2,1)S(1)} %get-tuple-element.21.mine_ref), channel_id=1, source_target_pairs={{0,4},{4,0},{1,5},{5,1},{2,6},{6,2},{3,7},{7,3},{8,12},{12,8},{9,1... | collective-permute-start | bytes 294920 | tf_op jit(solution)/shard_map/ppermute | solution.py:269
  65.0 41.1 %all-to-all-start.2 = ((bf16[16,8,256]{2,1,0:T(8,128)(2,1)}), bf16[16,8,256]{2,1,0:T(8,128)(2,1)S(1)}, u32[]{:S(2)}, u32[]{:S(2)}) async-start(bf16[16,8,256]{2,1,0:T(8,128)(2,1)} %shard_map.116), calls=%async_computation.2 | async-start | bytes 131072 | tf_op jit(solution)/shard_map/all_to_all | solution.py:35
  78.9 7.9 %collective-permute-start.5 = (bf16[192,128]{1,0:T(8,128)(2,1)S(1)}, bf16[192,128]{1,0:T(8,128)(2,1)S(1)}, u32[]{:S(2)}, u32[]{:S(2)}) collective-permute-start(bf16[192,128]{1,0:T(8,128)(2,1)S(1)} %get-tuple-element.15), channel_id=1, source_target_pairs={{4,0},{8,4},{12,8},{16,12},{20,16},{24,20},{28,24},{32,28},{36,32}... | collective-permute-start | bytes 147464 | tf_op jit(solution)/shard_map/ppermute | solution.py:26
  82.9 6.4 %collective-permute-start.6 = (bf16[192,128]{1,0:T(8,128)(2,1)S(1)}, bf16[192,128]{1,0:T(8,128)(2,1)S(1)}, u32[]{:S(2)}, u32[]{:S(2)}) collective-permute-start(bf16[192,128]{1,0:T(8,128)(2,1)S(1)} %get-tuple-element.16), channel_id=1, source_target_pairs={{128,0},{132,4},{136,8},{140,12},{144,16},{148,20},{152,24},{156,2... | collective-permute-start | bytes 147464 | tf_op jit(solution)/shard_map/ppermute | solution.py:26
  84.2 10.1 %collective-permute-start.7 = (bf16[192,128]{1,0:T(8,128)(2,1)S(1)}, bf16[192,128]{1,0:T(8,128)(2,1)S(1)}, u32[]{:S(2)}, u32[]{:S(2)}) collective-permute-start(bf16[192,128]{1,0:T(8,128)(2,1)S(1)} %get-tuple-element.17), channel_id=1, source_target_pairs={{256,0},{260,4},{264,8},{268,12},{272,16},{276,20},{280,24},{284,2... | collective-permute-start | bytes 147464 | tf_op jit(solution)/shard_map/ppermute | solution.py:26
  85.5 19.8 %collective-permute-start.8 = (bf16[192,128]{1,0:T(8,128)(2,1)S(1)}, bf16[192,128]{1,0:T(8,128)(2,1)S(1)}, u32[]{:S(2)}, u32[]{:S(2)}) collective-permute-start(bf16[192,128]{1,0:T(8,128)(2,1)S(1)} %get-tuple-element.18), channel_id=1, source_target_pairs={{512,0},{516,4},{520,8},{524,12},{528,16},{532,20},{536,24},{540,2... | collective-permute-start | bytes 147464 | tf_op jit(solution)/shard_map/ppermute | solution.py:26

commit v5 on v4

--- a/solution.py
+++ b/solution.py
@@ -17,12 +17,15 @@
 NT = (((1,), (1,)), ((), ()))
 TN = (((0,), (0,)), ((), ()))
 Y_ORDERS = ((4, 5, 6, 7, 0, 1, 2, 3), (3, 2, 1, 0, 7, 6, 5, 4))
+Z_ORDER = (8, 9, 10, 11, 12, 13, 14, 15, 0, 1, 2, 3, 4, 5, 6, 7)
+LANES = 128
 VMEM_LIMIT = 16 * 2**20
 
 
-def shifted(block, axis, distance):
+def shifted(block, axis, distance, senders=None, receivers=None):
     devices = range(lax.axis_size(axis))
-    route = [(i - distance, i) for i in devices if i - distance in devices]
+    senders, receivers = senders or devices, receivers or devices
+    route = [(i, i + distance) for i in senders if i + distance in receivers]
     return lax.ppermute(block, axis, route)
 
 
@@ -70,7 +73,7 @@
     return call(pack_kernel, 10**10, shape, kv)
 
 
-def spread_kernel(rows, ys, cores, peers, x_ref, out_ref):
+def spread_kernel(rows, ys, cores, peers, x_ref, out_ref, held, done):
     width = x_ref.shape[1]
     source = lax.broadcasted_iota(jnp.int32, (width, 1), 0)
     target = lax.broadcasted_iota(jnp.int32, (width, width), 1)
@@ -82,16 +85,35 @@
     move = jnp.where(place == target, 1.0, 0.0).astype(jnp.bfloat16)
     moved = dot(x_ref[...], move).astype(jnp.bfloat16)
     part = width // cores
+    copies = []
     for core in range(cores):
+        held[core] = moved[:, core * part : (core + 1) * part]
         for peer in range(peers):
-            out_ref[core * peers + peer] = moved[:, core * part : (core + 1) * part]
+            slot = core * peers + peer
+            copies.append(pltpu.make_async_copy(held.at[core], out_ref.at[slot], done.at[slot]))
+            copies[-1].start()
+    for copy in copies:
+        copy.wait()
 
 
 def spread(x, rows, ys, cores, peers):
     tokens, width = x.shape
-    kernel = functools.partial(spread_kernel, rows, ys, cores, peers)
-    shape = jax.ShapeDtypeStruct((cores * peers, tokens, width // cores), x.dtype)
-    return call(kernel, 2 * tokens * width * width, shape, x)
+    part = (tokens, width // cores)
+    return pl.pallas_call(
+        functools.partial(spread_kernel, rows, ys, cores, peers),
+        out_shape=jax.ShapeDtypeStruct((cores * peers, *part), x.dtype),
+        in_specs=[pl.BlockSpec(memory_space=pltpu.VMEM)],
+        out_specs=pl.BlockSpec(memory_space=pltpu.HBM),
+        scratch_shapes=[
+            pltpu.VMEM((cores, *part), x.dtype),
+            pltpu.SemaphoreType.DMA((cores * peers,)),
+        ],
+        cost_estimate=pl.CostEstimate(
+            flops=2 * tokens * width * width, bytes_accessed=10**6, transcendentals=0
+        ),
+        compiler_params=pltpu.CompilerParams(vmem_limit_bytes=VMEM_LIMIT),
+        name="spread",
+    )(x)
 
 
 def stacked(block, at):
@@ -119,33 +141,43 @@
 
 
 def attention_kernel(distances, chosen_ref, q_ref, go_ref, ao_ref, lse_ref, kv_ref, *refs):
-    one_ref, two_ref, traded_ref, fetched_ref, passed_ref = refs[: LEVELS + 1]
-    gq_ref, gq_too_ref, own_ref = refs[LEVELS + 1 : LEVELS + 4]
+    one_ref, *step_refs, traded_ref, fetched_ref, passed_ref = refs[: LEVELS + 2]
+    gq_ref, own_ref = refs[LEVELS + 2 : LEVELS + 4]
     back_refs = refs[LEVELS + 4 : 2 * LEVELS + 4]
-    sums, four_ref = refs[2 * LEVELS + 4 :]
-    at, quarter = lax.axis_index("z"), lax.axis_size("z") // 4
-    in_second = jnp.logical_and(at >= quarter, at < 2 * quarter)
-    four_ref[...] = jnp.where(in_second, traded_ref[...], fetched_ref[...])
-    far_refs = (one_ref, two_ref, four_ref, passed_ref)
+    sums, two_ref, four_ref, table, done = refs[2 * LEVELS + 4 :]
     blocks = q_ref.shape[0] // BLOCK
     heads = q_ref.shape[1] // DH
     me = lax.axis_index(KV)
+    width = table.shape[1]
+    start = jnp.minimum(me * blocks // LANES * LANES, chosen_ref.shape[1] - width)
+    start = pl.multiple_of(start, LANES)
+    copy = pltpu.make_async_copy(chosen_ref.at[:, pl.ds(start, width)], table, done)
+    copy.start()
+    at, quarter = lax.axis_index("z"), lax.axis_size("z") // 4
+    in_second = jnp.logical_and(at >= quarter, at < 2 * quarter)
+    is_late = me - distances[1] >= lax.axis_size(KV) // 2
+    two_ref[...] = jnp.where(is_late, step_refs[1][...], step_refs[0][...])
+    four_ref[...] = jnp.where(in_second, traded_ref[...], fetched_ref[...])
+    far_refs = (one_ref, two_ref, four_ref, passed_ref)
     lane = lax.broadcasted_iota(jnp.int32, (BLOCK, 2 * DH), 1)
-    sums[...] = jnp.zeros_like(sums)
     key_at = lax.broadcasted_iota(jnp.int32, (BLOCK, heads * BLOCK), 0)
     query_at = lax.broadcasted_iota(jnp.int32, (BLOCK, heads * BLOCK), 1) & (BLOCK - 1)
     causal = key_at <= query_at
+    sums[...] = jnp.zeros_like(sums)
+    staged = []
     for b in range(blocks):
         rows = slice(b * BLOCK, (b + 1) * BLOCK)
         low = stacked(q_ref[rows] * DH ** (-0.5), 0)
         high = stacked(go_ref[rows], DH)
         delta = row_sums(high * stacked(ao_ref[rows], DH), 2)
         lse = jnp.concatenate([lse_ref[h : h + 1, rows] for h in range(heads)], axis=1)
-        low = low.astype(jnp.bfloat16)
-        high = high.astype(jnp.bfloat16)
+        staged.append((low.astype(jnp.bfloat16), high.astype(jnp.bfloat16), lse, delta))
+    copy.wait()
+    for b, (low, high, lse, delta) in enumerate(staged):
+        rows = slice(b * BLOCK, (b + 1) * BLOCK)
         places = []
         for n in range(LEVELS * PER):
-            block = chosen_ref[n, me * blocks + b]
+            block = table[n, me * blocks - start + b]
             block = jnp.where(block >= 0, block - (me - distances[n // PER]) * blocks, 0)
             places.append(pl.multiple_of(block * BLOCK, BLOCK))
         kv = jnp.concatenate(
@@ -167,16 +199,16 @@
         for pair in range(heads // 2):
             first = grad_q[2 * pair * BLOCK : (2 * pair + 1) * BLOCK]
             second = grad_q[(2 * pair + 1) * BLOCK : (2 * pair + 2) * BLOCK]
-            both = jnp.where(lane < DH, first, pltpu.roll(second, DH, 1)).astype(gq_ref.dtype)
-            gq_ref[rows, pair * 2 * DH : (pair + 1) * 2 * DH] = both
-            gq_too_ref[rows, pair * 2 * DH : (pair + 1) * 2 * DH] = both
+            gq_ref[rows, pair * 2 * DH : (pair + 1) * 2 * DH] = jnp.where(
+                lane < DH, first, pltpu.roll(second, DH, 1)
+            ).astype(gq_ref.dtype)
     for level in range(LEVELS):
         back_refs[level][...] = sums[level].astype(jnp.bfloat16)
 
 
 def attention(distances, chosen, q, go, ao, lse, kv, far):
     tokens, width = q.shape
-    shape = (jax.ShapeDtypeStruct((tokens, width), jnp.bfloat16),) * 2
+    shape = (jax.ShapeDtypeStruct((tokens, width), jnp.bfloat16),)
     shape += (jax.ShapeDtypeStruct(kv.shape, jnp.float32),)
     shape += (jax.ShapeDtypeStruct(kv.shape, jnp.bfloat16),) * LEVELS
     return call(
@@ -190,8 +222,13 @@
         lse,
         kv,
         *far,
-        smem=1,
-        scratch=[pltpu.VMEM((LEVELS, *kv.shape), jnp.float32), pltpu.VMEM(kv.shape, kv.dtype)],
+        scratch=[
+            pltpu.VMEM((LEVELS, *kv.shape), jnp.float32),
+            pltpu.VMEM(kv.shape, kv.dtype),
+            pltpu.VMEM(kv.shape, kv.dtype),
+            pltpu.SMEM((chosen.shape[0], min(2 * LANES, chosen.shape[1])), chosen.dtype),
+            pltpu.SemaphoreType.DMA,
+        ],
     )
 
 
@@ -218,31 +255,39 @@
     return call(weight_kernel, flops, shape, mine, other, x)
 
 
-def sum_kernel(tiles_ref, out_ref):
+def sum_kernel(order, tiles_ref, out_ref):
     total = tiles_ref[0].astype(jnp.float32)
     for n in range(1, tiles_ref.shape[0]):
         total = total + tiles_ref[n].astype(jnp.float32)
-    out_ref[...] = total.astype(out_ref.dtype)
-
-
-def summed(tiles, dtype):
+    total = total.astype(out_ref.dtype)
+    if order is None:
+        out_ref[...] = total
+    else:
+        for slot, place in enumerate(order):
+            out_ref[slot] = total[place]
+
+
+def summed(tiles, dtype, order=None):
     shape = jax.ShapeDtypeStruct(tiles.shape[1:], dtype)
-    return call(sum_kernel, tiles.size, shape, tiles)
-
-
-def collect_kernel(own_ref, *refs):
+    return call(functools.partial(sum_kernel, order), tiles.size, shape, tiles)
+
+
+def collect_kernel(grads_ref, own_ref, *refs):
+    *parts, gq_ref, gk_ref, gv_ref = refs
     total = own_ref[...]
-    for ref in refs[:LEVELS]:
+    for ref in parts:
         total = total + ref[...].astype(jnp.float32)
     total = turned(total)
     width = total.shape[0] // 2
-    refs[LEVELS][...] = total[:width].astype(jnp.bfloat16)
-    refs[LEVELS + 1][...] = total[width:].astype(jnp.bfloat16)
-
-
-def collect(own, back):
+    gq_ref[...] = grads_ref[...]
+    gk_ref[...] = total[:width].astype(jnp.bfloat16)
+    gv_ref[...] = total[width:].astype(jnp.bfloat16)
+
+
+def collect(grads, own, back):
     shape = jax.ShapeDtypeStruct((own.shape[1] // 2, own.shape[0]), jnp.bfloat16)
-    return call(collect_kernel, 10**6, (shape, shape), own, *back)
+    shapes = (jax.ShapeDtypeStruct(grads.shape, grads.dtype), shape, shape)
+    return call(collect_kernel, 10**6, shapes, grads, own, *back)
 
 
 def shards(layer_input, queries, keys, values, attn_out, grad_out, log_sum, chosen):
@@ -251,18 +296,20 @@
     out_rows = layer_input.shape[1] * peers // axis_size
     distances = [1, axis_size // 8, axis_size // 4, axis_size // 2]
     key_pair = pack(keys.T, values.T)
-    far = []
-    for distance in distances[:2]:
-        far.append(shifted(key_pair, KV, distance))
+    near = shifted(key_pair, KV, distances[0])
+    halves = [range(axis_size // 2), range(axis_size // 2, axis_size)]
+    steps = []
+    for senders in halves:
+        steps.append(shifted(key_pair, KV, distances[1], senders))
     quarter = lax.axis_size("z") // 4
     quarters = [range(n * quarter, (n + 1) * quarter) for n in range(4)]
     traded = between(key_pair, quarters, ((0, 1), (1, 0)))
     passed = between(traded, quarters, ((1, 2), (0, 3)))
     fetched = between(key_pair, quarters, ((1, 2), (2, 3)))
-    far += [traded, fetched, passed]
+    far = [near, *steps, traded, fetched, passed]
     sent = spread(layer_input, out_rows, ys, cores, peers)
     whole_input = exchanged(sent, ("c", "x"))
-    grad_queries, grads, own, *back = attention(
+    grads, own, *back = attention(
         distances, chosen.T, queries, grad_out, attn_out, log_sum.T, key_pair, far
     )
     route = [(i, cores - 1 - i) for i in range(cores)]
@@ -271,11 +318,14 @@
     groups = [[y * cores + c for y in order] for c, order in enumerate(Y_ORDERS)]
     over_y = exchanged(parts, ("y", "c"), groups)
     returned = []
-    for level, distance in enumerate(distances):
-        returned.append(shifted(back[level], KV, -distance))
-    over_y = summed(over_y.reshape(ys, -1, out_rows, over_y.shape[2]), jnp.bfloat16)
-    over_z = exchanged(over_y, "z")
-    grad_keys, grad_values = collect(own, returned)
+    for level, distance in enumerate(distances[:-1]):
+        for receivers in halves:
+            block = shifted(back[level], KV, -distance, receivers=receivers)
+            returned.append(block)
+    returned.append(shifted(back[-1], KV, -distances[-1]))
+    over_y = summed(over_y.reshape(ys, -1, out_rows, over_y.shape[2]), jnp.bfloat16, Z_ORDER)
+    over_z = exchanged(over_y, "z", [list(Z_ORDER)])
+    grad_queries, grad_keys, grad_values = collect(grads, own, returned)
     grad_weight = summed(over_z, jnp.float32)
     return (grad_queries, grad_keys.T, grad_values.T, grad_weight)
 

time: 107 us -> 113 us (1.056)
  the two profiles are of different devices: /device:TPU:67 before, /device:TPU:6 now
where the time goes in v5:
time: 113 us; the launch traced here: 112 us
  starting transfers between devices  55.9 us (49%)
  waiting for transfers between devices  26 us (23%)
  blocking collectives  21.6 us (19%)
  Pallas kernels  6.44 us (6%)
    all_to_all x2, starting transfers between devices, exchanged(): lax.all_to_all(tiles, axis, split_axis=0, concat_axis=0, tiled=True, axis...  33 us
    all_to_all x1, blocking collectives, exchanged(): lax.all_to_all(tiles, axis, split_axis=0, concat_axis=0, tiled=True, axis...  21.6 us
    ppermute x10, waiting for transfers between devices, shifted(): return lax.ppermute(block, axis, route)  18.6 us
    ppermute x10, starting transfers between devices, shifted(): return lax.ppermute(block, axis, route)  12.6 us
    ppermute x3, starting transfers between devices, between(): return lax.ppermute(block, 'z', route)  8.11 us
    ppermute x3, waiting for transfers between devices, between(): return lax.ppermute(block, 'z', route)  6.52 us
    pallas_call x6, Pallas kernels, call(): pl.pallas_call(kernel, out_shape=out_shape, in_specs=[pl.BlockSpec(memory...  5.12 us
    ppermute x1, starting transfers between devices, shards(): other = lax.ppermute(grads, 'c', route)  2.3 us
  transfers between devices with their start and end apart: 16, of which 5 were waited for; matrix products, arithmetic and copies ran while one was open for 0% of the time, Pallas kernels for 3%

profile of v5, /device:TPU:6, one launch (start us, length us, event | category | flops | bytes accessed | tf_op | source)
XLA Modules:
  0.0 111.9 jit_solution(13375105132138075084)
XLA Ops:
  0.6 0.9 copy-done
  1.6 1.3 %spread.1 = bf16[8,192,256]{2,1,0:T(8,128)(2,1)} custom-call(bf16[192,512]{1,0:T(8,128)(2,1)S(1)} %copy-done), custom_call_target="tpu_custom_call" | custom-call | flops 100663296 | bytes 1000000 | tf_op jit(solution)/shard_map/spread/pallas_call | solution.py:102
  2.9 16.6 %all-to-all-start = ((bf16[8,192,256]{2,1,0:T(8,128)(2,1)}), bf16[8,192,256]{2,1,0:T(8,128)(2,1)S(1)}, u32[]{:S(2)}, u32[]{:S(2)}) async-start(bf16[8,192,256]{2,1,0:T(8,128)(2,1)} %spread.1), calls=%async_computation | async-start | bytes 1572864 | tf_op jit(solution)/shard_map/all_to_all | solution.py:38
  19.5 0.0 copy-start.1
  19.5 0.0 copy-start.2
  19.6 0.1 shard_map.111.kv_ref
  19.7 2.1 %collective-permute-start.3 = (bf16[192,128]{1,0:T(8,128)(2,1)S(1)}, bf16[192,128]{1,0:T(8,128)(2,1)S(1)}, u32[]{:S(2)}, u32[]{:S(2)}) collective-permute-start(bf16[192,128]{1,0:T(8,128)(2,1)S(1)} %shard_map.111.kv_ref), channel_id=1, source_target_pairs={{0,256},{64,320},{128,384},{192,448},{256,0},{320,64},{384,128},{4... | collective-permute-start | bytes 147464 | tf_op jit(solution)/shard_map/ppermute | solution.py:34
  21.7 0.7 collective-permute-start.4
  22.4 0.7 collective-permute-start.2
  23.1 3.3 %collective-permute-start.1 = (bf16[192,128]{1,0:T(8,128)(2,1)S(1)}, bf16[192,128]{1,0:T(8,128)(2,1)S(1)}, u32[]{:S(2)}, u32[]{:S(2)}) collective-permute-start(bf16[192,128]{1,0:T(8,128)(2,1)S(1)} %shard_map.111.kv_ref), channel_id=1, source_target_pairs={{0,128},{4,132},{8,136},{12,140},{16,144},{20,148},{24,152},{28,15... | collective-permute-start | bytes 147464 | tf_op jit(solution)/shard_map/ppermute | solution.py:29
  26.4 1.5 %collective-permute-start = (bf16[192,128]{1,0:T(8,128)(2,1)S(1)}, bf16[192,128]{1,0:T(8,128)(2,1)S(1)}, u32[]{:S(2)}, u32[]{:S(2)}) collective-permute-start(bf16[192,128]{1,0:T(8,128)(2,1)S(1)} %shard_map.111.kv_ref), channel_id=1, source_target_pairs={{0,4},{4,8},{8,12},{12,16},{16,20},{20,24},{24,28},{28,32},{32,36}... | collective-permute-start | bytes 147464 | tf_op jit(solution)/shard_map/ppermute | solution.py:29
  27.8 1.8 %collective-permute-done.3.refs_3_ = bf16[192,128]{1,0:T(8,128)(2,1)S(1)} collective-permute-done((bf16[192,128]{1,0:T(8,128)(2,1)S(1)}, bf16[192,128]{1,0:T(8,128)(2,1)S(1)}, u32[]{:S(2)}, u32[]{:S(2)}) %collective-permute-start.3) | collective-permute-done | bytes 49184 | tf_op jit(solution)/shard_map/ppermute | solution.py:34
  29.7 5.4 %collective-permute-start.5 = (bf16[192,128]{1,0:T(8,128)(2,1)S(1)}, bf16[192,128]{1,0:T(8,128)(2,1)S(1)}, u32[]{:S(2)}, u32[]{:S(2)}) collective-permute-start(bf16[192,128]{1,0:T(8,128)(2,1)S(1)} %collective-permute-done.3.refs_3_), channel_id=1, source_target_pairs={{256,512},{320,576},{384,640},{448,704},{0,768},{64,832},{128,896}... | collective-permute-start | bytes 147464 | tf_op jit(solution)/shard_map/ppermute | solution.py:34
  35.1 4.7 %collective-permute-done.5.refs_5_ = bf16[192,128]{1,0:T(8,128)(2,1)S(1)} collective-permute-done((bf16[192,128]{1,0:T(8,128)(2,1)S(1)}, bf16[192,128]{1,0:T(8,128)(2,1)S(1)}, u32[]{:S(2)}, u32[]{:S(2)}) %collective-permute-start.5) | collective-permute-done | bytes 49184 | tf_op jit(solution)/shard_map/ppermute | solution.py:34
  39.8 2.5 %shard_map.112 = (bf16[192,256]{1,0:T(8,128)(2,1)S(1)}, f32[192,128]{1,0:T(8,128)S(1)}, bf16[192,128]{1,0:T(8,128)(2,1)S(1)}, bf16[192,128]{1,0:T(8,128)(2,1)S(1...) custom-call(s32[8,768]{1,0:T(8,128)S(1)} %bitcast.8, bf16[192,256]{1,0:T(8,128)(2,1)S(1)} %copy-done.1, ...), custom_call_target="tpu_custom_call" | custom-call | flops 2000000000 | bytes 666624 | tf_op jit(solution)/shard_map/pallas_call | solution.py:51
  42.3 2.3 %collective-permute-start.13 = (bf16[192,256]{1,0:T(8,128)(2,1)S(1)}, bf16[192,256]{1,0:T(8,128)(2,1)S(1)}, u32[]{:S(2)}, u32[]{:S(2)}) collective-permute-start(bf16[192,256]{1,0:T(8,128)(2,1)S(1)} %get-tuple-element.13.grads_ref.mine_ref), channel_id=1, source_target_pairs={{0,4},{4,0},{1,5},{5,1},{2,6},{6,2},{3,7},{7,3},{8,12},{12,8},{9,1... | collective-permute-start | bytes 294920 | tf_op jit(solution)/shard_map/ppermute | solution.py:316
  44.6 0.9 collective-permute-done.13.other_ref
  45.6 0.5 shard_map.114
  46.1 21.6 %all_to_all.15 = bf16[8,128,256]{2,1,0:T(8,128)(2,1)S(1)} all-to-all(bf16[8,128,256]{2,1,0:T(8,128)(2,1)S(1)} %shard_map.114), channel_id=1, replica_groups={{32,40,48,56,0,8,16,24},{28,20,12,4,60,52,44,36},{33,41,49,57,1,9,17,25..., dimensions={0} | all-to-all | bytes 1048576 | tf_op jit(solution)/shard_map/all_to_all | solution.py:38
  67.7 0.7 shard_map.115
  68.4 16.4 %all-to-all-start.2 = ((bf16[16,8,256]{2,1,0:T(8,128)(2,1)}), bf16[16,8,256]{2,1,0:T(8,128)(2,1)S(1)}, u32[]{:S(2)}, u32[]{:S(2)}) async-start(bf16[16,8,256]{2,1,0:T(8,128)(2,1)} %shard_map.115), calls=%async_computation.2 | async-start | bytes 131072 | tf_op jit(solution)/shard_map/all_to_all | solution.py:38
  84.8 1.3 %collective-permute-start.12 = (bf16[192,128]{1,0:T(8,128)(2,1)S(1)}, bf16[192,128]{1,0:T(8,128)(2,1)S(1)}, u32[]{:S(2)}, u32[]{:S(2)}) collective-permute-start(bf16[192,128]{1,0:T(8,128)(2,1)S(1)} %get-tuple-element.18), channel_id=1, source_target_pairs={{512,0},{516,4},{520,8},{524,12},{528,16},{532,20},{536,24},{540,2... | collective-permute-start | bytes 147464 | tf_op jit(solution)/shard_map/ppermute | solution.py:29
  86.0 0.7 collective-permute-start.7
  86.7 1.3 %collective-permute-start.6 = (bf16[192,128]{1,0:T(8,128)(2,1)S(1)}, bf16[192,128]{1,0:T(8,128)(2,1)S(1)}, u32[]{:S(2)}, u32[]{:S(2)}) collective-permute-start(bf16[192,128]{1,0:T(8,128)(2,1)S(1)} %get-tuple-element.15), channel_id=1, source_target_pairs={{4,0},{8,4},{12,8},{16,12},{20,16},{24,20},{28,24},{32,28},{36,32}... | collective-permute-start | bytes 147464 | tf_op jit(solution)/shard_map/ppermute | solution.py:29
  88.0 0.7 collective-permute-start.9
  88.7 1.3 %collective-permute-start.8 = (bf16[192,128]{1,0:T(8,128)(2,1)S(1)}, bf16[192,128]{1,0:T(8,128)(2,1)S(1)}, u32[]{:S(2)}, u32[]{:S(2)}) collective-permute-start(bf16[192,128]{1,0:T(8,128)(2,1)S(1)} %get-tuple-element.16), channel_id=1, source_target_pairs={{128,0},{132,4},{136,8},{140,12},{144,16},{148,20},{152,24},{156,2... | collective-permute-start | bytes 147464 | tf_op jit(solution)/shard_map/ppermute | solution.py:29
  90.0 9.5 %collective-permute-done.12.refs_6_ = bf16[192,128]{1,0:T(8,128)(2,1)S(1)} collective-permute-done((bf16[192,128]{1,0:T(8,128)(2,1)S(1)}, bf16[192,128]{1,0:T(8,128)(2,1)S(1)}, u32[]{:S(2)}, u32[]{:S(2)}) %collective-permute-start.12) | collective-permute-done | bytes 49184 | tf_op jit(solution)/shard_map/ppermute | solution.py:29
  99.4 0.7 collective-permute-start.11
  100.1 1.3 %collective-permute-start.10 = (bf16[192,128]{1,0:T(8,128)(2,1)S(1)}, bf16[192,128]{1,0:T(8,128)(2,1)S(1)}, u32[]{:S(2)}, u32[]{:S(2)}) collective-permute-start(bf16[192,128]{1,0:T(8,128)(2,1)S(1)} %get-tuple-element.17), channel_id=1, source_target_pairs={{256,0},{260,4},{264,8},{268,12},{272,16},{276,20},{280,24},{284,2... | collective-permute-start | bytes 147464 | tf_op jit(solution)/shard_map/ppermute | solution.py:29
  101.5 9.1 %collective-permute-done.10.refs_4_ = bf16[192,128]{1,0:T(8,128)(2,1)S(1)} collective-permute-done((bf16[192,128]{1,0:T(8,128)(2,1)S(1)}, bf16[192,128]{1,0:T(8,128)(2,1)S(1)}, u32[]{:S(2)}, u32[]{:S(2)}) %collective-permute-start.10) | collective-permute-done | bytes 49184 | tf_op jit(solution)/shard_map/ppermute | solution.py:29
  110.5 0.7 shard_map.113
  111.3 0.6 shard_map.116
  (25 shorter events, 0.1 us)
Async XLA Ops:
  0.6 0.9 copy-start
  2.9 16.6 %copy-start.6 = (bf16[192,64]{0,1:T(8,128)(2,1)S(1)}, bf16[192,64]{0,1:T(8,128)(2,1)}, u32[]{:S(2)}) copy-start(bf16[192,64]{0,1:T(8,128)(2,1)} %param.11) | copy-start | bytes 73732
  2.9 16.6 %copy-start.7 = (bf16[192,64]{0,1:T(8,128)(2,1)S(1)}, bf16[192,64]{0,1:T(8,128)(2,1)}, u32[]{:S(2)}) copy-start(bf16[192,64]{0,1:T(8,128)(2,1)} %param.10) | copy-start | bytes 73732
  2.9 42.7 %all-to-all-start = ((bf16[8,192,256]{2,1,0:T(8,128)(2,1)}), bf16[8,192,256]{2,1,0:T(8,128)(2,1)S(1)}, u32[]{:S(2)}, u32[]{:S(2)}) async-start(bf16[8,192,256]{2,1,0:T(8,128)(2,1)} %spread.1), calls=%async_computation | async-start | bytes 1572864 | tf_op jit(solution)/shard_map/all_to_all | solution.py:38
  19.5 20.3 %copy-start.1 = (bf16[192,256]{1,0:T(8,128)(2,1)S(1)}, bf16[192,256]{1,0:T(8,128)(2,1)}, u32[]{:S(2)}) copy-start(bf16[192,256]{1,0:T(8,128)(2,1)} %q_ref.1) | copy-start | bytes 294916
  19.5 20.3 %copy-start.2 = (bf16[192,256]{1,0:T(8,128)(2,1)S(1)}, bf16[192,256]{1,0:T(8,128)(2,1)}, u32[]{:S(2)}) copy-start(bf16[192,256]{1,0:T(8,128)(2,1)} %go_ref.1) | copy-start | bytes 294916
  19.5 20.3 %copy-start.3 = (bf16[192,256]{1,0:T(8,128)(2,1)S(1)}, bf16[192,256]{1,0:T(8,128)(2,1)}, u32[]{:S(2)}) copy-start(bf16[192,256]{1,0:T(8,128)(2,1)} %ao_ref.1) | copy-start | bytes 294916
  19.5 20.3 %copy-start.4 = (s32[768,8]{0,1:T(8,128)S(1)}, s32[768,8]{0,1:T(8,128)}, u32[]{:S(2)}) copy-start(s32[768,8]{0,1:T(8,128)} %param.15) | copy-start | bytes 73732
  19.6 20.3 %copy-start.5 = (f32[192,4]{0,1:T(4,128)S(1)}, f32[192,4]{0,1:T(4,128)}, u32[]{:S(2)}) copy-start(f32[192,4]{0,1:T(4,128)} %param.14) | copy-start | bytes 9220
  19.7 10.0 %collective-permute-start.3 = (bf16[192,128]{1,0:T(8,128)(2,1)S(1)}, bf16[192,128]{1,0:T(8,128)(2,1)S(1)}, u32[]{:S(2)}, u32[]{:S(2)}) collective-permute-start(bf16[192,128]{1,0:T(8,128)(2,1)S(1)} %shard_map.111.kv_ref), channel_id=1, source_target_pairs={{0,256},{64,320},{128,384},{192,448},{256,0},{320,64},{384,128},{4... | collective-permute-start | bytes 147464 | tf_op jit(solution)/shard_map/ppermute | solution.py:34
  21.7 13.4 %collective-permute-start.4 = (bf16[192,128]{1,0:T(8,128)(2,1)S(1)}, bf16[192,128]{1,0:T(8,128)(2,1)S(1)}, u32[]{:S(2)}, u32[]{:S(2)}) collective-permute-start(bf16[192,128]{1,0:T(8,128)(2,1)S(1)} %shard_map.111.kv_ref), channel_id=1, source_target_pairs={{256,512},{320,576},{384,640},{448,704},{512,768},{576,832},{640,8... | collective-permute-start | bytes 147464 | tf_op jit(solution)/shard_map/ppermute | solution.py:34
  22.4 12.7 %collective-permute-start.2 = (bf16[192,128]{1,0:T(8,128)(2,1)S(1)}, bf16[192,128]{1,0:T(8,128)(2,1)S(1)}, u32[]{:S(2)}, u32[]{:S(2)}) collective-permute-start(bf16[192,128]{1,0:T(8,128)(2,1)S(1)} %shard_map.111.kv_ref), channel_id=1, source_target_pairs={{512,640},{516,644},{520,648},{524,652},{528,656},{532,660},{536,6... | collective-permute-start | bytes 147464 | tf_op jit(solution)/shard_map/ppermute | solution.py:29
  23.1 12.0 %collective-permute-start.1 = (bf16[192,128]{1,0:T(8,128)(2,1)S(1)}, bf16[192,128]{1,0:T(8,128)(2,1)S(1)}, u32[]{:S(2)}, u32[]{:S(2)}) collective-permute-start(bf16[192,128]{1,0:T(8,128)(2,1)S(1)} %shard_map.111.kv_ref), channel_id=1, source_target_pairs={{0,128},{4,132},{8,136},{12,140},{16,144},{20,148},{24,152},{28,15... | collective-permute-start | bytes 147464 | tf_op jit(solution)/shard_map/ppermute | solution.py:29
  26.4 8.8 %collective-permute-start = (bf16[192,128]{1,0:T(8,128)(2,1)S(1)}, bf16[192,128]{1,0:T(8,128)(2,1)S(1)}, u32[]{:S(2)}, u32[]{:S(2)}) collective-permute-start(bf16[192,128]{1,0:T(8,128)(2,1)S(1)} %shard_map.111.kv_ref), channel_id=1, source_target_pairs={{0,4},{4,8},{8,12},{12,16},{16,20},{20,24},{24,28},{28,32},{32,36}... | collective-permute-start | bytes 147464 | tf_op jit(solution)/shard_map/ppermute | solution.py:29
  29.7 10.1 %collective-permute-start.5 = (bf16[192,128]{1,0:T(8,128)(2,1)S(1)}, bf16[192,128]{1,0:T(8,128)(2,1)S(1)}, u32[]{:S(2)}, u32[]{:S(2)}) collective-permute-start(bf16[192,128]{1,0:T(8,128)(2,1)S(1)} %collective-permute-done.3.refs_3_), channel_id=1, source_target_pairs={{256,512},{320,576},{384,640},{448,704},{0,768},{64,832},{128,896}... | collective-permute-start | bytes 147464 | tf_op jit(solution)/shard_map/ppermute | solution.py:34
  42.3 3.2 %collective-permute-start.13 = (bf16[192,256]{1,0:T(8,128)(2,1)S(1)}, bf16[192,256]{1,0:T(8,128)(2,1)S(1)}, u32[]{:S(2)}, u32[]{:S(2)}) collective-permute-start(bf16[192,256]{1,0:T(8,128)(2,1)S(1)} %get-tuple-element.13.grads_ref.mine_ref), channel_id=1, source_target_pairs={{0,4},{4,0},{1,5},{5,1},{2,6},{6,2},{3,7},{7,3},{8,12},{12,8},{9,1... | collective-permute-start | bytes 294920 | tf_op jit(solution)/shard_map/ppermute | solution.py:316
  68.4 42.9 %all-to-all-start.2 = ((bf16[16,8,256]{2,1,0:T(8,128)(2,1)}), bf16[16,8,256]{2,1,0:T(8,128)(2,1)S(1)}, u32[]{:S(2)}, u32[]{:S(2)}) async-start(bf16[16,8,256]{2,1,0:T(8,128)(2,1)} %shard_map.115), calls=%async_computation.2 | async-start | bytes 131072 | tf_op jit(solution)/shard_map/all_to_all | solution.py:38
  84.8 14.7 %collective-permute-start.12 = (bf16[192,128]{1,0:T(8,128)(2,1)S(1)}, bf16[192,128]{1,0:T(8,128)(2,1)S(1)}, u32[]{:S(2)}, u32[]{:S(2)}) collective-permute-start(bf16[192,128]{1,0:T(8,128)(2,1)S(1)} %get-tuple-element.18), channel_id=1, source_target_pairs={{512,0},{516,4},{520,8},{524,12},{528,16},{532,20},{536,24},{540,2... | collective-permute-start | bytes 147464 | tf_op jit(solution)/shard_map/ppermute | solution.py:29
  86.0 14.1 %collective-permute-start.7 = (bf16[192,128]{1,0:T(8,128)(2,1)S(1)}, bf16[192,128]{1,0:T(8,128)(2,1)S(1)}, u32[]{:S(2)}, u32[]{:S(2)}) collective-permute-start(bf16[192,128]{1,0:T(8,128)(2,1)S(1)} %get-tuple-element.15), channel_id=1, source_target_pairs={{516,512},{520,516},{524,520},{528,524},{532,528},{536,532},{540,5... | collective-permute-start | bytes 147464 | tf_op jit(solution)/shard_map/ppermute | solution.py:29
  86.7 14.7 %collective-permute-start.6 = (bf16[192,128]{1,0:T(8,128)(2,1)S(1)}, bf16[192,128]{1,0:T(8,128)(2,1)S(1)}, u32[]{:S(2)}, u32[]{:S(2)}) collective-permute-start(bf16[192,128]{1,0:T(8,128)(2,1)S(1)} %get-tuple-element.15), channel_id=1, source_target_pairs={{4,0},{8,4},{12,8},{16,12},{20,16},{24,20},{28,24},{32,28},{36,32}... | collective-permute-start | bytes 147464 | tf_op jit(solution)/shard_map/ppermute | solution.py:29
  88.0 13.4 %collective-permute-start.9 = (bf16[192,128]{1,0:T(8,128)(2,1)S(1)}, bf16[192,128]{1,0:T(8,128)(2,1)S(1)}, u32[]{:S(2)}, u32[]{:S(2)}) collective-permute-start(bf16[192,128]{1,0:T(8,128)(2,1)S(1)} %get-tuple-element.16), channel_id=1, source_target_pairs={{640,512},{644,516},{648,520},{652,524},{656,528},{660,532},{664,5... | collective-permute-start | bytes 147464 | tf_op jit(solution)/shard_map/ppermute | solution.py:29
  88.7 12.7 %collective-permute-start.8 = (bf16[192,128]{1,0:T(8,128)(2,1)S(1)}, bf16[192,128]{1,0:T(8,128)(2,1)S(1)}, u32[]{:S(2)}, u32[]{:S(2)}) collective-permute-start(bf16[192,128]{1,0:T(8,128)(2,1)S(1)} %get-tuple-element.16), channel_id=1, source_target_pairs={{128,0},{132,4},{136,8},{140,12},{144,16},{148,20},{152,24},{156,2... | collective-permute-start | bytes 147464 | tf_op jit(solution)/shard_map/ppermute | solution.py:29
  99.4 2.0 %collective-permute-start.11 = (bf16[192,128]{1,0:T(8,128)(2,1)S(1)}, bf16[192,128]{1,0:T(8,128)(2,1)S(1)}, u32[]{:S(2)}, u32[]{:S(2)}) collective-permute-start(bf16[192,128]{1,0:T(8,128)(2,1)S(1)} %get-tuple-element.17), channel_id=1, source_target_pairs={{768,512},{772,516},{776,520},{780,524},{784,528},{788,532},{792,5... | collective-permute-start | bytes 147464 | tf_op jit(solution)/shard_map/ppermute | solution.py:29
  100.1 10.4 %collective-permute-start.10 = (bf16[192,128]{1,0:T(8,128)(2,1)S(1)}, bf16[192,128]{1,0:T(8,128)(2,1)S(1)}, u32[]{:S(2)}, u32[]{:S(2)}) collective-permute-start(bf16[192,128]{1,0:T(8,128)(2,1)S(1)} %get-tuple-element.17), channel_id=1, source_target_pairs={{256,0},{260,4},{264,8},{268,12},{272,16},{276,20},{280,24},{284,2... | collective-permute-start | bytes 147464 | tf_op jit(solution)/shard_map/ppermute | solution.py:29

commit v6 on v5

--- a/solution.py
+++ b/solution.py
@@ -16,9 +16,10 @@
 KV = ("z", "y", "c")
 NT = (((1,), (1,)), ((), ()))
 TN = (((0,), (0,)), ((), ()))
-Y_ORDERS = ((4, 5, 6, 7, 0, 1, 2, 3), (3, 2, 1, 0, 7, 6, 5, 4))
+Y_ORDERS = ((3, 2, 1, 0, 7, 6, 5, 4), (5, 6, 7, 0, 1, 2, 3, 4))
 Z_ORDER = (8, 9, 10, 11, 12, 13, 14, 15, 0, 1, 2, 3, 4, 5, 6, 7)
 LANES = 128
+WINDOWS = 2
 VMEM_LIMIT = 16 * 2**20
 
 
@@ -76,18 +77,17 @@
 def spread_kernel(rows, ys, cores, peers, x_ref, out_ref, held, done):
     width = x_ref.shape[1]
     source = lax.broadcasted_iota(jnp.int32, (width, 1), 0)
-    target = lax.broadcasted_iota(jnp.int32, (width, width), 1)
     inner, left = source & (rows - 1), source // rows
     core, left = left & (cores - 1), left // cores
     y, z = left & (ys - 1), left // ys
     zs = width // (rows * cores * ys)
     place = ((core * ys + y) * zs + z) * rows + inner
-    move = jnp.where(place == target, 1.0, 0.0).astype(jnp.bfloat16)
-    moved = dot(x_ref[...], move).astype(jnp.bfloat16)
     part = width // cores
+    target = lax.broadcasted_iota(jnp.int32, (width, part), 1)
     copies = []
     for core in range(cores):
-        held[core] = moved[:, core * part : (core + 1) * part]
+        move = jnp.where(place == target + core * part, 1.0, 0.0).astype(jnp.bfloat16)
+        held[core] = dot(x_ref[...], move).astype(jnp.bfloat16)
         for peer in range(peers):
             slot = core * peers + peer
             copies.append(pltpu.make_async_copy(held.at[core], out_ref.at[slot], done.at[slot]))
@@ -140,19 +140,64 @@
     return total[:1]
 
 
-def attention_kernel(distances, chosen_ref, q_ref, go_ref, ao_ref, lse_ref, kv_ref, *refs):
+def terms(kv, low, high, lse, delta, keep=None):
+    weights = jnp.exp(dot(kv, low, NT) - lse)
+    if keep is not None:
+        weights = jnp.where(keep, weights, 0.0)
+    dscores = (weights * (dot(kv, high, NT) - delta)).astype(jnp.bfloat16)
+    grad_kv = dot(dscores, low) + dot(weights.astype(jnp.bfloat16), high)
+    return dot(dscores, kv, TN), grad_kv
+
+
+def own_kernel(q_ref, go_ref, ao_ref, lse_ref, kv_ref, low_ref, high_ref, rows_ref, part_ref, own_ref):
+    heads = q_ref.shape[1] // DH
+    key_at = lax.broadcasted_iota(jnp.int32, (BLOCK, heads * BLOCK), 0)
+    query_at = lax.broadcasted_iota(jnp.int32, (BLOCK, heads * BLOCK), 1) & (BLOCK - 1)
+    for b in range(q_ref.shape[0] // BLOCK):
+        rows = slice(b * BLOCK, (b + 1) * BLOCK)
+        low = stacked(q_ref[rows] * DH ** (-0.5), 0)
+        high = stacked(go_ref[rows], DH)
+        delta = row_sums(high * stacked(ao_ref[rows], DH), 2)
+        lse = jnp.concatenate([lse_ref[h : h + 1, rows] for h in range(heads)], axis=1)
+        low = low.astype(jnp.bfloat16)
+        high = high.astype(jnp.bfloat16)
+        grad_q, grad_kv = terms(kv_ref[rows], low, high, lse, delta, key_at <= query_at)
+        low_ref[b] = low
+        high_ref[b] = high
+        rows_ref[b, :1] = lse
+        rows_ref[b, 1:] = delta
+        part_ref[b] = grad_q
+        own_ref[rows] = grad_kv
+
+
+def attend_own(q, go, ao, lse, kv):
+    tokens, width = q.shape
+    blocks, rows = tokens // BLOCK, width * BLOCK // DH
+    shape = (jax.ShapeDtypeStruct((blocks, rows, 2 * DH), jnp.bfloat16),) * 2
+    shape += (jax.ShapeDtypeStruct((blocks, 2, rows), jnp.float32),)
+    shape += (jax.ShapeDtypeStruct((blocks, rows, 2 * DH), jnp.float32),)
+    shape += (jax.ShapeDtypeStruct(kv.shape, jnp.float32),)
+    return call(own_kernel, 10**9, shape, q, go, ao, lse, kv)
+
+
+def far_kernel(distances, chosen_ref, low_ref, high_ref, rows_ref, part_ref, *refs):
     one_ref, *step_refs, traded_ref, fetched_ref, passed_ref = refs[: LEVELS + 2]
-    gq_ref, own_ref = refs[LEVELS + 2 : LEVELS + 4]
-    back_refs = refs[LEVELS + 4 : 2 * LEVELS + 4]
-    sums, two_ref, four_ref, table, done = refs[2 * LEVELS + 4 :]
-    blocks = q_ref.shape[0] // BLOCK
-    heads = q_ref.shape[1] // DH
+    gq_ref = refs[LEVELS + 2]
+    back_refs = refs[LEVELS + 3 : 2 * LEVELS + 3]
+    sums, two_ref, four_ref = refs[2 * LEVELS + 3 :]
+    blocks = low_ref.shape[0]
+    heads = low_ref.shape[1] // BLOCK
     me = lax.axis_index(KV)
-    width = table.shape[1]
-    start = jnp.minimum(me * blocks // LANES * LANES, chosen_ref.shape[1] - width)
-    start = pl.multiple_of(start, LANES)
-    copy = pltpu.make_async_copy(chosen_ref.at[:, pl.ds(start, width)], table, done)
-    copy.start()
+    first = me * blocks
+    start = jnp.minimum(first // LANES * LANES, chosen_ref.shape[1] - LANES * WINDOWS)
+    columns = lax.broadcasted_iota(jnp.int32, (LEVELS * PER, LANES), 1)
+    picked = [jnp.zeros((LEVELS * PER, LANES), jnp.int32)] * blocks
+    for window in range(WINDOWS):
+        tile = chosen_ref[:, pl.ds(pl.multiple_of(start + window * LANES, LANES), LANES)]
+        for b in range(blocks):
+            here = columns == first + b - start - window * LANES
+            picked[b] = picked[b] + jnp.where(here, tile, 0)
+    picked = [jnp.sum(tile.astype(jnp.float32), axis=1, keepdims=True).astype(jnp.int32) for tile in picked]
     at, quarter = lax.axis_index("z"), lax.axis_size("z") // 4
     in_second = jnp.logical_and(at >= quarter, at < 2 * quarter)
     is_late = me - distances[1] >= lax.axis_size(KV) // 2
@@ -160,42 +205,23 @@
     four_ref[...] = jnp.where(in_second, traded_ref[...], fetched_ref[...])
     far_refs = (one_ref, two_ref, four_ref, passed_ref)
     lane = lax.broadcasted_iota(jnp.int32, (BLOCK, 2 * DH), 1)
-    key_at = lax.broadcasted_iota(jnp.int32, (BLOCK, heads * BLOCK), 0)
-    query_at = lax.broadcasted_iota(jnp.int32, (BLOCK, heads * BLOCK), 1) & (BLOCK - 1)
-    causal = key_at <= query_at
     sums[...] = jnp.zeros_like(sums)
-    staged = []
     for b in range(blocks):
-        rows = slice(b * BLOCK, (b + 1) * BLOCK)
-        low = stacked(q_ref[rows] * DH ** (-0.5), 0)
-        high = stacked(go_ref[rows], DH)
-        delta = row_sums(high * stacked(ao_ref[rows], DH), 2)
-        lse = jnp.concatenate([lse_ref[h : h + 1, rows] for h in range(heads)], axis=1)
-        staged.append((low.astype(jnp.bfloat16), high.astype(jnp.bfloat16), lse, delta))
-    copy.wait()
-    for b, (low, high, lse, delta) in enumerate(staged):
         rows = slice(b * BLOCK, (b + 1) * BLOCK)
         places = []
         for n in range(LEVELS * PER):
-            block = table[n, me * blocks - start + b]
+            block = picked[b][n, 0]
             block = jnp.where(block >= 0, block - (me - distances[n // PER]) * blocks, 0)
-            places.append(pl.multiple_of(block * BLOCK, BLOCK))
+            places.append(pl.ds(pl.multiple_of(block * BLOCK, BLOCK), BLOCK))
         kv = jnp.concatenate(
-            [kv_ref[rows]]
-            + [far_refs[n // PER][pl.ds(places[n], BLOCK), :] for n in range(LEVELS * PER)],
-            axis=0,
+            [far_refs[n // PER][places[n], :] for n in range(LEVELS * PER)], axis=0
         )
-        weights = jnp.exp(dot(kv, low, NT) - lse)
-        weights = jnp.concatenate(
-            [jnp.where(causal, weights[:BLOCK], 0.0), weights[BLOCK:]], axis=0
+        grad_q, grad_kv = terms(
+            kv, low_ref[b], high_ref[b], rows_ref[b, :1], rows_ref[b, 1:]
         )
-        dscores = (weights * (dot(kv, high, NT) - delta)).astype(jnp.bfloat16)
-        grad_kv = dot(dscores, low) + dot(weights.astype(jnp.bfloat16), high)
-        own_ref[rows] = grad_kv[:BLOCK]
         for n in range(LEVELS * PER):
-            at = pl.ds(places[n], BLOCK)
-            sums[n // PER, at, :] += grad_kv[(n + 1) * BLOCK : (n + 2) * BLOCK]
-        grad_q = dot(dscores, kv, TN) * DH ** (-0.5)
+            sums[n // PER, places[n], :] += grad_kv[n * BLOCK : (n + 1) * BLOCK]
+        grad_q = (part_ref[b] + grad_q) * DH ** (-0.5)
         for pair in range(heads // 2):
             first = grad_q[2 * pair * BLOCK : (2 * pair + 1) * BLOCK]
             second = grad_q[(2 * pair + 1) * BLOCK : (2 * pair + 2) * BLOCK]
@@ -206,53 +232,71 @@
         back_refs[level][...] = sums[level].astype(jnp.bfloat16)
 
 
-def attention(distances, chosen, q, go, ao, lse, kv, far):
-    tokens, width = q.shape
+def attend_far(distances, chosen, low, high, rows, part, far):
+    tokens, width = low.shape[0] * BLOCK, low.shape[1] * DH // BLOCK
+    kv = far[0]
     shape = (jax.ShapeDtypeStruct((tokens, width), jnp.bfloat16),)
-    shape += (jax.ShapeDtypeStruct(kv.shape, jnp.float32),)
     shape += (jax.ShapeDtypeStruct(kv.shape, jnp.bfloat16),) * LEVELS
     return call(
-        functools.partial(attention_kernel, distances),
+        functools.partial(far_kernel, distances),
         2 * 10**9,
         shape,
         chosen,
-        q,
-        go,
-        ao,
-        lse,
-        kv,
+        low,
+        high,
+        rows,
+        part,
         *far,
         scratch=[
             pltpu.VMEM((LEVELS, *kv.shape), jnp.float32),
             pltpu.VMEM(kv.shape, kv.dtype),
             pltpu.VMEM(kv.shape, kv.dtype),
-            pltpu.SMEM((chosen.shape[0], min(2 * LANES, chosen.shape[1])), chosen.dtype),
-            pltpu.SemaphoreType.DMA,
         ],
     )
 
 
-def weight_kernel(mine_ref, other_ref, x_ref, out_ref):
+def weight_kernel(mine_ref, other_ref, x_ref, out_ref, held, done):
     core = lax.axis_index("c")
     peers = x_ref.shape[0] // 2
     ys = out_ref.shape[0]
+    step = x_ref.shape[2] // ys
     grads = jnp.concatenate([mine_ref[...], other_ref[...]], axis=0)
-    for peer in range(peers):
-        x = jnp.concatenate(
-            [x_ref[core * peers + peer], x_ref[(1 - core) * peers + peer]], axis=0
-        )
-        part = dot(x, grads, TN).astype(out_ref.dtype)
-        step = part.shape[0] // ys
-        for y in range(ys):
+    copies = []
+    for half in range(2):
+        mine = range(half * ys // 2, (half + 1) * ys // 2)
+        lanes = slice(mine[0] * step, (mine[-1] + 1) * step)
+        for peer in range(peers):
+            x = jnp.concatenate(
+                [x_ref[core * peers + peer, :, lanes], x_ref[(1 - core) * peers + peer, :, lanes]],
+                axis=0,
+            )
+            part = dot(x, grads, TN).astype(held.dtype)
+            for n, y in enumerate(mine):
+                held[y, peer * step : (peer + 1) * step] = part[n * step : (n + 1) * step]
+        for y in mine:
             slot = jnp.where(core == 0, *(order.index(y) for order in Y_ORDERS))
-            out_ref[slot, peer * step : (peer + 1) * step] = part[y * step : (y + 1) * step]
+            copies.append(pltpu.make_async_copy(held.at[y], out_ref.at[slot], done.at[y]))
+            copies[-1].start()
+    for copy in copies:
+        copy.wait()
 
 
 def weight(mine, other, x, ys):
     peers, tokens, part = x.shape[0] // 2, x.shape[1], x.shape[2]
-    shape = jax.ShapeDtypeStruct((ys, peers * part // ys, mine.shape[1]), jnp.bfloat16)
-    flops = 4 * tokens * peers * part * mine.shape[1]
-    return call(weight_kernel, flops, shape, mine, other, x)
+    shape = (ys, peers * part // ys, mine.shape[1])
+    vmem = pl.BlockSpec(memory_space=pltpu.VMEM)
+    return pl.pallas_call(
+        weight_kernel,
+        out_shape=jax.ShapeDtypeStruct(shape, jnp.bfloat16),
+        in_specs=[vmem] * 3,
+        out_specs=pl.BlockSpec(memory_space=pltpu.HBM),
+        scratch_shapes=[pltpu.VMEM(shape, jnp.bfloat16), pltpu.SemaphoreType.DMA((ys,))],
+        cost_estimate=pl.CostEstimate(
+            flops=4 * tokens * peers * part * mine.shape[1], bytes_accessed=10**6, transcendentals=0
+        ),
+        compiler_params=pltpu.CompilerParams(vmem_limit_bytes=VMEM_LIMIT),
+        name="weight",
+    )(mine, other, x)
 
 
 def sum_kernel(order, tiles_ref, out_ref):
@@ -309,9 +353,8 @@
     far = [near, *steps, traded, fetched, passed]
     sent = spread(layer_input, out_rows, ys, cores, peers)
     whole_input = exchanged(sent, ("c", "x"))
-    grads, own, *back = attention(
-        distances, chosen.T, queries, grad_out, attn_out, log_sum.T, key_pair, far
-    )
+    *staged, grad_own = attend_own(queries, grad_out, attn_out, log_sum.T, key_pair)
+    grads, *back = attend_far(distances, chosen.T, *staged, far)
     route = [(i, cores - 1 - i) for i in range(cores)]
     other = lax.ppermute(grads, "c", route)
     parts = weight(grads, other, whole_input, ys)
@@ -325,7 +368,7 @@
     returned.append(shifted(back[-1], KV, -distances[-1]))
     over_y = summed(over_y.reshape(ys, -1, out_rows, over_y.shape[2]), jnp.bfloat16, Z_ORDER)
     over_z = exchanged(over_y, "z", [list(Z_ORDER)])
-    grad_queries, grad_keys, grad_values = collect(grads, own, returned)
+    grad_queries, grad_keys, grad_values = collect(grads, grad_own, returned)
     grad_weight = summed(over_z, jnp.float32)
     return (grad_queries, grad_keys.T, grad_values.T, grad_weight)
 

time: 113 us -> 108 us (0.956)
  waiting for transfers between devices: 26 us -> 22.6 us
  blocking collectives: 21.6 us -> 20 us
    ppermute x3, waiting for transfers between devices: 6.52 us -> 4.36 us  [between(): return lax.ppermute(block, 'z', route)]
    all_to_all x1, blocking collectives: 21.6 us -> 20 us  [exchanged(): lax.all_to_all(tiles, axis, split_axis=0, concat_axis=0, tiled=True, axis...]
    pallas_call x0 -> x1, Pallas kernels: none -> 1.46 us  [weight(): pl.pallas_call(weight_kernel, out_shape=jax.ShapeDtypeStruct(shape, jnp.b...]
    ppermute x10, waiting for transfers between devices: 18.6 us -> 17.2 us  [shifted(): return lax.ppermute(block, axis, route)]
  transfers between devices with their start and end apart: 16 -> 16, of which waited for: 5 -> 6; matrix products, arithmetic and copies ran while one was open for 0% -> 0% of each run, Pallas kernels for 3% -> 3%
where the time goes in v6:
time: 108 us
  starting transfers between devices  55.7 us (52%)
  waiting for transfers between devices  22.6 us (21%)
  blocking collectives  20 us (19%)
  Pallas kernels  7.46 us (7%)
    all_to_all x2, starting transfers between devices, exchanged(): lax.all_to_all(tiles, axis, split_axis=0, concat_axis=0, tiled=True, axis...  32.3 us
    all_to_all x1, blocking collectives, exchanged(): lax.all_to_all(tiles, axis, split_axis=0, concat_axis=0, tiled=True, axis...  20 us
    ppermute x10, waiting for transfers between devices, shifted(): return lax.ppermute(block, axis, route)  17.2 us
    ppermute x10, starting transfers between devices, shifted(): return lax.ppermute(block, axis, route)  13 us
    ppermute x3, starting transfers between devices, between(): return lax.ppermute(block, 'z', route)  8.21 us
    pallas_call x6, Pallas kernels, call(): pl.pallas_call(kernel, out_shape=out_shape, in_specs=[pl.BlockSpec(memory...  4.67 us
    ppermute x3, waiting for transfers between devices, between(): return lax.ppermute(block, 'z', route)  4.36 us
    ppermute x1, starting transfers between devices, shards(): other = lax.ppermute(grads, 'c', route)  2.22 us
  transfers between devices with their start and end apart: 16, of which 6 were waited for; matrix products, arithmetic and copies ran while one was open for 0% of the time, Pallas kernels for 3%

profile of v6, /device:TPU:6, one launch (start us, length us, event | category | flops | bytes accessed | tf_op | source)
XLA Modules:
  0.0 107.7 jit_solution(150751058541595361)
XLA Ops:
  0.6 0.9 copy-done
  1.6 1.3 %spread.1 = bf16[8,192,256]{2,1,0:T(8,128)(2,1)} custom-call(bf16[192,512]{1,0:T(8,128)(2,1)S(1)} %copy-done), custom_call_target="tpu_custom_call" | custom-call | flops 100663296 | bytes 1000000 | tf_op jit(solution)/shard_map/spread/pallas_call | solution.py:102
  2.9 16.6 %all-to-all-start = ((bf16[8,192,256]{2,1,0:T(8,128)(2,1)}), bf16[8,192,256]{2,1,0:T(8,128)(2,1)S(1)}, u32[]{:S(2)}, u32[]{:S(2)}) async-start(bf16[8,192,256]{2,1,0:T(8,128)(2,1)} %spread.1), calls=%async_computation | async-start | bytes 1572864 | tf_op jit(solution)/shard_map/all_to_all | solution.py:39
  19.6 0.1 shard_map.111.kv_ref
  19.7 2.1 %collective-permute-start.3 = (bf16[192,128]{1,0:T(8,128)(2,1)S(1)}, bf16[192,128]{1,0:T(8,128)(2,1)S(1)}, u32[]{:S(2)}, u32[]{:S(2)}) collective-permute-start(bf16[192,128]{1,0:T(8,128)(2,1)S(1)} %shard_map.111.kv_ref), channel_id=1, source_target_pairs={{0,256},{64,320},{128,384},{192,448},{256,0},{320,64},{384,128},{4... | collective-permute-start | bytes 147464 | tf_op jit(solution)/shard_map/ppermute | solution.py:35
  21.7 2.0 %collective-permute-start = (bf16[192,128]{1,0:T(8,128)(2,1)S(1)}, bf16[192,128]{1,0:T(8,128)(2,1)S(1)}, u32[]{:S(2)}, u32[]{:S(2)}) collective-permute-start(bf16[192,128]{1,0:T(8,128)(2,1)S(1)} %shard_map.111.kv_ref), channel_id=1, source_target_pairs={{0,4},{4,8},{8,12},{12,16},{16,20},{20,24},{24,28},{28,32},{32,36}... | collective-permute-start | bytes 147464 | tf_op jit(solution)/shard_map/ppermute | solution.py:30
  23.8 3.2 %collective-permute-start.1 = (bf16[192,128]{1,0:T(8,128)(2,1)S(1)}, bf16[192,128]{1,0:T(8,128)(2,1)S(1)}, u32[]{:S(2)}, u32[]{:S(2)}) collective-permute-start(bf16[192,128]{1,0:T(8,128)(2,1)S(1)} %shard_map.111.kv_ref), channel_id=1, source_target_pairs={{0,128},{4,132},{8,136},{12,140},{16,144},{20,148},{24,152},{28,15... | collective-permute-start | bytes 147464 | tf_op jit(solution)/shard_map/ppermute | solution.py:30
  27.0 0.7 collective-permute-start.2
  27.6 0.7 collective-permute-start.4
  28.3 1.4 %collective-permute-done.3.refs_3_ = bf16[192,128]{1,0:T(8,128)(2,1)S(1)} collective-permute-done((bf16[192,128]{1,0:T(8,128)(2,1)S(1)}, bf16[192,128]{1,0:T(8,128)(2,1)S(1)}, u32[]{:S(2)}, u32[]{:S(2)}) %collective-permute-start.3) | collective-permute-done | bytes 49184 | tf_op jit(solution)/shard_map/ppermute | solution.py:35
  29.7 5.5 %collective-permute-start.5 = (bf16[192,128]{1,0:T(8,128)(2,1)S(1)}, bf16[192,128]{1,0:T(8,128)(2,1)S(1)}, u32[]{:S(2)}, u32[]{:S(2)}) collective-permute-start(bf16[192,128]{1,0:T(8,128)(2,1)S(1)} %collective-permute-done.3.refs_3_), channel_id=1, source_target_pairs={{256,512},{320,576},{384,640},{448,704},{0,768},{64,832},{128,896}... | collective-permute-start | bytes 147464 | tf_op jit(solution)/shard_map/ppermute | solution.py:35
  35.2 1.0 shard_map.112
  36.3 3.0 %collective-permute-done.5.refs_5_ = bf16[192,128]{1,0:T(8,128)(2,1)S(1)} collective-permute-done((bf16[192,128]{1,0:T(8,128)(2,1)S(1)}, bf16[192,128]{1,0:T(8,128)(2,1)S(1)}, u32[]{:S(2)}, u32[]{:S(2)}) %collective-permute-start.5) | collective-permute-done | bytes 49184 | tf_op jit(solution)/shard_map/ppermute | solution.py:35
  39.3 1.5 %shard_map.113 = (bf16[192,256]{1,0:T(8,128)(2,1)S(1)}, bf16[192,128]{1,0:T(8,128)(2,1)S(1)}, bf16[192,128]{1,0:T(8,128)(2,1)S(1)}, bf16[192,128]{1,0:T(8,128)(2,1)S(1)}, bf16[192,128]{1,0:T(8,128)(2,1)S(1)}) custom-call(s32[8,768]{1,0:T(8,128)S(1)} %bitcast.8, bf16[3,256,128]{2,1,0:T(8,128)(2,1)S(1)} %get-tuple-element.17.low_ref, ...), custom_call_target="tpu_custom_call" | custom-call | flops 2000000000 | bytes 1112064 | tf_op jit(solution)/shard_map/pallas_call | solution.py:52
  40.8 2.2 %collective-permute-start.13 = (bf16[192,256]{1,0:T(8,128)(2,1)S(1)}, bf16[192,256]{1,0:T(8,128)(2,1)S(1)}, u32[]{:S(2)}, u32[]{:S(2)}) collective-permute-start(bf16[192,256]{1,0:T(8,128)(2,1)S(1)} %get-tuple-element.21.grads_ref.mine_ref), channel_id=1, source_target_pairs={{0,4},{4,0},{1,5},{5,1},{2,6},{6,2},{3,7},{7,3},{8,12},{12,8},{9,1... | collective-permute-start | bytes 294920 | tf_op jit(solution)/shard_map/ppermute | solution.py:359
  43.0 1.0 collective-permute-done.13.other_ref
  44.0 1.5 %weight.1 = bf16[8,128,256]{2,1,0:T(8,128)(2,1)S(1)} custom-call(bf16[192,256]{1,0:T(8,128)(2,1)S(1)} %get-tuple-element.21.grads_ref.mine_ref, bf16[192,256]{1,0:T(8,128)(2,1)S(1)} %collective-permute-done.13.other_ref, bf16[8,192,256]{2,1,0:T(8,128)(2,1)S(1)} %all-to-all-done.x_ref), custom_call_target="tpu_custom_call" | custom-call | flops 201326592 | bytes 1000000 | tf_op jit(solution)/shard_map/weight/pallas_call | solution.py:288
  45.5 20.0 %all_to_all.15 = bf16[8,128,256]{2,1,0:T(8,128)(2,1)S(1)} all-to-all(bf16[8,128,256]{2,1,0:T(8,128)(2,1)S(1)} %weight.1), channel_id=1, replica_groups={{24,16,8,0,56,48,40,32},{44,52,60,4,12,20,28,36},{25,17,9,1,57,49,41,33..., dimensions={0} | all-to-all | bytes 1048576 | tf_op jit(solution)/shard_map/all_to_all | solution.py:39
  65.5 0.7 shard_map.115
  66.2 15.7 %all-to-all-start.2 = ((bf16[16,8,256]{2,1,0:T(8,128)(2,1)}), bf16[16,8,256]{2,1,0:T(8,128)(2,1)S(1)}, u32[]{:S(2)}, u32[]{:S(2)}) async-start(bf16[16,8,256]{2,1,0:T(8,128)(2,1)} %shard_map.115), calls=%async_computation.2 | async-start | bytes 131072 | tf_op jit(solution)/shard_map/all_to_all | solution.py:39
  81.9 1.3 %collective-permute-start.6 = (bf16[192,128]{1,0:T(8,128)(2,1)S(1)}, bf16[192,128]{1,0:T(8,128)(2,1)S(1)}, u32[]{:S(2)}, u32[]{:S(2)}) collective-permute-start(bf16[192,128]{1,0:T(8,128)(2,1)S(1)} %get-tuple-element.23), channel_id=1, source_target_pairs={{4,0},{8,4},{12,8},{16,12},{20,16},{24,20},{28,24},{32,28},{36,32}... | collective-permute-start | bytes 147464 | tf_op jit(solution)/shard_map/ppermute | solution.py:30
  83.2 0.7 collective-permute-start.7
  83.8 1.3 %collective-permute-start.8 = (bf16[192,128]{1,0:T(8,128)(2,1)S(1)}, bf16[192,128]{1,0:T(8,128)(2,1)S(1)}, u32[]{:S(2)}, u32[]{:S(2)}) collective-permute-start(bf16[192,128]{1,0:T(8,128)(2,1)S(1)} %get-tuple-element.24), channel_id=1, source_target_pairs={{128,0},{132,4},{136,8},{140,12},{144,16},{148,20},{152,24},{156,2... | collective-permute-start | bytes 147464 | tf_op jit(solution)/shard_map/ppermute | solution.py:30
  85.1 0.7 collective-permute-start.9
  85.8 1.3 %collective-permute-start.10 = (bf16[192,128]{1,0:T(8,128)(2,1)S(1)}, bf16[192,128]{1,0:T(8,128)(2,1)S(1)}, u32[]{:S(2)}, u32[]{:S(2)}) collective-permute-start(bf16[192,128]{1,0:T(8,128)(2,1)S(1)} %get-tuple-element.25), channel_id=1, source_target_pairs={{256,0},{260,4},{264,8},{268,12},{272,16},{276,20},{280,24},{284,2... | collective-permute-start | bytes 147464 | tf_op jit(solution)/shard_map/ppermute | solution.py:30
  87.1 0.7 collective-permute-start.11
  87.8 1.3 %collective-permute-start.12 = (bf16[192,128]{1,0:T(8,128)(2,1)S(1)}, bf16[192,128]{1,0:T(8,128)(2,1)S(1)}, u32[]{:S(2)}, u32[]{:S(2)}) collective-permute-start(bf16[192,128]{1,0:T(8,128)(2,1)S(1)} %get-tuple-element.26), channel_id=1, source_target_pairs={{512,0},{516,4},{520,8},{524,12},{528,16},{532,20},{536,24},{540,2... | collective-permute-start | bytes 147464 | tf_op jit(solution)/shard_map/ppermute | solution.py:30
  89.1 3.0 %collective-permute-done.8.refs_2_ = bf16[192,128]{1,0:T(8,128)(2,1)S(1)} collective-permute-done((bf16[192,128]{1,0:T(8,128)(2,1)S(1)}, bf16[192,128]{1,0:T(8,128)(2,1)S(1)}, u32[]{:S(2)}, u32[]{:S(2)}) %collective-permute-start.8) | collective-permute-done | bytes 49184 | tf_op jit(solution)/shard_map/ppermute | solution.py:30
  92.1 7.8 %collective-permute-done.10.refs_4_ = bf16[192,128]{1,0:T(8,128)(2,1)S(1)} collective-permute-done((bf16[192,128]{1,0:T(8,128)(2,1)S(1)}, bf16[192,128]{1,0:T(8,128)(2,1)S(1)}, u32[]{:S(2)}, u32[]{:S(2)}) %collective-permute-start.10) | collective-permute-done | bytes 49184 | tf_op jit(solution)/shard_map/ppermute | solution.py:30
  99.9 6.4 %collective-permute-done.12.refs_6_ = bf16[192,128]{1,0:T(8,128)(2,1)S(1)} collective-permute-done((bf16[192,128]{1,0:T(8,128)(2,1)S(1)}, bf16[192,128]{1,0:T(8,128)(2,1)S(1)}, u32[]{:S(2)}, u32[]{:S(2)}) %collective-permute-start.12) | collective-permute-done | bytes 49184 | tf_op jit(solution)/shard_map/ppermute | solution.py:30
  106.3 0.7 shard_map.114
  107.1 0.6 shard_map.116
  (26 shorter events, 0.1 us)
Async XLA Ops:
  0.6 0.9 copy-start
  2.9 16.6 %copy-start.6 = (bf16[192,64]{0,1:T(8,128)(2,1)S(1)}, bf16[192,64]{0,1:T(8,128)(2,1)}, u32[]{:S(2)}) copy-start(bf16[192,64]{0,1:T(8,128)(2,1)} %param.11) | copy-start | bytes 73732
  2.9 16.6 %copy-start.7 = (bf16[192,64]{0,1:T(8,128)(2,1)S(1)}, bf16[192,64]{0,1:T(8,128)(2,1)}, u32[]{:S(2)}) copy-start(bf16[192,64]{0,1:T(8,128)(2,1)} %param.10) | copy-start | bytes 73732
  2.9 41.1 %all-to-all-start = ((bf16[8,192,256]{2,1,0:T(8,128)(2,1)}), bf16[8,192,256]{2,1,0:T(8,128)(2,1)S(1)}, u32[]{:S(2)}, u32[]{:S(2)}) async-start(bf16[8,192,256]{2,1,0:T(8,128)(2,1)} %spread.1), calls=%async_computation | async-start | bytes 1572864 | tf_op jit(solution)/shard_map/all_to_all | solution.py:39
  19.5 15.7 %copy-start.1 = (bf16[192,256]{1,0:T(8,128)(2,1)S(1)}, bf16[192,256]{1,0:T(8,128)(2,1)}, u32[]{:S(2)}) copy-start(bf16[192,256]{1,0:T(8,128)(2,1)} %q_ref.1) | copy-start | bytes 294916
  19.5 15.7 %copy-start.2 = (bf16[192,256]{1,0:T(8,128)(2,1)S(1)}, bf16[192,256]{1,0:T(8,128)(2,1)}, u32[]{:S(2)}) copy-start(bf16[192,256]{1,0:T(8,128)(2,1)} %go_ref.1) | copy-start | bytes 294916
  19.5 15.7 %copy-start.3 = (bf16[192,256]{1,0:T(8,128)(2,1)S(1)}, bf16[192,256]{1,0:T(8,128)(2,1)}, u32[]{:S(2)}) copy-start(bf16[192,256]{1,0:T(8,128)(2,1)} %ao_ref.1) | copy-start | bytes 294916
  19.6 15.7 %copy-start.5 = (f32[192,4]{0,1:T(4,128)S(1)}, f32[192,4]{0,1:T(4,128)}, u32[]{:S(2)}) copy-start(f32[192,4]{0,1:T(4,128)} %param.14) | copy-start | bytes 9220
  19.7 10.0 %collective-permute-start.3 = (bf16[192,128]{1,0:T(8,128)(2,1)S(1)}, bf16[192,128]{1,0:T(8,128)(2,1)S(1)}, u32[]{:S(2)}, u32[]{:S(2)}) collective-permute-start(bf16[192,128]{1,0:T(8,128)(2,1)S(1)} %shard_map.111.kv_ref), channel_id=1, source_target_pairs={{0,256},{64,320},{128,384},{192,448},{256,0},{320,64},{384,128},{4... | collective-permute-start | bytes 147464 | tf_op jit(solution)/shard_map/ppermute | solution.py:35
  21.7 14.5 %collective-permute-start = (bf16[192,128]{1,0:T(8,128)(2,1)S(1)}, bf16[192,128]{1,0:T(8,128)(2,1)S(1)}, u32[]{:S(2)}, u32[]{:S(2)}) collective-permute-start(bf16[192,128]{1,0:T(8,128)(2,1)S(1)} %shard_map.111.kv_ref), channel_id=1, source_target_pairs={{0,4},{4,8},{8,12},{12,16},{16,20},{20,24},{24,28},{28,32},{32,36}... | collective-permute-start | bytes 147464 | tf_op jit(solution)/shard_map/ppermute | solution.py:30
  23.8 12.5 %collective-permute-start.1 = (bf16[192,128]{1,0:T(8,128)(2,1)S(1)}, bf16[192,128]{1,0:T(8,128)(2,1)S(1)}, u32[]{:S(2)}, u32[]{:S(2)}) collective-permute-start(bf16[192,128]{1,0:T(8,128)(2,1)S(1)} %shard_map.111.kv_ref), channel_id=1, source_target_pairs={{0,128},{4,132},{8,136},{12,140},{16,144},{20,148},{24,152},{28,15... | collective-permute-start | bytes 147464 | tf_op jit(solution)/shard_map/ppermute | solution.py:30
  27.0 9.3 %collective-permute-start.2 = (bf16[192,128]{1,0:T(8,128)(2,1)S(1)}, bf16[192,128]{1,0:T(8,128)(2,1)S(1)}, u32[]{:S(2)}, u32[]{:S(2)}) collective-permute-start(bf16[192,128]{1,0:T(8,128)(2,1)S(1)} %shard_map.111.kv_ref), channel_id=1, source_target_pairs={{512,640},{516,644},{520,648},{524,652},{528,656},{532,660},{536,6... | collective-permute-start | bytes 147464 | tf_op jit(solution)/shard_map/ppermute | solution.py:30
  27.6 8.6 %collective-permute-start.4 = (bf16[192,128]{1,0:T(8,128)(2,1)S(1)}, bf16[192,128]{1,0:T(8,128)(2,1)S(1)}, u32[]{:S(2)}, u32[]{:S(2)}) collective-permute-start(bf16[192,128]{1,0:T(8,128)(2,1)S(1)} %shard_map.111.kv_ref), channel_id=1, source_target_pairs={{256,512},{320,576},{384,640},{448,704},{512,768},{576,832},{640,8... | collective-permute-start | bytes 147464 | tf_op jit(solution)/shard_map/ppermute | solution.py:35
  29.7 9.6 %collective-permute-start.5 = (bf16[192,128]{1,0:T(8,128)(2,1)S(1)}, bf16[192,128]{1,0:T(8,128)(2,1)S(1)}, u32[]{:S(2)}, u32[]{:S(2)}) collective-permute-start(bf16[192,128]{1,0:T(8,128)(2,1)S(1)} %collective-permute-done.3.refs_3_), channel_id=1, source_target_pairs={{256,512},{320,576},{384,640},{448,704},{0,768},{64,832},{128,896}... | collective-permute-start | bytes 147464 | tf_op jit(solution)/shard_map/ppermute | solution.py:35
  35.2 4.0 %copy-start.4 = (s32[768,8]{0,1:T(8,128)S(1)}, s32[768,8]{0,1:T(8,128)}, u32[]{:S(2)}) copy-start(s32[768,8]{0,1:T(8,128)} %param.15) | copy-start | bytes 73732
  40.8 3.2 %collective-permute-start.13 = (bf16[192,256]{1,0:T(8,128)(2,1)S(1)}, bf16[192,256]{1,0:T(8,128)(2,1)S(1)}, u32[]{:S(2)}, u32[]{:S(2)}) collective-permute-start(bf16[192,256]{1,0:T(8,128)(2,1)S(1)} %get-tuple-element.21.grads_ref.mine_ref), channel_id=1, source_target_pairs={{0,4},{4,0},{1,5},{5,1},{2,6},{6,2},{3,7},{7,3},{8,12},{12,8},{9,1... | collective-permute-start | bytes 294920 | tf_op jit(solution)/shard_map/ppermute | solution.py:359
  66.2 40.9 %all-to-all-start.2 = ((bf16[16,8,256]{2,1,0:T(8,128)(2,1)}), bf16[16,8,256]{2,1,0:T(8,128)(2,1)S(1)}, u32[]{:S(2)}, u32[]{:S(2)}) async-start(bf16[16,8,256]{2,1,0:T(8,128)(2,1)} %shard_map.115), calls=%async_computation.2 | async-start | bytes 131072 | tf_op jit(solution)/shard_map/all_to_all | solution.py:39
  81.9 5.2 %collective-permute-start.6 = (bf16[192,128]{1,0:T(8,128)(2,1)S(1)}, bf16[192,128]{1,0:T(8,128)(2,1)S(1)}, u32[]{:S(2)}, u32[]{:S(2)}) collective-permute-start(bf16[192,128]{1,0:T(8,128)(2,1)S(1)} %get-tuple-element.23), channel_id=1, source_target_pairs={{4,0},{8,4},{12,8},{16,12},{20,16},{24,20},{28,24},{32,28},{36,32}... | collective-permute-start | bytes 147464 | tf_op jit(solution)/shard_map/ppermute | solution.py:30
  83.2 4.6 %collective-permute-start.7 = (bf16[192,128]{1,0:T(8,128)(2,1)S(1)}, bf16[192,128]{1,0:T(8,128)(2,1)S(1)}, u32[]{:S(2)}, u32[]{:S(2)}) collective-permute-start(bf16[192,128]{1,0:T(8,128)(2,1)S(1)} %get-tuple-element.23), channel_id=1, source_target_pairs={{516,512},{520,516},{524,520},{528,524},{532,528},{536,532},{540,5... | collective-permute-start | bytes 147464 | tf_op jit(solution)/shard_map/ppermute | solution.py:30
  83.8 8.3 %collective-permute-start.8 = (bf16[192,128]{1,0:T(8,128)(2,1)S(1)}, bf16[192,128]{1,0:T(8,128)(2,1)S(1)}, u32[]{:S(2)}, u32[]{:S(2)}) collective-permute-start(bf16[192,128]{1,0:T(8,128)(2,1)S(1)} %get-tuple-element.24), channel_id=1, source_target_pairs={{128,0},{132,4},{136,8},{140,12},{144,16},{148,20},{152,24},{156,2... | collective-permute-start | bytes 147464 | tf_op jit(solution)/shard_map/ppermute | solution.py:30
  85.1 7.0 %collective-permute-start.9 = (bf16[192,128]{1,0:T(8,128)(2,1)S(1)}, bf16[192,128]{1,0:T(8,128)(2,1)S(1)}, u32[]{:S(2)}, u32[]{:S(2)}) collective-permute-start(bf16[192,128]{1,0:T(8,128)(2,1)S(1)} %get-tuple-element.24), channel_id=1, source_target_pairs={{640,512},{644,516},{648,520},{652,524},{656,528},{660,532},{664,5... | collective-permute-start | bytes 147464 | tf_op jit(solution)/shard_map/ppermute | solution.py:30
  85.8 14.1 %collective-permute-start.10 = (bf16[192,128]{1,0:T(8,128)(2,1)S(1)}, bf16[192,128]{1,0:T(8,128)(2,1)S(1)}, u32[]{:S(2)}, u32[]{:S(2)}) collective-permute-start(bf16[192,128]{1,0:T(8,128)(2,1)S(1)} %get-tuple-element.25), channel_id=1, source_target_pairs={{256,0},{260,4},{264,8},{268,12},{272,16},{276,20},{280,24},{284,2... | collective-permute-start | bytes 147464 | tf_op jit(solution)/shard_map/ppermute | solution.py:30
  87.1 12.8 %collective-permute-start.11 = (bf16[192,128]{1,0:T(8,128)(2,1)S(1)}, bf16[192,128]{1,0:T(8,128)(2,1)S(1)}, u32[]{:S(2)}, u32[]{:S(2)}) collective-permute-start(bf16[192,128]{1,0:T(8,128)(2,1)S(1)} %get-tuple-element.25), channel_id=1, source_target_pairs={{768,512},{772,516},{776,520},{780,524},{784,528},{788,532},{792,5... | collective-permute-start | bytes 147464 | tf_op jit(solution)/shard_map/ppermute | solution.py:30
  87.8 18.5 %collective-permute-start.12 = (bf16[192,128]{1,0:T(8,128)(2,1)S(1)}, bf16[192,128]{1,0:T(8,128)(2,1)S(1)}, u32[]{:S(2)}, u32[]{:S(2)}) collective-permute-start(bf16[192,128]{1,0:T(8,128)(2,1)S(1)} %get-tuple-element.26), channel_id=1, source_target_pairs={{512,0},{516,4},{520,8},{524,12},{528,16},{532,20},{536,24},{540,2... | collective-permute-start | bytes 147464 | tf_op jit(solution)/shard_map/ppermute | solution.py:30

commit v7 on v6

--- a/solution.py
+++ b/solution.py
@@ -18,6 +18,7 @@
 TN = (((0,), (0,)), ((), ()))
 Y_ORDERS = ((3, 2, 1, 0, 7, 6, 5, 4), (5, 6, 7, 0, 1, 2, 3, 4))
 Z_ORDER = (8, 9, 10, 11, 12, 13, 14, 15, 0, 1, 2, 3, 4, 5, 6, 7)
+X_ORDER = (4, 5, 6, 7, 0, 1, 2, 3)
 LANES = 128
 WINDOWS = 2
 VMEM_LIMIT = 16 * 2**20
@@ -89,7 +90,7 @@
         move = jnp.where(place == target + core * part, 1.0, 0.0).astype(jnp.bfloat16)
         held[core] = dot(x_ref[...], move).astype(jnp.bfloat16)
         for peer in range(peers):
-            slot = core * peers + peer
+            slot = X_ORDER.index(core * peers + peer)
             copies.append(pltpu.make_async_copy(held.at[core], out_ref.at[slot], done.at[slot]))
             copies[-1].start()
     for copy in copies:
@@ -180,13 +181,7 @@
     return call(own_kernel, 10**9, shape, q, go, ao, lse, kv)
 
 
-def far_kernel(distances, chosen_ref, low_ref, high_ref, rows_ref, part_ref, *refs):
-    one_ref, *step_refs, traded_ref, fetched_ref, passed_ref = refs[: LEVELS + 2]
-    gq_ref = refs[LEVELS + 2]
-    back_refs = refs[LEVELS + 3 : 2 * LEVELS + 3]
-    sums, two_ref, four_ref = refs[2 * LEVELS + 3 :]
-    blocks = low_ref.shape[0]
-    heads = low_ref.shape[1] // BLOCK
+def chosen_places(chosen_ref, distances, levels, blocks):
     me = lax.axis_index(KV)
     first = me * blocks
     start = jnp.minimum(first // LANES * LANES, chosen_ref.shape[1] - LANES * WINDOWS)
@@ -197,30 +192,66 @@
         for b in range(blocks):
             here = columns == first + b - start - window * LANES
             picked[b] = picked[b] + jnp.where(here, tile, 0)
-    picked = [jnp.sum(tile.astype(jnp.float32), axis=1, keepdims=True).astype(jnp.int32) for tile in picked]
+    places = []
+    for tile in picked:
+        column = jnp.sum(tile.astype(jnp.float32), axis=1, keepdims=True).astype(jnp.int32)
+        row = {}
+        for level in levels:
+            for n in range(PER):
+                block = column[level * PER + n, 0]
+                block = jnp.where(block >= 0, block - (me - distances[level]) * blocks, 0)
+                row[level, n] = pl.ds(pl.multiple_of(block * BLOCK, BLOCK), BLOCK)
+        places.append(row)
+    return places
+
+
+def far_terms(places, far_refs, low_ref, high_ref, rows_ref, sums, b):
+    kv = jnp.concatenate([far_refs[level][at, :] for (level, _), at in places.items()], axis=0)
+    grad_q, grad_kv = terms(kv, low_ref[b], high_ref[b], rows_ref[b, :1], rows_ref[b, 1:])
+    for n, ((level, _), at) in enumerate(places.items()):
+        sums[level][at, :] += grad_kv[n * BLOCK : (n + 1) * BLOCK]
+    return grad_q
+
+
+def far_kernel(distances, chosen_ref, low_ref, high_ref, rows_ref, part_ref, *refs):
+    *step_refs, traded_ref, fetched_ref, passed_ref, out_ref = refs[:6]
+    back_refs, (two_ref, four_ref) = refs[6 : 5 + LEVELS], refs[-2:]
+    sums = dict(zip(range(1, LEVELS), refs[5 + LEVELS : -2]))
     at, quarter = lax.axis_index("z"), lax.axis_size("z") // 4
     in_second = jnp.logical_and(at >= quarter, at < 2 * quarter)
-    is_late = me - distances[1] >= lax.axis_size(KV) // 2
+    is_late = lax.axis_index(KV) - distances[1] >= lax.axis_size(KV) // 2
     two_ref[...] = jnp.where(is_late, step_refs[1][...], step_refs[0][...])
     four_ref[...] = jnp.where(in_second, traded_ref[...], fetched_ref[...])
-    far_refs = (one_ref, two_ref, four_ref, passed_ref)
+    far_refs = {1: two_ref, 2: four_ref, 3: passed_ref}
+    for level in sums:
+        sums[level][...] = jnp.zeros_like(sums[level])
+    blocks = low_ref.shape[0]
+    places = chosen_places(chosen_ref, distances, tuple(sums), blocks)
+    for b in range(blocks):
+        grad_q = far_terms(places[b], far_refs, low_ref, high_ref, rows_ref, sums, b)
+        out_ref[b] = part_ref[b] + grad_q
+    for level, back_ref in zip(sums, back_refs):
+        back_ref[...] = sums[level][...].astype(back_ref.dtype)
+
+
+def attend_far(distances, chosen, low, high, rows, part, far):
+    kv = far[0]
+    shape = (jax.ShapeDtypeStruct(part.shape, part.dtype),)
+    shape += (jax.ShapeDtypeStruct(kv.shape, jnp.bfloat16),) * (LEVELS - 1)
+    scratch = [pltpu.VMEM(kv.shape, jnp.float32)] * (LEVELS - 1) + [pltpu.VMEM(kv.shape, kv.dtype)] * 2
+    kernel = functools.partial(far_kernel, distances)
+    args = (chosen, low, high, rows, part, *far)
+    return call(kernel, 2 * 10**9, shape, *args, scratch=scratch)
+
+
+def near_kernel(distances, chosen_ref, low_ref, high_ref, rows_ref, part_ref, one_ref, gq_ref, back_ref, total):
+    blocks, heads = low_ref.shape[0], low_ref.shape[1] // BLOCK
     lane = lax.broadcasted_iota(jnp.int32, (BLOCK, 2 * DH), 1)
-    sums[...] = jnp.zeros_like(sums)
+    total[...] = jnp.zeros_like(total)
+    places = chosen_places(chosen_ref, distances, (0,), blocks)
     for b in range(blocks):
         rows = slice(b * BLOCK, (b + 1) * BLOCK)
-        places = []
-        for n in range(LEVELS * PER):
-            block = picked[b][n, 0]
-            block = jnp.where(block >= 0, block - (me - distances[n // PER]) * blocks, 0)
-            places.append(pl.ds(pl.multiple_of(block * BLOCK, BLOCK), BLOCK))
-        kv = jnp.concatenate(
-            [far_refs[n // PER][places[n], :] for n in range(LEVELS * PER)], axis=0
-        )
-        grad_q, grad_kv = terms(
-            kv, low_ref[b], high_ref[b], rows_ref[b, :1], rows_ref[b, 1:]
-        )
-        for n in range(LEVELS * PER):
-            sums[n // PER, places[n], :] += grad_kv[n * BLOCK : (n + 1) * BLOCK]
+        grad_q = far_terms(places[b], {0: one_ref}, low_ref, high_ref, rows_ref, {0: total}, b)
         grad_q = (part_ref[b] + grad_q) * DH ** (-0.5)
         for pair in range(heads // 2):
             first = grad_q[2 * pair * BLOCK : (2 * pair + 1) * BLOCK]
@@ -228,31 +259,18 @@
             gq_ref[rows, pair * 2 * DH : (pair + 1) * 2 * DH] = jnp.where(
                 lane < DH, first, pltpu.roll(second, DH, 1)
             ).astype(gq_ref.dtype)
-    for level in range(LEVELS):
-        back_refs[level][...] = sums[level].astype(jnp.bfloat16)
-
-
-def attend_far(distances, chosen, low, high, rows, part, far):
+    back_ref[...] = total[...].astype(back_ref.dtype)
+
+
+def attend_near(distances, chosen, low, high, rows, part, near):
     tokens, width = low.shape[0] * BLOCK, low.shape[1] * DH // BLOCK
-    kv = far[0]
-    shape = (jax.ShapeDtypeStruct((tokens, width), jnp.bfloat16),)
-    shape += (jax.ShapeDtypeStruct(kv.shape, jnp.bfloat16),) * LEVELS
-    return call(
-        functools.partial(far_kernel, distances),
-        2 * 10**9,
-        shape,
-        chosen,
-        low,
-        high,
-        rows,
-        part,
-        *far,
-        scratch=[
-            pltpu.VMEM((LEVELS, *kv.shape), jnp.float32),
-            pltpu.VMEM(kv.shape, kv.dtype),
-            pltpu.VMEM(kv.shape, kv.dtype),
-        ],
+    shape = (
+        jax.ShapeDtypeStruct((tokens, width), jnp.bfloat16),
+        jax.ShapeDtypeStruct(near.shape, jnp.bfloat16),
     )
+    kernel = functools.partial(near_kernel, distances)
+    args = (chosen, low, high, rows, part, near)
+    return call(kernel, 10**9, shape, *args, scratch=[pltpu.VMEM(near.shape, jnp.float32)])
 
 
 def weight_kernel(mine_ref, other_ref, x_ref, out_ref, held, done):
@@ -266,10 +284,9 @@
         mine = range(half * ys // 2, (half + 1) * ys // 2)
         lanes = slice(mine[0] * step, (mine[-1] + 1) * step)
         for peer in range(peers):
-            x = jnp.concatenate(
-                [x_ref[core * peers + peer, :, lanes], x_ref[(1 - core) * peers + peer, :, lanes]],
-                axis=0,
-            )
+            slots = [X_ORDER.index(c * peers + peer) for c in range(2)]
+            first, second = jnp.where(core == 0, *slots), jnp.where(core == 0, *slots[::-1])
+            x = jnp.concatenate([x_ref[first, :, lanes], x_ref[second, :, lanes]], axis=0)
             part = dot(x, grads, TN).astype(held.dtype)
             for n, y in enumerate(mine):
                 held[y, peer * step : (peer + 1) * step] = part[n * step : (n + 1) * step]
@@ -350,11 +367,13 @@
     traded = between(key_pair, quarters, ((0, 1), (1, 0)))
     passed = between(traded, quarters, ((1, 2), (0, 3)))
     fetched = between(key_pair, quarters, ((1, 2), (2, 3)))
-    far = [near, *steps, traded, fetched, passed]
+    far = [*steps, traded, fetched, passed]
     sent = spread(layer_input, out_rows, ys, cores, peers)
-    whole_input = exchanged(sent, ("c", "x"))
-    *staged, grad_own = attend_own(queries, grad_out, attn_out, log_sum.T, key_pair)
-    grads, *back = attend_far(distances, chosen.T, *staged, far)
+    whole_input = exchanged(sent, ("c", "x"), [list(X_ORDER)])
+    *staged, part, grad_own = attend_own(queries, grad_out, attn_out, log_sum.T, key_pair)
+    part, *back = attend_far(distances, chosen.T, *staged, part, far)
+    grads, back_near = attend_near(distances, chosen.T, *staged, part, near)
+    back = [back_near, *back]
     route = [(i, cores - 1 - i) for i in range(cores)]
     other = lax.ppermute(grads, "c", route)
     parts = weight(grads, other, whole_input, ys)

time: 108 us -> 107 us (level)
  waiting for transfers between devices: 22.6 us -> 20.1 us
    all_to_all x2, starting transfers between devices: 32.3 us -> 29.4 us  [exchanged(): lax.all_to_all(tiles, axis, split_axis=0, concat_axis=0, tiled=True, axis...]
    ppermute x3, starting transfers between devices: 8.21 us -> 9.9 us  [between(): return lax.ppermute(block, 'z', route)]
    ppermute x10, starting transfers between devices: 13 us -> 14.4 us  [shifted(): return lax.ppermute(block, axis, route)]
    ppermute x3, waiting for transfers between devices: 4.36 us -> 3.05 us  [between(): return lax.ppermute(block, 'z', route)]
    ppermute x10, waiting for transfers between devices: 17.2 us -> 16.1 us  [shifted(): return lax.ppermute(block, axis, route)]
    pallas_call x6 -> x7, Pallas kernels: 4.67 us -> 5.42 us  [call(): pl.pallas_call(kernel, out_shape=out_shape, in_specs=[pl.BlockSpec(memory...]
  transfers between devices with their start and end apart: 16 -> 16, of which waited for: 6 -> 6; matrix products, arithmetic and copies ran while one was open for 0% -> 0% of each run, Pallas kernels for 3% -> 4%
where the time goes in v7:
time: 107 us; the launch traced here: 106 us
  starting transfers between devices  55.9 us (52%)
  waiting for transfers between devices  20.1 us (19%)
  blocking collectives  19.8 us (19%)
  Pallas kernels  8.22 us (8%)
    all_to_all x2, starting transfers between devices, exchanged(): lax.all_to_all(tiles, axis, split_axis=0, concat_axis=0, tiled=True, axis...  29.4 us
    all_to_all x1, blocking collectives, exchanged(): lax.all_to_all(tiles, axis, split_axis=0, concat_axis=0, tiled=True, axis...  19.8 us
    ppermute x10, waiting for transfers between devices, shifted(): return lax.ppermute(block, axis, route)  16.1 us
    ppermute x10, starting transfers between devices, shifted(): return lax.ppermute(block, axis, route)  14.4 us
    ppermute x3, starting transfers between devices, between(): return lax.ppermute(block, 'z', route)  9.9 us
    pallas_call x7, Pallas kernels, call(): pl.pallas_call(kernel, out_shape=out_shape, in_specs=[pl.BlockSpec(memory...  5.42 us
    ppermute x3, waiting for transfers between devices, between(): return lax.ppermute(block, 'z', route)  3.05 us
    ppermute x1, starting transfers between devices, shards(): other = lax.ppermute(grads, 'c', route)  2.27 us
  transfers between devices with their start and end apart: 16, of which 6 were waited for; matrix products, arithmetic and copies ran while one was open for 0% of the time, Pallas kernels for 4%

profile of v7, /device:TPU:6, one launch (start us, length us, event | category | flops | bytes accessed | tf_op | source)
XLA Modules:
  0.0 106.0 jit_solution(14611557909856024437)
XLA Ops:
  0.6 0.9 copy-done
  1.6 1.3 %spread.1 = bf16[8,192,256]{2,1,0:T(8,128)(2,1)} custom-call(bf16[192,512]{1,0:T(8,128)(2,1)S(1)} %copy-done), custom_call_target="tpu_custom_call" | custom-call | flops 100663296 | bytes 1000000 | tf_op jit(solution)/shard_map/spread/pallas_call | solution.py:103
  2.9 14.5 %all-to-all-start = ((bf16[8,192,256]{2,1,0:T(8,128)(2,1)}), bf16[8,192,256]{2,1,0:T(8,128)(2,1)S(1)}, u32[]{:S(2)}, u32[]{:S(2)}) async-start(bf16[8,192,256]{2,1,0:T(8,128)(2,1)} %spread.1), calls=%async_computation | async-start | bytes 1572864 | tf_op jit(solution)/shard_map/all_to_all | solution.py:40
  17.5 0.1 shard_map.111.kv_ref
  17.6 2.1 %collective-permute-start.2 = (bf16[192,128]{1,0:T(8,128)(2,1)S(1)}, bf16[192,128]{1,0:T(8,128)(2,1)S(1)}, u32[]{:S(2)}, u32[]{:S(2)}) collective-permute-start(bf16[192,128]{1,0:T(8,128)(2,1)S(1)} %shard_map.111.kv_ref), channel_id=1, source_target_pairs={{0,256},{64,320},{128,384},{192,448},{256,0},{320,64},{384,128},{4... | collective-permute-start | bytes 147464 | tf_op jit(solution)/shard_map/ppermute | solution.py:36
  19.7 5.1 %collective-permute-start = (bf16[192,128]{1,0:T(8,128)(2,1)S(1)}, bf16[192,128]{1,0:T(8,128)(2,1)S(1)}, u32[]{:S(2)}, u32[]{:S(2)}) collective-permute-start(bf16[192,128]{1,0:T(8,128)(2,1)S(1)} %shard_map.111.kv_ref), channel_id=1, source_target_pairs={{0,128},{4,132},{8,136},{12,140},{16,144},{20,148},{24,152},{28,15... | collective-permute-start | bytes 147464 | tf_op jit(solution)/shard_map/ppermute | solution.py:31
  24.8 0.7 collective-permute-start.1
  25.4 0.7 collective-permute-start.3
  26.1 1.5 %collective-permute-start.5 = (bf16[192,128]{1,0:T(8,128)(2,1)S(1)}, bf16[192,128]{1,0:T(8,128)(2,1)S(1)}, u32[]{:S(2)}, u32[]{:S(2)}) collective-permute-start(bf16[192,128]{1,0:T(8,128)(2,1)S(1)} %shard_map.111.kv_ref), channel_id=1, source_target_pairs={{0,4},{4,8},{8,12},{12,16},{16,20},{20,24},{24,28},{28,32},{32,36}... | collective-permute-start | bytes 147464 | tf_op jit(solution)/shard_map/ppermute | solution.py:31
  27.6 7.2 %collective-permute-start.4 = (bf16[192,128]{1,0:T(8,128)(2,1)S(1)}, bf16[192,128]{1,0:T(8,128)(2,1)S(1)}, u32[]{:S(2)}, u32[]{:S(2)}) collective-permute-start(bf16[192,128]{1,0:T(8,128)(2,1)S(1)} %collective-permute-done.2.refs_2_), channel_id=1, source_target_pairs={{256,512},{320,576},{384,640},{448,704},{0,768},{64,832},{128,896}... | collective-permute-start | bytes 147464 | tf_op jit(solution)/shard_map/ppermute | solution.py:36
  34.9 1.0 shard_map.112
  35.9 3.0 %collective-permute-done.4.refs_4_ = bf16[192,128]{1,0:T(8,128)(2,1)S(1)} collective-permute-done((bf16[192,128]{1,0:T(8,128)(2,1)S(1)}, bf16[192,128]{1,0:T(8,128)(2,1)S(1)}, u32[]{:S(2)}, u32[]{:S(2)}) %collective-permute-start.4) | collective-permute-done | bytes 49184 | tf_op jit(solution)/shard_map/ppermute | solution.py:36
  38.9 1.3 %shard_map.113 = (f32[3,256,128]{2,1,0:T(8,128)S(1)}, bf16[192,128]{1,0:T(8,128)(2,1)S(1)}, bf16[192,128]{1,0:T(8,128)(2,1)S(1)}, bf16[192,128]{1,0:T(8,128)(2,1)S(1)}) custom-call(s32[8,768]{1,0:T(8,128)S(1)} %bitcast.8, bf16[3,256,128]{2,1,0:T(8,128)(2,1)S(1)} %get-tuple-element.18.low_ref, bf16[3,256,128]{2,1,0:T(8,128)(2,1)S(1)} %get-tuple-element.19.high_ref, ...), custom_call_target="tpu_custom_call" | custom-call | flops 2000000000 | bytes 1062912 | tf_op jit(solution)/shard_map/pallas_call | solution.py:53
  40.2 1.0 shard_map.114
  41.2 2.3 %collective-permute-start.13 = (bf16[192,256]{1,0:T(8,128)(2,1)S(1)}, bf16[192,256]{1,0:T(8,128)(2,1)S(1)}, u32[]{:S(2)}, u32[]{:S(2)}) collective-permute-start(bf16[192,256]{1,0:T(8,128)(2,1)S(1)} %get-tuple-element.23.grads_ref.mine_ref), channel_id=1, source_target_pairs={{0,4},{4,0},{1,5},{5,1},{2,6},{6,2},{3,7},{7,3},{8,12},{12,8},{9,1... | collective-permute-start | bytes 294920 | tf_op jit(solution)/shard_map/ppermute | solution.py:378
  43.5 0.9 collective-permute-done.13.other_ref
  44.4 1.5 %weight.1 = bf16[8,128,256]{2,1,0:T(8,128)(2,1)S(1)} custom-call(bf16[192,256]{1,0:T(8,128)(2,1)S(1)} %get-tuple-element.23.grads_ref.mine_ref, bf16[192,256]{1,0:T(8,128)(2,1)S(1)} %collective-permute-done.13.other_ref, bf16[8,192,256]{2,1,0:T(8,128)(2,1)S(1)} %all-to-all-done.x_ref), custom_call_target="tpu_custom_call" | custom-call | flops 201326592 | bytes 1000000 | tf_op jit(solution)/shard_map/weight/pallas_call | solution.py:305
  45.9 19.8 %all_to_all.15 = bf16[8,128,256]{2,1,0:T(8,128)(2,1)S(1)} all-to-all(bf16[8,128,256]{2,1,0:T(8,128)(2,1)S(1)} %weight.1), channel_id=1, replica_groups={{24,16,8,0,56,48,40,32},{44,52,60,4,12,20,28,36},{25,17,9,1,57,49,41,33..., dimensions={0} | all-to-all | bytes 1048576 | tf_op jit(solution)/shard_map/all_to_all | solution.py:40
  65.7 0.7 shard_map.116
  66.4 14.9 %all-to-all-start.2 = ((bf16[16,8,256]{2,1,0:T(8,128)(2,1)}), bf16[16,8,256]{2,1,0:T(8,128)(2,1)S(1)}, u32[]{:S(2)}, u32[]{:S(2)}) async-start(bf16[16,8,256]{2,1,0:T(8,128)(2,1)} %shard_map.116), calls=%async_computation.2 | async-start | bytes 131072 | tf_op jit(solution)/shard_map/all_to_all | solution.py:40
  81.3 1.3 %collective-permute-start.6 = (bf16[192,128]{1,0:T(8,128)(2,1)S(1)}, bf16[192,128]{1,0:T(8,128)(2,1)S(1)}, u32[]{:S(2)}, u32[]{:S(2)}) collective-permute-start(bf16[192,128]{1,0:T(8,128)(2,1)S(1)} %get-tuple-element.25), channel_id=1, source_target_pairs={{4,0},{8,4},{12,8},{16,12},{20,16},{24,20},{28,24},{32,28},{36,32}... | collective-permute-start | bytes 147464 | tf_op jit(solution)/shard_map/ppermute | solution.py:31
  82.6 0.7 collective-permute-start.7
  83.2 1.3 %collective-permute-start.8 = (bf16[192,128]{1,0:T(8,128)(2,1)S(1)}, bf16[192,128]{1,0:T(8,128)(2,1)S(1)}, u32[]{:S(2)}, u32[]{:S(2)}) collective-permute-start(bf16[192,128]{1,0:T(8,128)(2,1)S(1)} %get-tuple-element.26), channel_id=1, source_target_pairs={{128,0},{132,4},{136,8},{140,12},{144,16},{148,20},{152,24},{156,2... | collective-permute-start | bytes 147464 | tf_op jit(solution)/shard_map/ppermute | solution.py:31
  84.5 0.7 collective-permute-start.9
  85.2 1.3 %collective-permute-start.10 = (bf16[192,128]{1,0:T(8,128)(2,1)S(1)}, bf16[192,128]{1,0:T(8,128)(2,1)S(1)}, u32[]{:S(2)}, u32[]{:S(2)}) collective-permute-start(bf16[192,128]{1,0:T(8,128)(2,1)S(1)} %get-tuple-element.27), channel_id=1, source_target_pairs={{256,0},{260,4},{264,8},{268,12},{272,16},{276,20},{280,24},{284,2... | collective-permute-start | bytes 147464 | tf_op jit(solution)/shard_map/ppermute | solution.py:31
  86.5 0.7 collective-permute-start.11
  87.2 1.3 %collective-permute-start.12 = (bf16[192,128]{1,0:T(8,128)(2,1)S(1)}, bf16[192,128]{1,0:T(8,128)(2,1)S(1)}, u32[]{:S(2)}, u32[]{:S(2)}) collective-permute-start(bf16[192,128]{1,0:T(8,128)(2,1)S(1)} %get-tuple-element.28), channel_id=1, source_target_pairs={{512,0},{516,4},{520,8},{524,12},{528,16},{532,20},{536,24},{540,2... | collective-permute-start | bytes 147464 | tf_op jit(solution)/shard_map/ppermute | solution.py:31
  88.5 2.8 %collective-permute-done.8.refs_2_ = bf16[192,128]{1,0:T(8,128)(2,1)S(1)} collective-permute-done((bf16[192,128]{1,0:T(8,128)(2,1)S(1)}, bf16[192,128]{1,0:T(8,128)(2,1)S(1)}, u32[]{:S(2)}, u32[]{:S(2)}) %collective-permute-start.8) | collective-permute-done | bytes 49184 | tf_op jit(solution)/shard_map/ppermute | solution.py:31
  91.3 5.3 %collective-permute-done.10.refs_4_ = bf16[192,128]{1,0:T(8,128)(2,1)S(1)} collective-permute-done((bf16[192,128]{1,0:T(8,128)(2,1)S(1)}, bf16[192,128]{1,0:T(8,128)(2,1)S(1)}, u32[]{:S(2)}, u32[]{:S(2)}) %collective-permute-start.10) | collective-permute-done | bytes 49184 | tf_op jit(solution)/shard_map/ppermute | solution.py:31
  96.6 8.0 %collective-permute-done.12.refs_6_ = bf16[192,128]{1,0:T(8,128)(2,1)S(1)} collective-permute-done((bf16[192,128]{1,0:T(8,128)(2,1)S(1)}, bf16[192,128]{1,0:T(8,128)(2,1)S(1)}, u32[]{:S(2)}, u32[]{:S(2)}) %collective-permute-start.12) | collective-permute-done | bytes 49184 | tf_op jit(solution)/shard_map/ppermute | solution.py:31
  104.6 0.7 shard_map.115
  105.4 0.6 shard_map.117
  (27 shorter events, 0.1 us)
Async XLA Ops:
  0.6 0.9 copy-start
  2.9 14.5 %copy-start.6 = (bf16[192,64]{0,1:T(8,128)(2,1)S(1)}, bf16[192,64]{0,1:T(8,128)(2,1)}, u32[]{:S(2)}) copy-start(bf16[192,64]{0,1:T(8,128)(2,1)} %param.11) | copy-start | bytes 73732
  2.9 14.5 %copy-start.7 = (bf16[192,64]{0,1:T(8,128)(2,1)S(1)}, bf16[192,64]{0,1:T(8,128)(2,1)}, u32[]{:S(2)}) copy-start(bf16[192,64]{0,1:T(8,128)(2,1)} %param.10) | copy-start | bytes 73732
  2.9 41.5 %all-to-all-start = ((bf16[8,192,256]{2,1,0:T(8,128)(2,1)}), bf16[8,192,256]{2,1,0:T(8,128)(2,1)S(1)}, u32[]{:S(2)}, u32[]{:S(2)}) async-start(bf16[8,192,256]{2,1,0:T(8,128)(2,1)} %spread.1), calls=%async_computation | async-start | bytes 1572864 | tf_op jit(solution)/shard_map/all_to_all | solution.py:40
  17.5 17.4 %copy-start.1 = (bf16[192,256]{1,0:T(8,128)(2,1)S(1)}, bf16[192,256]{1,0:T(8,128)(2,1)}, u32[]{:S(2)}) copy-start(bf16[192,256]{1,0:T(8,128)(2,1)} %q_ref.1) | copy-start | bytes 294916
  17.5 17.4 %copy-start.2 = (bf16[192,256]{1,0:T(8,128)(2,1)S(1)}, bf16[192,256]{1,0:T(8,128)(2,1)}, u32[]{:S(2)}) copy-start(bf16[192,256]{1,0:T(8,128)(2,1)} %go_ref.1) | copy-start | bytes 294916
  17.5 17.4 %copy-start.3 = (bf16[192,256]{1,0:T(8,128)(2,1)S(1)}, bf16[192,256]{1,0:T(8,128)(2,1)}, u32[]{:S(2)}) copy-start(bf16[192,256]{1,0:T(8,128)(2,1)} %ao_ref.1) | copy-start | bytes 294916
  17.5 17.4 %copy-start.5 = (f32[192,4]{0,1:T(4,128)S(1)}, f32[192,4]{0,1:T(4,128)}, u32[]{:S(2)}) copy-start(f32[192,4]{0,1:T(4,128)} %param.14) | copy-start | bytes 9220
  17.6 10.0 %collective-permute-start.2 = (bf16[192,128]{1,0:T(8,128)(2,1)S(1)}, bf16[192,128]{1,0:T(8,128)(2,1)S(1)}, u32[]{:S(2)}, u32[]{:S(2)}) collective-permute-start(bf16[192,128]{1,0:T(8,128)(2,1)S(1)} %shard_map.111.kv_ref), channel_id=1, source_target_pairs={{0,256},{64,320},{128,384},{192,448},{256,0},{320,64},{384,128},{4... | collective-permute-start | bytes 147464 | tf_op jit(solution)/shard_map/ppermute | solution.py:36
  19.7 16.2 %collective-permute-start = (bf16[192,128]{1,0:T(8,128)(2,1)S(1)}, bf16[192,128]{1,0:T(8,128)(2,1)S(1)}, u32[]{:S(2)}, u32[]{:S(2)}) collective-permute-start(bf16[192,128]{1,0:T(8,128)(2,1)S(1)} %shard_map.111.kv_ref), channel_id=1, source_target_pairs={{0,128},{4,132},{8,136},{12,140},{16,144},{20,148},{24,152},{28,15... | collective-permute-start | bytes 147464 | tf_op jit(solution)/shard_map/ppermute | solution.py:31
  24.8 11.1 %collective-permute-start.1 = (bf16[192,128]{1,0:T(8,128)(2,1)S(1)}, bf16[192,128]{1,0:T(8,128)(2,1)S(1)}, u32[]{:S(2)}, u32[]{:S(2)}) collective-permute-start(bf16[192,128]{1,0:T(8,128)(2,1)S(1)} %shard_map.111.kv_ref), channel_id=1, source_target_pairs={{512,640},{516,644},{520,648},{524,652},{528,656},{532,660},{536,6... | collective-permute-start | bytes 147464 | tf_op jit(solution)/shard_map/ppermute | solution.py:31
  25.4 10.5 %collective-permute-start.3 = (bf16[192,128]{1,0:T(8,128)(2,1)S(1)}, bf16[192,128]{1,0:T(8,128)(2,1)S(1)}, u32[]{:S(2)}, u32[]{:S(2)}) collective-permute-start(bf16[192,128]{1,0:T(8,128)(2,1)S(1)} %shard_map.111.kv_ref), channel_id=1, source_target_pairs={{256,512},{320,576},{384,640},{448,704},{512,768},{576,832},{640,8... | collective-permute-start | bytes 147464 | tf_op jit(solution)/shard_map/ppermute | solution.py:36
  26.1 14.1 %collective-permute-start.5 = (bf16[192,128]{1,0:T(8,128)(2,1)S(1)}, bf16[192,128]{1,0:T(8,128)(2,1)S(1)}, u32[]{:S(2)}, u32[]{:S(2)}) collective-permute-start(bf16[192,128]{1,0:T(8,128)(2,1)S(1)} %shard_map.111.kv_ref), channel_id=1, source_target_pairs={{0,4},{4,8},{8,12},{12,16},{16,20},{20,24},{24,28},{28,32},{32,36}... | collective-permute-start | bytes 147464 | tf_op jit(solution)/shard_map/ppermute | solution.py:31
  27.6 11.3 %collective-permute-start.4 = (bf16[192,128]{1,0:T(8,128)(2,1)S(1)}, bf16[192,128]{1,0:T(8,128)(2,1)S(1)}, u32[]{:S(2)}, u32[]{:S(2)}) collective-permute-start(bf16[192,128]{1,0:T(8,128)(2,1)S(1)} %collective-permute-done.2.refs_2_), channel_id=1, source_target_pairs={{256,512},{320,576},{384,640},{448,704},{0,768},{64,832},{128,896}... | collective-permute-start | bytes 147464 | tf_op jit(solution)/shard_map/ppermute | solution.py:36
  34.9 4.0 %copy-start.4 = (s32[768,8]{0,1:T(8,128)S(1)}, s32[768,8]{0,1:T(8,128)}, u32[]{:S(2)}) copy-start(s32[768,8]{0,1:T(8,128)} %param.15) | copy-start | bytes 73732
  41.2 3.2 %collective-permute-start.13 = (bf16[192,256]{1,0:T(8,128)(2,1)S(1)}, bf16[192,256]{1,0:T(8,128)(2,1)S(1)}, u32[]{:S(2)}, u32[]{:S(2)}) collective-permute-start(bf16[192,256]{1,0:T(8,128)(2,1)S(1)} %get-tuple-element.23.grads_ref.mine_ref), channel_id=1, source_target_pairs={{0,4},{4,0},{1,5},{5,1},{2,6},{6,2},{3,7},{7,3},{8,12},{12,8},{9,1... | collective-permute-start | bytes 294920 | tf_op jit(solution)/shard_map/ppermute | solution.py:378
  66.4 39.0 %all-to-all-start.2 = ((bf16[16,8,256]{2,1,0:T(8,128)(2,1)}), bf16[16,8,256]{2,1,0:T(8,128)(2,1)S(1)}, u32[]{:S(2)}, u32[]{:S(2)}) async-start(bf16[16,8,256]{2,1,0:T(8,128)(2,1)} %shard_map.116), calls=%async_computation.2 | async-start | bytes 131072 | tf_op jit(solution)/shard_map/all_to_all | solution.py:40
  81.3 5.2 %collective-permute-start.6 = (bf16[192,128]{1,0:T(8,128)(2,1)S(1)}, bf16[192,128]{1,0:T(8,128)(2,1)S(1)}, u32[]{:S(2)}, u32[]{:S(2)}) collective-permute-start(bf16[192,128]{1,0:T(8,128)(2,1)S(1)} %get-tuple-element.25), channel_id=1, source_target_pairs={{4,0},{8,4},{12,8},{16,12},{20,16},{24,20},{28,24},{32,28},{36,32}... | collective-permute-start | bytes 147464 | tf_op jit(solution)/shard_map/ppermute | solution.py:31
  82.6 4.6 %collective-permute-start.7 = (bf16[192,128]{1,0:T(8,128)(2,1)S(1)}, bf16[192,128]{1,0:T(8,128)(2,1)S(1)}, u32[]{:S(2)}, u32[]{:S(2)}) collective-permute-start(bf16[192,128]{1,0:T(8,128)(2,1)S(1)} %get-tuple-element.25), channel_id=1, source_target_pairs={{516,512},{520,516},{524,520},{528,524},{532,528},{536,532},{540,5... | collective-permute-start | bytes 147464 | tf_op jit(solution)/shard_map/ppermute | solution.py:31
  83.2 8.1 %collective-permute-start.8 = (bf16[192,128]{1,0:T(8,128)(2,1)S(1)}, bf16[192,128]{1,0:T(8,128)(2,1)S(1)}, u32[]{:S(2)}, u32[]{:S(2)}) collective-permute-start(bf16[192,128]{1,0:T(8,128)(2,1)S(1)} %get-tuple-element.26), channel_id=1, source_target_pairs={{128,0},{132,4},{136,8},{140,12},{144,16},{148,20},{152,24},{156,2... | collective-permute-start | bytes 147464 | tf_op jit(solution)/shard_map/ppermute | solution.py:31
  84.5 6.8 %collective-permute-start.9 = (bf16[192,128]{1,0:T(8,128)(2,1)S(1)}, bf16[192,128]{1,0:T(8,128)(2,1)S(1)}, u32[]{:S(2)}, u32[]{:S(2)}) collective-permute-start(bf16[192,128]{1,0:T(8,128)(2,1)S(1)} %get-tuple-element.26), channel_id=1, source_target_pairs={{640,512},{644,516},{648,520},{652,524},{656,528},{660,532},{664,5... | collective-permute-start | bytes 147464 | tf_op jit(solution)/shard_map/ppermute | solution.py:31
  85.2 11.4 %collective-permute-start.10 = (bf16[192,128]{1,0:T(8,128)(2,1)S(1)}, bf16[192,128]{1,0:T(8,128)(2,1)S(1)}, u32[]{:S(2)}, u32[]{:S(2)}) collective-permute-start(bf16[192,128]{1,0:T(8,128)(2,1)S(1)} %get-tuple-element.27), channel_id=1, source_target_pairs={{256,0},{260,4},{264,8},{268,12},{272,16},{276,20},{280,24},{284,2... | collective-permute-start | bytes 147464 | tf_op jit(solution)/shard_map/ppermute | solution.py:31
  86.5 10.1 %collective-permute-start.11 = (bf16[192,128]{1,0:T(8,128)(2,1)S(1)}, bf16[192,128]{1,0:T(8,128)(2,1)S(1)}, u32[]{:S(2)}, u32[]{:S(2)}) collective-permute-start(bf16[192,128]{1,0:T(8,128)(2,1)S(1)} %get-tuple-element.27), channel_id=1, source_target_pairs={{768,512},{772,516},{776,520},{780,524},{784,528},{788,532},{792,5... | collective-permute-start | bytes 147464 | tf_op jit(solution)/shard_map/ppermute | solution.py:31
  87.2 17.4 %collective-permute-start.12 = (bf16[192,128]{1,0:T(8,128)(2,1)S(1)}, bf16[192,128]{1,0:T(8,128)(2,1)S(1)}, u32[]{:S(2)}, u32[]{:S(2)}) collective-permute-start(bf16[192,128]{1,0:T(8,128)(2,1)S(1)} %get-tuple-element.28), channel_id=1, source_target_pairs={{512,0},{516,4},{520,8},{524,12},{528,16},{532,20},{536,24},{540,2... | collective-permute-start | bytes 147464 | tf_op jit(solution)/shard_map/ppermute | solution.py:31

commit v8 on v7

--- a/solution.py
+++ b/solution.py
@@ -18,7 +18,7 @@
 TN = (((0,), (0,)), ((), ()))
 Y_ORDERS = ((3, 2, 1, 0, 7, 6, 5, 4), (5, 6, 7, 0, 1, 2, 3, 4))
 Z_ORDER = (8, 9, 10, 11, 12, 13, 14, 15, 0, 1, 2, 3, 4, 5, 6, 7)
-X_ORDER = (4, 5, 6, 7, 0, 1, 2, 3)
+X_ORDER = (5, 4, 6, 7, 1, 0, 2, 3)
 LANES = 128
 WINDOWS = 2
 VMEM_LIMIT = 16 * 2**20
@@ -213,64 +213,83 @@
     return grad_q
 
 
+def comes_late(distances):
+    return lax.axis_index(KV) - distances[1] >= lax.axis_size(KV) // 2
+
+
 def far_kernel(distances, chosen_ref, low_ref, high_ref, rows_ref, part_ref, *refs):
-    *step_refs, traded_ref, fetched_ref, passed_ref, out_ref = refs[:6]
-    back_refs, (two_ref, four_ref) = refs[6 : 5 + LEVELS], refs[-2:]
-    sums = dict(zip(range(1, LEVELS), refs[5 + LEVELS : -2]))
+    early_ref, traded_ref, fetched_ref, passed_ref, out_ref, *back_refs = refs[: 4 + LEVELS]
+    four_ref, *totals = refs[4 + LEVELS :]
+    sums = dict(zip(range(1, LEVELS), totals))
     at, quarter = lax.axis_index("z"), lax.axis_size("z") // 4
     in_second = jnp.logical_and(at >= quarter, at < 2 * quarter)
-    is_late = lax.axis_index(KV) - distances[1] >= lax.axis_size(KV) // 2
-    two_ref[...] = jnp.where(is_late, step_refs[1][...], step_refs[0][...])
     four_ref[...] = jnp.where(in_second, traded_ref[...], fetched_ref[...])
-    far_refs = {1: two_ref, 2: four_ref, 3: passed_ref}
-    for level in sums:
-        sums[level][...] = jnp.zeros_like(sums[level])
+    far_refs = {1: early_ref, 2: four_ref, 3: passed_ref}
+    for total in totals:
+        total[...] = jnp.zeros_like(total)
     blocks = low_ref.shape[0]
-    places = chosen_places(chosen_ref, distances, tuple(sums), blocks)
-    for b in range(blocks):
-        grad_q = far_terms(places[b], far_refs, low_ref, high_ref, rows_ref, sums, b)
-        out_ref[b] = part_ref[b] + grad_q
-    for level, back_ref in zip(sums, back_refs):
-        back_ref[...] = sums[level][...].astype(back_ref.dtype)
+    is_late = comes_late(distances)
+
+    def attend(levels):
+        places = chosen_places(chosen_ref, distances, levels, blocks)
+        for b in range(blocks):
+            grad_q = far_terms(places[b], far_refs, low_ref, high_ref, rows_ref, sums, b)
+            out_ref[b] = part_ref[b] + grad_q
+
+    pl.when(is_late)(lambda: attend((2, 3)))
+    pl.when(jnp.logical_not(is_late))(lambda: attend((1, 2, 3)))
+    for total, back_ref in zip(totals, back_refs):
+        back_ref[...] = total[...].astype(back_ref.dtype)
 
 
 def attend_far(distances, chosen, low, high, rows, part, far):
     kv = far[0]
     shape = (jax.ShapeDtypeStruct(part.shape, part.dtype),)
     shape += (jax.ShapeDtypeStruct(kv.shape, jnp.bfloat16),) * (LEVELS - 1)
-    scratch = [pltpu.VMEM(kv.shape, jnp.float32)] * (LEVELS - 1) + [pltpu.VMEM(kv.shape, kv.dtype)] * 2
+    scratch = [pltpu.VMEM(kv.shape, kv.dtype)] + [pltpu.VMEM(kv.shape, jnp.float32)] * (LEVELS - 1)
     kernel = functools.partial(far_kernel, distances)
     args = (chosen, low, high, rows, part, *far)
     return call(kernel, 2 * 10**9, shape, *args, scratch=scratch)
 
 
-def near_kernel(distances, chosen_ref, low_ref, high_ref, rows_ref, part_ref, one_ref, gq_ref, back_ref, total):
+def near_kernel(distances, chosen_ref, low_ref, high_ref, rows_ref, part_ref, *refs):
+    one_ref, late_ref, found_ref, gq_ref, one_back_ref, two_back_ref, *totals = refs
     blocks, heads = low_ref.shape[0], low_ref.shape[1] // BLOCK
     lane = lax.broadcasted_iota(jnp.int32, (BLOCK, 2 * DH), 1)
-    total[...] = jnp.zeros_like(total)
-    places = chosen_places(chosen_ref, distances, (0,), blocks)
-    for b in range(blocks):
-        rows = slice(b * BLOCK, (b + 1) * BLOCK)
-        grad_q = far_terms(places[b], {0: one_ref}, low_ref, high_ref, rows_ref, {0: total}, b)
-        grad_q = (part_ref[b] + grad_q) * DH ** (-0.5)
-        for pair in range(heads // 2):
-            first = grad_q[2 * pair * BLOCK : (2 * pair + 1) * BLOCK]
-            second = grad_q[(2 * pair + 1) * BLOCK : (2 * pair + 2) * BLOCK]
-            gq_ref[rows, pair * 2 * DH : (pair + 1) * 2 * DH] = jnp.where(
-                lane < DH, first, pltpu.roll(second, DH, 1)
-            ).astype(gq_ref.dtype)
-    back_ref[...] = total[...].astype(back_ref.dtype)
-
-
-def attend_near(distances, chosen, low, high, rows, part, near):
+    sums = dict(enumerate(totals))
+    is_late = comes_late(distances)
+    for total in totals:
+        total[...] = jnp.zeros_like(total)
+
+    def attend(levels):
+        places = chosen_places(chosen_ref, distances, levels, blocks)
+        for b in range(blocks):
+            rows = slice(b * BLOCK, (b + 1) * BLOCK)
+            near_refs = {0: one_ref, 1: late_ref}
+            grad_q = far_terms(places[b], near_refs, low_ref, high_ref, rows_ref, sums, b)
+            grad_q = (part_ref[b] + grad_q) * DH ** (-0.5)
+            for pair in range(heads // 2):
+                first = grad_q[2 * pair * BLOCK : (2 * pair + 1) * BLOCK]
+                second = grad_q[(2 * pair + 1) * BLOCK : (2 * pair + 2) * BLOCK]
+                gq_ref[rows, pair * 2 * DH : (pair + 1) * 2 * DH] = jnp.where(
+                    lane < DH, first, pltpu.roll(second, DH, 1)
+                ).astype(gq_ref.dtype)
+
+    pl.when(is_late)(lambda: attend((0, 1)))
+    pl.when(jnp.logical_not(is_late))(lambda: attend((0,)))
+    one_back_ref[...] = totals[0][...].astype(one_back_ref.dtype)
+    two_back = totals[1][...].astype(two_back_ref.dtype)
+    two_back_ref[...] = jnp.where(is_late, two_back, found_ref[...])
+
+
+def attend_near(distances, chosen, low, high, rows, part, near, late, found):
     tokens, width = low.shape[0] * BLOCK, low.shape[1] * DH // BLOCK
-    shape = (
-        jax.ShapeDtypeStruct((tokens, width), jnp.bfloat16),
-        jax.ShapeDtypeStruct(near.shape, jnp.bfloat16),
-    )
+    shape = (jax.ShapeDtypeStruct((tokens, width), jnp.bfloat16),)
+    shape += (jax.ShapeDtypeStruct(near.shape, jnp.bfloat16),) * 2
     kernel = functools.partial(near_kernel, distances)
-    args = (chosen, low, high, rows, part, near)
-    return call(kernel, 10**9, shape, *args, scratch=[pltpu.VMEM(near.shape, jnp.float32)])
+    args = (chosen, low, high, rows, part, near, late, found)
+    scratch = [pltpu.VMEM(near.shape, jnp.float32)] * 2
+    return call(kernel, 10**9, shape, *args, scratch=scratch)
 
 
 def weight_kernel(mine_ref, other_ref, x_ref, out_ref, held, done):
@@ -367,13 +386,14 @@
     traded = between(key_pair, quarters, ((0, 1), (1, 0)))
     passed = between(traded, quarters, ((1, 2), (0, 3)))
     fetched = between(key_pair, quarters, ((1, 2), (2, 3)))
-    far = [*steps, traded, fetched, passed]
+    far = [steps[0], traded, fetched, passed]
     sent = spread(layer_input, out_rows, ys, cores, peers)
     whole_input = exchanged(sent, ("c", "x"), [list(X_ORDER)])
     *staged, part, grad_own = attend_own(queries, grad_out, attn_out, log_sum.T, key_pair)
-    part, *back = attend_far(distances, chosen.T, *staged, part, far)
-    grads, back_near = attend_near(distances, chosen.T, *staged, part, near)
-    back = [back_near, *back]
+    part, found, *back_far = attend_far(distances, chosen.T, *staged, part, far)
+    near = (near, steps[1], found)
+    grads, *back = attend_near(distances, chosen.T, *staged, part, *near)
+    back += back_far
     route = [(i, cores - 1 - i) for i in range(cores)]
     other = lax.ppermute(grads, "c", route)
     parts = weight(grads, other, whole_input, ys)

time: 107 us -> 109 us (1.019)
  waiting for transfers between devices: 20.1 us -> 21.4 us
    all_to_all x2, starting transfers between devices: 29.4 us -> 31.8 us  [exchanged(): lax.all_to_all(tiles, axis, split_axis=0, concat_axis=0, tiled=True, axis...]
where the time goes in v8:
time: 109 us; the launch traced here: 108 us
  starting transfers between devices  56.3 us (52%)
  waiting for transfers between devices  21.4 us (20%)
  blocking collectives  20.1 us (18%)
  Pallas kernels  8.27 us (8%)
    all_to_all x2, starting transfers between devices, exchanged(): lax.all_to_all(tiles, axis, split_axis=0, concat_axis=0, tiled=True, axis...  31.8 us
    all_to_all x1, blocking collectives, exchanged(): lax.all_to_all(tiles, axis, split_axis=0, concat_axis=0, tiled=True, axis...  20.1 us
    ppermute x10, waiting for transfers between devices, shifted(): return lax.ppermute(block, axis, route)  16.4 us
    ppermute x10, starting transfers between devices, shifted(): return lax.ppermute(block, axis, route)  13.3 us
    ppermute x3, starting transfers between devices, between(): return lax.ppermute(block, 'z', route)  8.96 us
    pallas_call x7, Pallas kernels, call(): pl.pallas_call(kernel, out_shape=out_shape, in_specs=[pl.BlockSpec(memory...  5.48 us
    ppermute x3, waiting for transfers between devices, between(): return lax.ppermute(block, 'z', route)  4.03 us
    ppermute x1, starting transfers between devices, shards(): other = lax.ppermute(grads, 'c', route)  2.22 us
  transfers between devices with their start and end apart: 16, of which 6 were waited for; matrix products, arithmetic and copies ran while one was open for 0% of the time, Pallas kernels for 4%

profile of v8, /device:TPU:6, one launch (start us, length us, event | category | flops | bytes accessed | tf_op | source)
XLA Modules:
  0.0 108.0 jit_solution(4265362381192152946)
XLA Ops:
  0.6 0.9 copy-done
  1.6 1.3 %spread.1 = bf16[8,192,256]{2,1,0:T(8,128)(2,1)} custom-call(bf16[192,512]{1,0:T(8,128)(2,1)S(1)} %copy-done), custom_call_target="tpu_custom_call" | custom-call | flops 100663296 | bytes 1000000 | tf_op jit(solution)/shard_map/spread/pallas_call | solution.py:103
  2.9 15.6 %all-to-all-start = ((bf16[8,192,256]{2,1,0:T(8,128)(2,1)}), bf16[8,192,256]{2,1,0:T(8,128)(2,1)S(1)}, u32[]{:S(2)}, u32[]{:S(2)}) async-start(bf16[8,192,256]{2,1,0:T(8,128)(2,1)} %spread.1), calls=%async_computation | async-start | bytes 1572864 | tf_op jit(solution)/shard_map/all_to_all | solution.py:40
  18.7 2.1 %collective-permute-start.1 = (bf16[192,128]{1,0:T(8,128)(2,1)S(1)}, bf16[192,128]{1,0:T(8,128)(2,1)S(1)}, u32[]{:S(2)}, u32[]{:S(2)}) collective-permute-start(bf16[192,128]{1,0:T(8,128)(2,1)S(1)} %shard_map.111.kv_ref), channel_id=1, source_target_pairs={{0,256},{64,320},{128,384},{192,448},{256,0},{320,64},{384,128},{4... | collective-permute-start | bytes 147464 | tf_op jit(solution)/shard_map/ppermute | solution.py:36
  20.7 4.0 %collective-permute-start = (bf16[192,128]{1,0:T(8,128)(2,1)S(1)}, bf16[192,128]{1,0:T(8,128)(2,1)S(1)}, u32[]{:S(2)}, u32[]{:S(2)}) collective-permute-start(bf16[192,128]{1,0:T(8,128)(2,1)S(1)} %shard_map.111.kv_ref), channel_id=1, source_target_pairs={{0,128},{4,132},{8,136},{12,140},{16,144},{20,148},{24,152},{28,15... | collective-permute-start | bytes 147464 | tf_op jit(solution)/shard_map/ppermute | solution.py:31
  24.8 0.7 collective-permute-start.2
  25.4 1.5 %collective-permute-start.4 = (bf16[192,128]{1,0:T(8,128)(2,1)S(1)}, bf16[192,128]{1,0:T(8,128)(2,1)S(1)}, u32[]{:S(2)}, u32[]{:S(2)}) collective-permute-start(bf16[192,128]{1,0:T(8,128)(2,1)S(1)} %shard_map.111.kv_ref), channel_id=1, source_target_pairs={{0,4},{4,8},{8,12},{12,16},{16,20},{20,24},{24,28},{28,32},{32,36}... | collective-permute-start | bytes 147464 | tf_op jit(solution)/shard_map/ppermute | solution.py:31
  26.9 0.7 collective-permute-start.5
  27.6 1.1 %collective-permute-done.1.refs_1_ = bf16[192,128]{1,0:T(8,128)(2,1)S(1)} collective-permute-done((bf16[192,128]{1,0:T(8,128)(2,1)S(1)}, bf16[192,128]{1,0:T(8,128)(2,1)S(1)}, u32[]{:S(2)}, u32[]{:S(2)}) %collective-permute-start.1) | collective-permute-done | bytes 49184 | tf_op jit(solution)/shard_map/ppermute | solution.py:36
  28.7 6.2 %collective-permute-start.3 = (bf16[192,128]{1,0:T(8,128)(2,1)S(1)}, bf16[192,128]{1,0:T(8,128)(2,1)S(1)}, u32[]{:S(2)}, u32[]{:S(2)}) collective-permute-start(bf16[192,128]{1,0:T(8,128)(2,1)S(1)} %collective-permute-done.1.refs_1_), channel_id=1, source_target_pairs={{256,512},{320,576},{384,640},{448,704},{0,768},{64,832},{128,896}... | collective-permute-start | bytes 147464 | tf_op jit(solution)/shard_map/ppermute | solution.py:36
  35.0 1.0 shard_map.112
  36.0 2.9 %collective-permute-done.3.refs_3_ = bf16[192,128]{1,0:T(8,128)(2,1)S(1)} collective-permute-done((bf16[192,128]{1,0:T(8,128)(2,1)S(1)}, bf16[192,128]{1,0:T(8,128)(2,1)S(1)}, u32[]{:S(2)}, u32[]{:S(2)}) %collective-permute-start.3) | collective-permute-done | bytes 49184 | tf_op jit(solution)/shard_map/ppermute | solution.py:36
  38.9 1.3 %shard_map.113 = (f32[3,256,128]{2,1,0:T(8,128)S(1)}, bf16[192,128]{1,0:T(8,128)(2,1)S(1)}, bf16[192,128]{1,0:T(8,128)(2,1)S(1)}, bf16[192,128]{1,0:T(8,128)(2,1)S(1)}) custom-call(s32[8,768]{1,0:T(8,128)S(1)} %bitcast.8, bf16[3,256,128]{2,1,0:T(8,128)(2,1)S(1)} %get-tuple-element.19.low_ref, bf16[3,256,128]{2,1,0:T(8,128)(2,1)S(1)} %get-tuple-element.20.high_ref, ...), custom_call_target="tpu_custom_call" | custom-call | flops 2000000000 | bytes 1013760 | tf_op jit(solution)/shard_map/pallas_call | solution.py:53
  40.3 1.1 shard_map.114
  41.3 2.2 %collective-permute-start.13 = (bf16[192,256]{1,0:T(8,128)(2,1)S(1)}, bf16[192,256]{1,0:T(8,128)(2,1)S(1)}, u32[]{:S(2)}, u32[]{:S(2)}) collective-permute-start(bf16[192,256]{1,0:T(8,128)(2,1)S(1)} %get-tuple-element.25.grads_ref.mine_ref), channel_id=1, source_target_pairs={{0,4},{4,0},{1,5},{5,1},{2,6},{6,2},{3,7},{7,3},{8,12},{12,8},{9,1... | collective-permute-start | bytes 294920 | tf_op jit(solution)/shard_map/ppermute | solution.py:398
  43.6 1.0 collective-permute-done.13.other_ref
  44.5 1.5 %weight.1 = bf16[8,128,256]{2,1,0:T(8,128)(2,1)S(1)} custom-call(bf16[192,256]{1,0:T(8,128)(2,1)S(1)} %get-tuple-element.25.grads_ref.mine_ref, bf16[192,256]{1,0:T(8,128)(2,1)S(1)} %collective-permute-done.13.other_ref, bf16[8,192,256]{2,1,0:T(8,128)(2,1)S(1)} %all-to-all-done.x_ref), custom_call_target="tpu_custom_call" | custom-call | flops 201326592 | bytes 1000000 | tf_op jit(solution)/shard_map/weight/pallas_call | solution.py:324
  46.0 20.1 %all_to_all.15 = bf16[8,128,256]{2,1,0:T(8,128)(2,1)S(1)} all-to-all(bf16[8,128,256]{2,1,0:T(8,128)(2,1)S(1)} %weight.1), channel_id=1, replica_groups={{24,16,8,0,56,48,40,32},{44,52,60,4,12,20,28,36},{25,17,9,1,57,49,41,33..., dimensions={0} | all-to-all | bytes 1048576 | tf_op jit(solution)/shard_map/all_to_all | solution.py:40
  66.1 0.7 shard_map.116
  66.8 16.2 %all-to-all-start.2 = ((bf16[16,8,256]{2,1,0:T(8,128)(2,1)}), bf16[16,8,256]{2,1,0:T(8,128)(2,1)S(1)}, u32[]{:S(2)}, u32[]{:S(2)}) async-start(bf16[16,8,256]{2,1,0:T(8,128)(2,1)} %shard_map.116), calls=%async_computation.2 | async-start | bytes 131072 | tf_op jit(solution)/shard_map/all_to_all | solution.py:40
  83.0 1.3 %collective-permute-start.6 = (bf16[192,128]{1,0:T(8,128)(2,1)S(1)}, bf16[192,128]{1,0:T(8,128)(2,1)S(1)}, u32[]{:S(2)}, u32[]{:S(2)}) collective-permute-start(bf16[192,128]{1,0:T(8,128)(2,1)S(1)} %get-tuple-element.27), channel_id=1, source_target_pairs={{4,0},{8,4},{12,8},{16,12},{20,16},{24,20},{28,24},{32,28},{36,32}... | collective-permute-start | bytes 147464 | tf_op jit(solution)/shard_map/ppermute | solution.py:31
  84.3 0.7 collective-permute-start.7
  84.9 1.3 %collective-permute-start.8 = (bf16[192,128]{1,0:T(8,128)(2,1)S(1)}, bf16[192,128]{1,0:T(8,128)(2,1)S(1)}, u32[]{:S(2)}, u32[]{:S(2)}) collective-permute-start(bf16[192,128]{1,0:T(8,128)(2,1)S(1)} %get-tuple-element.28), channel_id=1, source_target_pairs={{128,0},{132,4},{136,8},{140,12},{144,16},{148,20},{152,24},{156,2... | collective-permute-start | bytes 147464 | tf_op jit(solution)/shard_map/ppermute | solution.py:31
  86.2 0.7 collective-permute-start.9
  86.9 1.3 %collective-permute-start.10 = (bf16[192,128]{1,0:T(8,128)(2,1)S(1)}, bf16[192,128]{1,0:T(8,128)(2,1)S(1)}, u32[]{:S(2)}, u32[]{:S(2)}) collective-permute-start(bf16[192,128]{1,0:T(8,128)(2,1)S(1)} %get-tuple-element.29), channel_id=1, source_target_pairs={{256,0},{260,4},{264,8},{268,12},{272,16},{276,20},{280,24},{284,2... | collective-permute-start | bytes 147464 | tf_op jit(solution)/shard_map/ppermute | solution.py:31
  88.2 0.7 collective-permute-start.11
  88.9 1.3 %collective-permute-start.12 = (bf16[192,128]{1,0:T(8,128)(2,1)S(1)}, bf16[192,128]{1,0:T(8,128)(2,1)S(1)}, u32[]{:S(2)}, u32[]{:S(2)}) collective-permute-start(bf16[192,128]{1,0:T(8,128)(2,1)S(1)} %get-tuple-element.30), channel_id=1, source_target_pairs={{512,0},{516,4},{520,8},{524,12},{528,16},{532,20},{536,24},{540,2... | collective-permute-start | bytes 147464 | tf_op jit(solution)/shard_map/ppermute | solution.py:31
  90.2 2.8 %collective-permute-done.8.refs_2_ = bf16[192,128]{1,0:T(8,128)(2,1)S(1)} collective-permute-done((bf16[192,128]{1,0:T(8,128)(2,1)S(1)}, bf16[192,128]{1,0:T(8,128)(2,1)S(1)}, u32[]{:S(2)}, u32[]{:S(2)}) %collective-permute-start.8) | collective-permute-done | bytes 49184 | tf_op jit(solution)/shard_map/ppermute | solution.py:31
  93.0 5.6 %collective-permute-done.10.refs_4_ = bf16[192,128]{1,0:T(8,128)(2,1)S(1)} collective-permute-done((bf16[192,128]{1,0:T(8,128)(2,1)S(1)}, bf16[192,128]{1,0:T(8,128)(2,1)S(1)}, u32[]{:S(2)}, u32[]{:S(2)}) %collective-permute-start.10) | collective-permute-done | bytes 49184 | tf_op jit(solution)/shard_map/ppermute | solution.py:31
  98.6 8.0 %collective-permute-done.12.refs_6_ = bf16[192,128]{1,0:T(8,128)(2,1)S(1)} collective-permute-done((bf16[192,128]{1,0:T(8,128)(2,1)S(1)}, bf16[192,128]{1,0:T(8,128)(2,1)S(1)}, u32[]{:S(2)}, u32[]{:S(2)}) %collective-permute-start.12) | collective-permute-done | bytes 49184 | tf_op jit(solution)/shard_map/ppermute | solution.py:31
  106.6 0.7 shard_map.115
  107.4 0.6 shard_map.117
  (27 shorter events, 0.2 us)
Async XLA Ops:
  0.6 0.9 copy-start
  2.9 15.6 %copy-start.6 = (bf16[192,64]{0,1:T(8,128)(2,1)S(1)}, bf16[192,64]{0,1:T(8,128)(2,1)}, u32[]{:S(2)}) copy-start(bf16[192,64]{0,1:T(8,128)(2,1)} %param.11) | copy-start | bytes 73732
  2.9 15.6 %copy-start.7 = (bf16[192,64]{0,1:T(8,128)(2,1)S(1)}, bf16[192,64]{0,1:T(8,128)(2,1)}, u32[]{:S(2)}) copy-start(bf16[192,64]{0,1:T(8,128)(2,1)} %param.10) | copy-start | bytes 73732
  2.9 41.6 %all-to-all-start = ((bf16[8,192,256]{2,1,0:T(8,128)(2,1)}), bf16[8,192,256]{2,1,0:T(8,128)(2,1)S(1)}, u32[]{:S(2)}, u32[]{:S(2)}) async-start(bf16[8,192,256]{2,1,0:T(8,128)(2,1)} %spread.1), calls=%async_computation | async-start | bytes 1572864 | tf_op jit(solution)/shard_map/all_to_all | solution.py:40
  18.5 16.4 %copy-start.1 = (bf16[192,256]{1,0:T(8,128)(2,1)S(1)}, bf16[192,256]{1,0:T(8,128)(2,1)}, u32[]{:S(2)}) copy-start(bf16[192,256]{1,0:T(8,128)(2,1)} %q_ref.1) | copy-start | bytes 294916
  18.5 16.4 %copy-start.2 = (bf16[192,256]{1,0:T(8,128)(2,1)S(1)}, bf16[192,256]{1,0:T(8,128)(2,1)}, u32[]{:S(2)}) copy-start(bf16[192,256]{1,0:T(8,128)(2,1)} %go_ref.1) | copy-start | bytes 294916
  18.5 16.4 %copy-start.3 = (bf16[192,256]{1,0:T(8,128)(2,1)S(1)}, bf16[192,256]{1,0:T(8,128)(2,1)}, u32[]{:S(2)}) copy-start(bf16[192,256]{1,0:T(8,128)(2,1)} %ao_ref.1) | copy-start | bytes 294916
  18.5 16.4 %copy-start.5 = (f32[192,4]{0,1:T(4,128)S(1)}, f32[192,4]{0,1:T(4,128)}, u32[]{:S(2)}) copy-start(f32[192,4]{0,1:T(4,128)} %param.14) | copy-start | bytes 9220
  18.7 10.0 %collective-permute-start.1 = (bf16[192,128]{1,0:T(8,128)(2,1)S(1)}, bf16[192,128]{1,0:T(8,128)(2,1)S(1)}, u32[]{:S(2)}, u32[]{:S(2)}) collective-permute-start(bf16[192,128]{1,0:T(8,128)(2,1)S(1)} %shard_map.111.kv_ref), channel_id=1, source_target_pairs={{0,256},{64,320},{128,384},{192,448},{256,0},{320,64},{384,128},{4... | collective-permute-start | bytes 147464 | tf_op jit(solution)/shard_map/ppermute | solution.py:36
  20.7 15.3 %collective-permute-start = (bf16[192,128]{1,0:T(8,128)(2,1)S(1)}, bf16[192,128]{1,0:T(8,128)(2,1)S(1)}, u32[]{:S(2)}, u32[]{:S(2)}) collective-permute-start(bf16[192,128]{1,0:T(8,128)(2,1)S(1)} %shard_map.111.kv_ref), channel_id=1, source_target_pairs={{0,128},{4,132},{8,136},{12,140},{16,144},{20,148},{24,152},{28,15... | collective-permute-start | bytes 147464 | tf_op jit(solution)/shard_map/ppermute | solution.py:31
  24.8 11.2 %collective-permute-start.2 = (bf16[192,128]{1,0:T(8,128)(2,1)S(1)}, bf16[192,128]{1,0:T(8,128)(2,1)S(1)}, u32[]{:S(2)}, u32[]{:S(2)}) collective-permute-start(bf16[192,128]{1,0:T(8,128)(2,1)S(1)} %shard_map.111.kv_ref), channel_id=1, source_target_pairs={{256,512},{320,576},{384,640},{448,704},{512,768},{576,832},{640,8... | collective-permute-start | bytes 147464 | tf_op jit(solution)/shard_map/ppermute | solution.py:36
  25.4 14.8 %collective-permute-start.4 = (bf16[192,128]{1,0:T(8,128)(2,1)S(1)}, bf16[192,128]{1,0:T(8,128)(2,1)S(1)}, u32[]{:S(2)}, u32[]{:S(2)}) collective-permute-start(bf16[192,128]{1,0:T(8,128)(2,1)S(1)} %shard_map.111.kv_ref), channel_id=1, source_target_pairs={{0,4},{4,8},{8,12},{12,16},{16,20},{20,24},{24,28},{28,32},{32,36}... | collective-permute-start | bytes 147464 | tf_op jit(solution)/shard_map/ppermute | solution.py:31
  26.9 13.3 %collective-permute-start.5 = (bf16[192,128]{1,0:T(8,128)(2,1)S(1)}, bf16[192,128]{1,0:T(8,128)(2,1)S(1)}, u32[]{:S(2)}, u32[]{:S(2)}) collective-permute-start(bf16[192,128]{1,0:T(8,128)(2,1)S(1)} %shard_map.111.kv_ref), channel_id=1, source_target_pairs={{512,640},{516,644},{520,648},{524,652},{528,656},{532,660},{536,6... | collective-permute-start | bytes 147464 | tf_op jit(solution)/shard_map/ppermute | solution.py:31
  28.7 10.3 %collective-permute-start.3 = (bf16[192,128]{1,0:T(8,128)(2,1)S(1)}, bf16[192,128]{1,0:T(8,128)(2,1)S(1)}, u32[]{:S(2)}, u32[]{:S(2)}) collective-permute-start(bf16[192,128]{1,0:T(8,128)(2,1)S(1)} %collective-permute-done.1.refs_1_), channel_id=1, source_target_pairs={{256,512},{320,576},{384,640},{448,704},{0,768},{64,832},{128,896}... | collective-permute-start | bytes 147464 | tf_op jit(solution)/shard_map/ppermute | solution.py:36
  35.0 4.0 %copy-start.4 = (s32[768,8]{0,1:T(8,128)S(1)}, s32[768,8]{0,1:T(8,128)}, u32[]{:S(2)}) copy-start(s32[768,8]{0,1:T(8,128)} %param.15) | copy-start | bytes 73732
  41.3 3.2 %collective-permute-start.13 = (bf16[192,256]{1,0:T(8,128)(2,1)S(1)}, bf16[192,256]{1,0:T(8,128)(2,1)S(1)}, u32[]{:S(2)}, u32[]{:S(2)}) collective-permute-start(bf16[192,256]{1,0:T(8,128)(2,1)S(1)} %get-tuple-element.25.grads_ref.mine_ref), channel_id=1, source_target_pairs={{0,4},{4,0},{1,5},{5,1},{2,6},{6,2},{3,7},{7,3},{8,12},{12,8},{9,1... | collective-permute-start | bytes 294920 | tf_op jit(solution)/shard_map/ppermute | solution.py:398
  66.8 40.6 %all-to-all-start.2 = ((bf16[16,8,256]{2,1,0:T(8,128)(2,1)}), bf16[16,8,256]{2,1,0:T(8,128)(2,1)S(1)}, u32[]{:S(2)}, u32[]{:S(2)}) async-start(bf16[16,8,256]{2,1,0:T(8,128)(2,1)} %shard_map.116), calls=%async_computation.2 | async-start | bytes 131072 | tf_op jit(solution)/shard_map/all_to_all | solution.py:40
  83.0 5.2 %collective-permute-start.6 = (bf16[192,128]{1,0:T(8,128)(2,1)S(1)}, bf16[192,128]{1,0:T(8,128)(2,1)S(1)}, u32[]{:S(2)}, u32[]{:S(2)}) collective-permute-start(bf16[192,128]{1,0:T(8,128)(2,1)S(1)} %get-tuple-element.27), channel_id=1, source_target_pairs={{4,0},{8,4},{12,8},{16,12},{20,16},{24,20},{28,24},{32,28},{36,32}... | collective-permute-start | bytes 147464 | tf_op jit(solution)/shard_map/ppermute | solution.py:31
  84.3 4.6 %collective-permute-start.7 = (bf16[192,128]{1,0:T(8,128)(2,1)S(1)}, bf16[192,128]{1,0:T(8,128)(2,1)S(1)}, u32[]{:S(2)}, u32[]{:S(2)}) collective-permute-start(bf16[192,128]{1,0:T(8,128)(2,1)S(1)} %get-tuple-element.27), channel_id=1, source_target_pairs={{516,512},{520,516},{524,520},{528,524},{532,528},{536,532},{540,5... | collective-permute-start | bytes 147464 | tf_op jit(solution)/shard_map/ppermute | solution.py:31
  84.9 8.1 %collective-permute-start.8 = (bf16[192,128]{1,0:T(8,128)(2,1)S(1)}, bf16[192,128]{1,0:T(8,128)(2,1)S(1)}, u32[]{:S(2)}, u32[]{:S(2)}) collective-permute-start(bf16[192,128]{1,0:T(8,128)(2,1)S(1)} %get-tuple-element.28), channel_id=1, source_target_pairs={{128,0},{132,4},{136,8},{140,12},{144,16},{148,20},{152,24},{156,2... | collective-permute-start | bytes 147464 | tf_op jit(solution)/shard_map/ppermute | solution.py:31
  86.2 6.8 %collective-permute-start.9 = (bf16[192,128]{1,0:T(8,128)(2,1)S(1)}, bf16[192,128]{1,0:T(8,128)(2,1)S(1)}, u32[]{:S(2)}, u32[]{:S(2)}) collective-permute-start(bf16[192,128]{1,0:T(8,128)(2,1)S(1)} %get-tuple-element.28), channel_id=1, source_target_pairs={{640,512},{644,516},{648,520},{652,524},{656,528},{660,532},{664,5... | collective-permute-start | bytes 147464 | tf_op jit(solution)/shard_map/ppermute | solution.py:31
  86.9 11.7 %collective-permute-start.10 = (bf16[192,128]{1,0:T(8,128)(2,1)S(1)}, bf16[192,128]{1,0:T(8,128)(2,1)S(1)}, u32[]{:S(2)}, u32[]{:S(2)}) collective-permute-start(bf16[192,128]{1,0:T(8,128)(2,1)S(1)} %get-tuple-element.29), channel_id=1, source_target_pairs={{256,0},{260,4},{264,8},{268,12},{272,16},{276,20},{280,24},{284,2... | collective-permute-start | bytes 147464 | tf_op jit(solution)/shard_map/ppermute | solution.py:31
  88.2 10.4 %collective-permute-start.11 = (bf16[192,128]{1,0:T(8,128)(2,1)S(1)}, bf16[192,128]{1,0:T(8,128)(2,1)S(1)}, u32[]{:S(2)}, u32[]{:S(2)}) collective-permute-start(bf16[192,128]{1,0:T(8,128)(2,1)S(1)} %get-tuple-element.29), channel_id=1, source_target_pairs={{768,512},{772,516},{776,520},{780,524},{784,528},{788,532},{792,5... | collective-permute-start | bytes 147464 | tf_op jit(solution)/shard_map/ppermute | solution.py:31
  88.9 17.7 %collective-permute-start.12 = (bf16[192,128]{1,0:T(8,128)(2,1)S(1)}, bf16[192,128]{1,0:T(8,128)(2,1)S(1)}, u32[]{:S(2)}, u32[]{:S(2)}) collective-permute-start(bf16[192,128]{1,0:T(8,128)(2,1)S(1)} %get-tuple-element.30), channel_id=1, source_target_pairs={{512,0},{516,4},{520,8},{524,12},{528,16},{532,20},{536,24},{540,2... | collective-permute-start | bytes 147464 | tf_op jit(solution)/shard_map/ppermute | solution.py:31

commit v9 on v8

--- a/solution.py
+++ b/solution.py
@@ -18,7 +18,7 @@
 TN = (((0,), (0,)), ((), ()))
 Y_ORDERS = ((3, 2, 1, 0, 7, 6, 5, 4), (5, 6, 7, 0, 1, 2, 3, 4))
 Z_ORDER = (8, 9, 10, 11, 12, 13, 14, 15, 0, 1, 2, 3, 4, 5, 6, 7)
-X_ORDER = (5, 4, 6, 7, 1, 0, 2, 3)
+X_ORDER = (5, 1, 6, 2, 7, 3, 4, 0)
 LANES = 128
 WINDOWS = 2
 VMEM_LIMIT = 16 * 2**20
@@ -205,12 +205,26 @@
     return places
 
 
-def far_terms(places, far_refs, low_ref, high_ref, rows_ref, sums, b):
-    kv = jnp.concatenate([far_refs[level][at, :] for (level, _), at in places.items()], axis=0)
-    grad_q, grad_kv = terms(kv, low_ref[b], high_ref[b], rows_ref[b, :1], rows_ref[b, 1:])
-    for n, ((level, _), at) in enumerate(places.items()):
-        sums[level][at, :] += grad_kv[n * BLOCK : (n + 1) * BLOCK]
-    return grad_q
+def far_terms(places, far_refs, low_ref, high_ref, rows_ref, sums):
+    count = range(len(places))
+    kvs = [
+        jnp.concatenate([far_refs[level][at, :] for (level, _), at in row.items()], axis=0)
+        for row in places
+    ]
+    lows, highs = [low_ref[b] for b in count], [high_ref[b] for b in count]
+    scores = [dot(kvs[b], lows[b], NT) for b in count]
+    dweights = [dot(kvs[b], highs[b], NT) for b in count]
+    weights = [jnp.exp(scores[b] - rows_ref[b, :1]) for b in count]
+    dscores = [
+        (weights[b] * (dweights[b] - rows_ref[b, 1:])).astype(jnp.bfloat16) for b in count
+    ]
+    weights = [one.astype(jnp.bfloat16) for one in weights]
+    grad_qs = [dot(dscores[b], kvs[b], TN) for b in count]
+    grad_kvs = [dot(dscores[b], lows[b]) + dot(weights[b], highs[b]) for b in count]
+    for row, grad_kv in zip(places, grad_kvs):
+        for n, ((level, _), at) in enumerate(row.items()):
+            sums[level][at, :] += grad_kv[n * BLOCK : (n + 1) * BLOCK]
+    return grad_qs
 
 
 def comes_late(distances):
@@ -232,8 +246,8 @@
 
     def attend(levels):
         places = chosen_places(chosen_ref, distances, levels, blocks)
-        for b in range(blocks):
-            grad_q = far_terms(places[b], far_refs, low_ref, high_ref, rows_ref, sums, b)
+        grads = far_terms(places, far_refs, low_ref, high_ref, rows_ref, sums)
+        for b, grad_q in enumerate(grads):
             out_ref[b] = part_ref[b] + grad_q
 
     pl.when(is_late)(lambda: attend((2, 3)))
@@ -263,10 +277,10 @@
 
     def attend(levels):
         places = chosen_places(chosen_ref, distances, levels, blocks)
-        for b in range(blocks):
+        near_refs = {0: one_ref, 1: late_ref}
+        grads = far_terms(places, near_refs, low_ref, high_ref, rows_ref, sums)
+        for b, grad_q in enumerate(grads):
             rows = slice(b * BLOCK, (b + 1) * BLOCK)
-            near_refs = {0: one_ref, 1: late_ref}
-            grad_q = far_terms(places[b], near_refs, low_ref, high_ref, rows_ref, sums, b)
             grad_q = (part_ref[b] + grad_q) * DH ** (-0.5)
             for pair in range(heads // 2):
                 first = grad_q[2 * pair * BLOCK : (2 * pair + 1) * BLOCK]

time: 109 us -> 108 us (level)
  no operation moved by 1% of the time
where the time goes in v9:
time: 108 us; the launch traced here: 107 us
  starting transfers between devices  56 us (52%)
  waiting for transfers between devices  21.4 us (20%)
  blocking collectives  20.1 us (19%)
  Pallas kernels  7.86 us (7%)
    all_to_all x2, starting transfers between devices, exchanged(): lax.all_to_all(tiles, axis, split_axis=0, concat_axis=0, tiled=True, axis...  31.5 us
    all_to_all x1, blocking collectives, exchanged(): lax.all_to_all(tiles, axis, split_axis=0, concat_axis=0, tiled=True, axis...  20.1 us
    ppermute x10, waiting for transfers between devices, shifted(): return lax.ppermute(block, axis, route)  16.4 us
    ppermute x10, starting transfers between devices, shifted(): return lax.ppermute(block, axis, route)  13.3 us
    ppermute x3, starting transfers between devices, between(): return lax.ppermute(block, 'z', route)  8.96 us
    pallas_call x7, Pallas kernels, call(): pl.pallas_call(kernel, out_shape=out_shape, in_specs=[pl.BlockSpec(memory...  5.07 us
    ppermute x3, waiting for transfers between devices, between(): return lax.ppermute(block, 'z', route)  4.03 us
    ppermute x1, starting transfers between devices, shards(): other = lax.ppermute(grads, 'c', route)  2.22 us
  transfers between devices with their start and end apart: 16, of which 6 were waited for; matrix products, arithmetic and copies ran while one was open for 0% of the time, Pallas kernels for 4%

profile of v9, /device:TPU:6, one launch (start us, length us, event | category | flops | bytes accessed | tf_op | source)
XLA Modules:
  0.0 107.3 jit_solution(1052226328440120253)
XLA Ops:
  0.6 0.9 copy-done
  1.6 1.3 %spread.1 = bf16[8,192,256]{2,1,0:T(8,128)(2,1)} custom-call(bf16[192,512]{1,0:T(8,128)(2,1)S(1)} %copy-done), custom_call_target="tpu_custom_call" | custom-call | flops 100663296 | bytes 1000000 | tf_op jit(solution)/shard_map/spread/pallas_call | solution.py:103
  2.9 15.6 %all-to-all-start = ((bf16[8,192,256]{2,1,0:T(8,128)(2,1)}), bf16[8,192,256]{2,1,0:T(8,128)(2,1)S(1)}, u32[]{:S(2)}, u32[]{:S(2)}) async-start(bf16[8,192,256]{2,1,0:T(8,128)(2,1)} %spread.1), calls=%async_computation | async-start | bytes 1572864 | tf_op jit(solution)/shard_map/all_to_all | solution.py:40
  18.7 2.1 %collective-permute-start.1 = (bf16[192,128]{1,0:T(8,128)(2,1)S(1)}, bf16[192,128]{1,0:T(8,128)(2,1)S(1)}, u32[]{:S(2)}, u32[]{:S(2)}) collective-permute-start(bf16[192,128]{1,0:T(8,128)(2,1)S(1)} %shard_map.111.kv_ref), channel_id=1, source_target_pairs={{0,256},{64,320},{128,384},{192,448},{256,0},{320,64},{384,128},{4... | collective-permute-start | bytes 147464 | tf_op jit(solution)/shard_map/ppermute | solution.py:36
  20.7 4.0 %collective-permute-start = (bf16[192,128]{1,0:T(8,128)(2,1)S(1)}, bf16[192,128]{1,0:T(8,128)(2,1)S(1)}, u32[]{:S(2)}, u32[]{:S(2)}) collective-permute-start(bf16[192,128]{1,0:T(8,128)(2,1)S(1)} %shard_map.111.kv_ref), channel_id=1, source_target_pairs={{0,128},{4,132},{8,136},{12,140},{16,144},{20,148},{24,152},{28,15... | collective-permute-start | bytes 147464 | tf_op jit(solution)/shard_map/ppermute | solution.py:31
  24.8 0.7 collective-permute-start.2
  25.4 1.5 %collective-permute-start.4 = (bf16[192,128]{1,0:T(8,128)(2,1)S(1)}, bf16[192,128]{1,0:T(8,128)(2,1)S(1)}, u32[]{:S(2)}, u32[]{:S(2)}) collective-permute-start(bf16[192,128]{1,0:T(8,128)(2,1)S(1)} %shard_map.111.kv_ref), channel_id=1, source_target_pairs={{0,4},{4,8},{8,12},{12,16},{16,20},{20,24},{24,28},{28,32},{32,36}... | collective-permute-start | bytes 147464 | tf_op jit(solution)/shard_map/ppermute | solution.py:31
  26.9 0.7 collective-permute-start.5
  27.6 1.1 %collective-permute-done.1.refs_1_ = bf16[192,128]{1,0:T(8,128)(2,1)S(1)} collective-permute-done((bf16[192,128]{1,0:T(8,128)(2,1)S(1)}, bf16[192,128]{1,0:T(8,128)(2,1)S(1)}, u32[]{:S(2)}, u32[]{:S(2)}) %collective-permute-start.1) | collective-permute-done | bytes 49184 | tf_op jit(solution)/shard_map/ppermute | solution.py:36
  28.7 6.2 %collective-permute-start.3 = (bf16[192,128]{1,0:T(8,128)(2,1)S(1)}, bf16[192,128]{1,0:T(8,128)(2,1)S(1)}, u32[]{:S(2)}, u32[]{:S(2)}) collective-permute-start(bf16[192,128]{1,0:T(8,128)(2,1)S(1)} %collective-permute-done.1.refs_1_), channel_id=1, source_target_pairs={{256,512},{320,576},{384,640},{448,704},{0,768},{64,832},{128,896}... | collective-permute-start | bytes 147464 | tf_op jit(solution)/shard_map/ppermute | solution.py:36
  35.0 1.0 shard_map.112
  36.0 2.9 %collective-permute-done.3.refs_3_ = bf16[192,128]{1,0:T(8,128)(2,1)S(1)} collective-permute-done((bf16[192,128]{1,0:T(8,128)(2,1)S(1)}, bf16[192,128]{1,0:T(8,128)(2,1)S(1)}, u32[]{:S(2)}, u32[]{:S(2)}) %collective-permute-start.3) | collective-permute-done | bytes 49184 | tf_op jit(solution)/shard_map/ppermute | solution.py:36
  38.9 1.2 %shard_map.113 = (f32[3,256,128]{2,1,0:T(8,128)S(1)}, bf16[192,128]{1,0:T(8,128)(2,1)S(1)}, bf16[192,128]{1,0:T(8,128)(2,1)S(1)}, bf16[192,128]{1,0:T(8,128)(2,1)S(1)}) custom-call(s32[8,768]{1,0:T(8,128)S(1)} %bitcast.8, bf16[3,256,128]{2,1,0:T(8,128)(2,1)S(1)} %get-tuple-element.19.low_ref, bf16[3,256,128]{2,1,0:T(8,128)(2,1)S(1)} %get-tuple-element.20.high_ref, ...), custom_call_target="tpu_custom_call" | custom-call | flops 2000000000 | bytes 1013760 | tf_op jit(solution)/shard_map/pallas_call | solution.py:53
  40.2 0.7 shard_map.114
  40.9 2.2 %collective-permute-start.13 = (bf16[192,256]{1,0:T(8,128)(2,1)S(1)}, bf16[192,256]{1,0:T(8,128)(2,1)S(1)}, u32[]{:S(2)}, u32[]{:S(2)}) collective-permute-start(bf16[192,256]{1,0:T(8,128)(2,1)S(1)} %get-tuple-element.25.grads_ref.mine_ref), channel_id=1, source_target_pairs={{0,4},{4,0},{1,5},{5,1},{2,6},{6,2},{3,7},{7,3},{8,12},{12,8},{9,1... | collective-permute-start | bytes 294920 | tf_op jit(solution)/shard_map/ppermute | solution.py:412
  43.2 1.0 collective-permute-done.13.other_ref
  44.1 1.5 %weight.1 = bf16[8,128,256]{2,1,0:T(8,128)(2,1)S(1)} custom-call(bf16[192,256]{1,0:T(8,128)(2,1)S(1)} %get-tuple-element.25.grads_ref.mine_ref, bf16[192,256]{1,0:T(8,128)(2,1)S(1)} %collective-permute-done.13.other_ref, bf16[8,192,256]{2,1,0:T(8,128)(2,1)S(1)} %all-to-all-done.x_ref), custom_call_target="tpu_custom_call" | custom-call | flops 201326592 | bytes 1000000 | tf_op jit(solution)/shard_map/weight/pallas_call | solution.py:338
  45.6 20.1 %all_to_all.15 = bf16[8,128,256]{2,1,0:T(8,128)(2,1)S(1)} all-to-all(bf16[8,128,256]{2,1,0:T(8,128)(2,1)S(1)} %weight.1), channel_id=1, replica_groups={{24,16,8,0,56,48,40,32},{44,52,60,4,12,20,28,36},{25,17,9,1,57,49,41,33..., dimensions={0} | all-to-all | bytes 1048576 | tf_op jit(solution)/shard_map/all_to_all | solution.py:40
  65.7 0.7 shard_map.116
  66.4 15.9 %all-to-all-start.2 = ((bf16[16,8,256]{2,1,0:T(8,128)(2,1)}), bf16[16,8,256]{2,1,0:T(8,128)(2,1)S(1)}, u32[]{:S(2)}, u32[]{:S(2)}) async-start(bf16[16,8,256]{2,1,0:T(8,128)(2,1)} %shard_map.116), calls=%async_computation.2 | async-start | bytes 131072 | tf_op jit(solution)/shard_map/all_to_all | solution.py:40
  82.3 1.3 %collective-permute-start.6 = (bf16[192,128]{1,0:T(8,128)(2,1)S(1)}, bf16[192,128]{1,0:T(8,128)(2,1)S(1)}, u32[]{:S(2)}, u32[]{:S(2)}) collective-permute-start(bf16[192,128]{1,0:T(8,128)(2,1)S(1)} %get-tuple-element.27), channel_id=1, source_target_pairs={{4,0},{8,4},{12,8},{16,12},{20,16},{24,20},{28,24},{32,28},{36,32}... | collective-permute-start | bytes 147464 | tf_op jit(solution)/shard_map/ppermute | solution.py:31
  83.6 0.7 collective-permute-start.7
  84.2 1.3 %collective-permute-start.8 = (bf16[192,128]{1,0:T(8,128)(2,1)S(1)}, bf16[192,128]{1,0:T(8,128)(2,1)S(1)}, u32[]{:S(2)}, u32[]{:S(2)}) collective-permute-start(bf16[192,128]{1,0:T(8,128)(2,1)S(1)} %get-tuple-element.28), channel_id=1, source_target_pairs={{128,0},{132,4},{136,8},{140,12},{144,16},{148,20},{152,24},{156,2... | collective-permute-start | bytes 147464 | tf_op jit(solution)/shard_map/ppermute | solution.py:31
  85.5 0.7 collective-permute-start.9
  86.2 1.3 %collective-permute-start.10 = (bf16[192,128]{1,0:T(8,128)(2,1)S(1)}, bf16[192,128]{1,0:T(8,128)(2,1)S(1)}, u32[]{:S(2)}, u32[]{:S(2)}) collective-permute-start(bf16[192,128]{1,0:T(8,128)(2,1)S(1)} %get-tuple-element.29), channel_id=1, source_target_pairs={{256,0},{260,4},{264,8},{268,12},{272,16},{276,20},{280,24},{284,2... | collective-permute-start | bytes 147464 | tf_op jit(solution)/shard_map/ppermute | solution.py:31
  87.5 0.7 collective-permute-start.11
  88.2 1.3 %collective-permute-start.12 = (bf16[192,128]{1,0:T(8,128)(2,1)S(1)}, bf16[192,128]{1,0:T(8,128)(2,1)S(1)}, u32[]{:S(2)}, u32[]{:S(2)}) collective-permute-start(bf16[192,128]{1,0:T(8,128)(2,1)S(1)} %get-tuple-element.30), channel_id=1, source_target_pairs={{512,0},{516,4},{520,8},{524,12},{528,16},{532,20},{536,24},{540,2... | collective-permute-start | bytes 147464 | tf_op jit(solution)/shard_map/ppermute | solution.py:31
  89.5 2.8 %collective-permute-done.8.refs_2_ = bf16[192,128]{1,0:T(8,128)(2,1)S(1)} collective-permute-done((bf16[192,128]{1,0:T(8,128)(2,1)S(1)}, bf16[192,128]{1,0:T(8,128)(2,1)S(1)}, u32[]{:S(2)}, u32[]{:S(2)}) %collective-permute-start.8) | collective-permute-done | bytes 49184 | tf_op jit(solution)/shard_map/ppermute | solution.py:31
  92.3 5.6 %collective-permute-done.10.refs_4_ = bf16[192,128]{1,0:T(8,128)(2,1)S(1)} collective-permute-done((bf16[192,128]{1,0:T(8,128)(2,1)S(1)}, bf16[192,128]{1,0:T(8,128)(2,1)S(1)}, u32[]{:S(2)}, u32[]{:S(2)}) %collective-permute-start.10) | collective-permute-done | bytes 49184 | tf_op jit(solution)/shard_map/ppermute | solution.py:31
  97.9 8.0 %collective-permute-done.12.refs_6_ = bf16[192,128]{1,0:T(8,128)(2,1)S(1)} collective-permute-done((bf16[192,128]{1,0:T(8,128)(2,1)S(1)}, bf16[192,128]{1,0:T(8,128)(2,1)S(1)}, u32[]{:S(2)}, u32[]{:S(2)}) %collective-permute-start.12) | collective-permute-done | bytes 49184 | tf_op jit(solution)/shard_map/ppermute | solution.py:31
  105.9 0.7 shard_map.115
  106.7 0.6 shard_map.117
  (27 shorter events, 0.2 us)
Async XLA Ops:
  0.6 0.9 copy-start
  2.9 15.6 %copy-start.6 = (bf16[192,64]{0,1:T(8,128)(2,1)S(1)}, bf16[192,64]{0,1:T(8,128)(2,1)}, u32[]{:S(2)}) copy-start(bf16[192,64]{0,1:T(8,128)(2,1)} %param.11) | copy-start | bytes 73732
  2.9 15.6 %copy-start.7 = (bf16[192,64]{0,1:T(8,128)(2,1)S(1)}, bf16[192,64]{0,1:T(8,128)(2,1)}, u32[]{:S(2)}) copy-start(bf16[192,64]{0,1:T(8,128)(2,1)} %param.10) | copy-start | bytes 73732
  2.9 41.2 %all-to-all-start = ((bf16[8,192,256]{2,1,0:T(8,128)(2,1)}), bf16[8,192,256]{2,1,0:T(8,128)(2,1)S(1)}, u32[]{:S(2)}, u32[]{:S(2)}) async-start(bf16[8,192,256]{2,1,0:T(8,128)(2,1)} %spread.1), calls=%async_computation | async-start | bytes 1572864 | tf_op jit(solution)/shard_map/all_to_all | solution.py:40
  18.5 16.4 %copy-start.1 = (bf16[192,256]{1,0:T(8,128)(2,1)S(1)}, bf16[192,256]{1,0:T(8,128)(2,1)}, u32[]{:S(2)}) copy-start(bf16[192,256]{1,0:T(8,128)(2,1)} %q_ref.1) | copy-start | bytes 294916
  18.5 16.4 %copy-start.2 = (bf16[192,256]{1,0:T(8,128)(2,1)S(1)}, bf16[192,256]{1,0:T(8,128)(2,1)}, u32[]{:S(2)}) copy-start(bf16[192,256]{1,0:T(8,128)(2,1)} %go_ref.1) | copy-start | bytes 294916
  18.5 16.4 %copy-start.3 = (bf16[192,256]{1,0:T(8,128)(2,1)S(1)}, bf16[192,256]{1,0:T(8,128)(2,1)}, u32[]{:S(2)}) copy-start(bf16[192,256]{1,0:T(8,128)(2,1)} %ao_ref.1) | copy-start | bytes 294916
  18.5 16.4 %copy-start.5 = (f32[192,4]{0,1:T(4,128)S(1)}, f32[192,4]{0,1:T(4,128)}, u32[]{:S(2)}) copy-start(f32[192,4]{0,1:T(4,128)} %param.14) | copy-start | bytes 9220
  18.7 10.0 %collective-permute-start.1 = (bf16[192,128]{1,0:T(8,128)(2,1)S(1)}, bf16[192,128]{1,0:T(8,128)(2,1)S(1)}, u32[]{:S(2)}, u32[]{:S(2)}) collective-permute-start(bf16[192,128]{1,0:T(8,128)(2,1)S(1)} %shard_map.111.kv_ref), channel_id=1, source_target_pairs={{0,256},{64,320},{128,384},{192,448},{256,0},{320,64},{384,128},{4... | collective-permute-start | bytes 147464 | tf_op jit(solution)/shard_map/ppermute | solution.py:36
  20.7 15.3 %collective-permute-start = (bf16[192,128]{1,0:T(8,128)(2,1)S(1)}, bf16[192,128]{1,0:T(8,128)(2,1)S(1)}, u32[]{:S(2)}, u32[]{:S(2)}) collective-permute-start(bf16[192,128]{1,0:T(8,128)(2,1)S(1)} %shard_map.111.kv_ref), channel_id=1, source_target_pairs={{0,128},{4,132},{8,136},{12,140},{16,144},{20,148},{24,152},{28,15... | collective-permute-start | bytes 147464 | tf_op jit(solution)/shard_map/ppermute | solution.py:31
  24.8 11.2 %collective-permute-start.2 = (bf16[192,128]{1,0:T(8,128)(2,1)S(1)}, bf16[192,128]{1,0:T(8,128)(2,1)S(1)}, u32[]{:S(2)}, u32[]{:S(2)}) collective-permute-start(bf16[192,128]{1,0:T(8,128)(2,1)S(1)} %shard_map.111.kv_ref), channel_id=1, source_target_pairs={{256,512},{320,576},{384,640},{448,704},{512,768},{576,832},{640,8... | collective-permute-start | bytes 147464 | tf_op jit(solution)/shard_map/ppermute | solution.py:36
  25.4 14.7 %collective-permute-start.4 = (bf16[192,128]{1,0:T(8,128)(2,1)S(1)}, bf16[192,128]{1,0:T(8,128)(2,1)S(1)}, u32[]{:S(2)}, u32[]{:S(2)}) collective-permute-start(bf16[192,128]{1,0:T(8,128)(2,1)S(1)} %shard_map.111.kv_ref), channel_id=1, source_target_pairs={{0,4},{4,8},{8,12},{12,16},{16,20},{20,24},{24,28},{28,32},{32,36}... | collective-permute-start | bytes 147464 | tf_op jit(solution)/shard_map/ppermute | solution.py:31
  26.9 13.3 %collective-permute-start.5 = (bf16[192,128]{1,0:T(8,128)(2,1)S(1)}, bf16[192,128]{1,0:T(8,128)(2,1)S(1)}, u32[]{:S(2)}, u32[]{:S(2)}) collective-permute-start(bf16[192,128]{1,0:T(8,128)(2,1)S(1)} %shard_map.111.kv_ref), channel_id=1, source_target_pairs={{512,640},{516,644},{520,648},{524,652},{528,656},{532,660},{536,6... | collective-permute-start | bytes 147464 | tf_op jit(solution)/shard_map/ppermute | solution.py:31
  28.7 10.3 %collective-permute-start.3 = (bf16[192,128]{1,0:T(8,128)(2,1)S(1)}, bf16[192,128]{1,0:T(8,128)(2,1)S(1)}, u32[]{:S(2)}, u32[]{:S(2)}) collective-permute-start(bf16[192,128]{1,0:T(8,128)(2,1)S(1)} %collective-permute-done.1.refs_1_), channel_id=1, source_target_pairs={{256,512},{320,576},{384,640},{448,704},{0,768},{64,832},{128,896}... | collective-permute-start | bytes 147464 | tf_op jit(solution)/shard_map/ppermute | solution.py:36
  35.0 4.0 %copy-start.4 = (s32[768,8]{0,1:T(8,128)S(1)}, s32[768,8]{0,1:T(8,128)}, u32[]{:S(2)}) copy-start(s32[768,8]{0,1:T(8,128)} %param.15) | copy-start | bytes 73732
  40.9 3.2 %collective-permute-start.13 = (bf16[192,256]{1,0:T(8,128)(2,1)S(1)}, bf16[192,256]{1,0:T(8,128)(2,1)S(1)}, u32[]{:S(2)}, u32[]{:S(2)}) collective-permute-start(bf16[192,256]{1,0:T(8,128)(2,1)S(1)} %get-tuple-element.25.grads_ref.mine_ref), channel_id=1, source_target_pairs={{0,4},{4,0},{1,5},{5,1},{2,6},{6,2},{3,7},{7,3},{8,12},{12,8},{9,1... | collective-permute-start | bytes 294920 | tf_op jit(solution)/shard_map/ppermute | solution.py:412
  66.4 40.3 %all-to-all-start.2 = ((bf16[16,8,256]{2,1,0:T(8,128)(2,1)}), bf16[16,8,256]{2,1,0:T(8,128)(2,1)S(1)}, u32[]{:S(2)}, u32[]{:S(2)}) async-start(bf16[16,8,256]{2,1,0:T(8,128)(2,1)} %shard_map.116), calls=%async_computation.2 | async-start | bytes 131072 | tf_op jit(solution)/shard_map/all_to_all | solution.py:40
  82.3 5.2 %collective-permute-start.6 = (bf16[192,128]{1,0:T(8,128)(2,1)S(1)}, bf16[192,128]{1,0:T(8,128)(2,1)S(1)}, u32[]{:S(2)}, u32[]{:S(2)}) collective-permute-start(bf16[192,128]{1,0:T(8,128)(2,1)S(1)} %get-tuple-element.27), channel_id=1, source_target_pairs={{4,0},{8,4},{12,8},{16,12},{20,16},{24,20},{28,24},{32,28},{36,32}... | collective-permute-start | bytes 147464 | tf_op jit(solution)/shard_map/ppermute | solution.py:31
  83.6 4.6 %collective-permute-start.7 = (bf16[192,128]{1,0:T(8,128)(2,1)S(1)}, bf16[192,128]{1,0:T(8,128)(2,1)S(1)}, u32[]{:S(2)}, u32[]{:S(2)}) collective-permute-start(bf16[192,128]{1,0:T(8,128)(2,1)S(1)} %get-tuple-element.27), channel_id=1, source_target_pairs={{516,512},{520,516},{524,520},{528,524},{532,528},{536,532},{540,5... | collective-permute-start | bytes 147464 | tf_op jit(solution)/shard_map/ppermute | solution.py:31
  84.2 8.1 %collective-permute-start.8 = (bf16[192,128]{1,0:T(8,128)(2,1)S(1)}, bf16[192,128]{1,0:T(8,128)(2,1)S(1)}, u32[]{:S(2)}, u32[]{:S(2)}) collective-permute-start(bf16[192,128]{1,0:T(8,128)(2,1)S(1)} %get-tuple-element.28), channel_id=1, source_target_pairs={{128,0},{132,4},{136,8},{140,12},{144,16},{148,20},{152,24},{156,2... | collective-permute-start | bytes 147464 | tf_op jit(solution)/shard_map/ppermute | solution.py:31
  85.5 6.8 %collective-permute-start.9 = (bf16[192,128]{1,0:T(8,128)(2,1)S(1)}, bf16[192,128]{1,0:T(8,128)(2,1)S(1)}, u32[]{:S(2)}, u32[]{:S(2)}) collective-permute-start(bf16[192,128]{1,0:T(8,128)(2,1)S(1)} %get-tuple-element.28), channel_id=1, source_target_pairs={{640,512},{644,516},{648,520},{652,524},{656,528},{660,532},{664,5... | collective-permute-start | bytes 147464 | tf_op jit(solution)/shard_map/ppermute | solution.py:31
  86.2 11.7 %collective-permute-start.10 = (bf16[192,128]{1,0:T(8,128)(2,1)S(1)}, bf16[192,128]{1,0:T(8,128)(2,1)S(1)}, u32[]{:S(2)}, u32[]{:S(2)}) collective-permute-start(bf16[192,128]{1,0:T(8,128)(2,1)S(1)} %get-tuple-element.29), channel_id=1, source_target_pairs={{256,0},{260,4},{264,8},{268,12},{272,16},{276,20},{280,24},{284,2... | collective-permute-start | bytes 147464 | tf_op jit(solution)/shard_map/ppermute | solution.py:31
  87.5 10.4 %collective-permute-start.11 = (bf16[192,128]{1,0:T(8,128)(2,1)S(1)}, bf16[192,128]{1,0:T(8,128)(2,1)S(1)}, u32[]{:S(2)}, u32[]{:S(2)}) collective-permute-start(bf16[192,128]{1,0:T(8,128)(2,1)S(1)} %get-tuple-element.29), channel_id=1, source_target_pairs={{768,512},{772,516},{776,520},{780,524},{784,528},{788,532},{792,5... | collective-permute-start | bytes 147464 | tf_op jit(solution)/shard_map/ppermute | solution.py:31
  88.2 17.7 %collective-permute-start.12 = (bf16[192,128]{1,0:T(8,128)(2,1)S(1)}, bf16[192,128]{1,0:T(8,128)(2,1)S(1)}, u32[]{:S(2)}, u32[]{:S(2)}) collective-permute-start(bf16[192,128]{1,0:T(8,128)(2,1)S(1)} %get-tuple-element.30), channel_id=1, source_target_pairs={{512,0},{516,4},{520,8},{524,12},{528,16},{532,20},{536,24},{540,2... | collective-permute-start | bytes 147464 | tf_op jit(solution)/shard_map/ppermute | solution.py:31
